TPU v7x, 128 devices: a whole 4x4x4 slice. The times are simulated.
128 devices in a mesh: fs: 16 (over z, y), tp: 8 (over x, core).
Axes of the slice: x: 4, y: 4, z: 4, core: 2. Of those that a mesh axis runs over, the one named last changes fastest.
Arguments:
- inputs: bfloat16 [8192, 3072], P('fs', 'tp'), may hold values from -6 to 6
- cotangent: bfloat16 [8192, 3072], P('fs', 'tp'), may hold values from -6 to 6
- pre_norm: bfloat16 [8192, 3072], P('fs', 'tp'), may hold values from -28 to 28, as said below
- gate_pre: bfloat16 [8192, 5632], P('fs', 'tp'), may hold values from -8 to 8
- value_pre: bfloat16 [8192, 5632], P('fs', 'tp'), may hold values from -6 to 6
- gate_weight: bfloat16 [3072, 5632], P('fs', 'tp'), may hold values from -0.109375 to 0.109375
- value_weight: bfloat16 [3072, 5632], P('fs', 'tp'), may hold values from -0.109375 to 0.109375
- down_weight: bfloat16 [5632, 3072], P('tp', 'fs'), may hold values from -0.078125 to 0.078125
- conv_taps: float32 [3, 5632], P(None, 'tp'), may hold values from -3.5 to 3.5
- norm_gain: float32 [3072], P('tp'), may hold values from 0.1 to 1.9
Outputs:
- grad_input: bfloat16 [8192, 3072], P('fs', 'tp')
- grad_gate: float32 [3072, 5632], P('fs', 'tp')
- grad_value: float32 [3072, 5632], P('fs', 'tp')
- grad_down: float32 [5632, 3072], P('tp', 'fs')
- grad_taps: float32 [3, 5632], P(None, 'tp')
- grad_gain: float32 [3072], P('tp')
Inputs may be any that keep to these rules, and one draw needn't show every extreme that they name: `pre_norm`: every entry has magnitude 0.075 or more.
All inputs are finite; a program needn't handle non-finite values.
Results may differ from a plain program's by a relative error of at most 0.014.
Values may be sent and summed in bfloat16 or wider, within the bound.
No kernel may reach another device: no remote copies, remote signals or barrier semaphores. Data moves between devices by JAX's collectives and lax.ppermute only.
A program may use at most 128 MiB of HBM per device.

v0:
```python
import jax
import jax.numpy as jnp
from jax import lax
from jax.experimental import pallas as pl
from jax.experimental.pallas import tpu as pltpu
from jax.sharding import Mesh
from jax.sharding import PartitionSpec as P


D = 3072
SEQ = 128
EPSILON = 1e-06
F32 = jnp.float32
BF16 = jnp.bfloat16
FS = ("z", "y")
TP = ("x", "c")
ROWS = 192
HALF = ROWS // 2
UNITS = 704
WIDE = 768
TOKS = 512
COLS = 384


VMEM = pl.BlockSpec(memory_space=pltpu.VMEM)
SMEM = pl.BlockSpec(memory_space=pltpu.SMEM)


def moved(value, axis, by):
    return lax.ppermute(value, axis, [(i, (i + by) % 4) for i in range(4)])


def swapped(value):
    return lax.ppermute(value, "c", [(0, 1), (1, 0)])


def gathered(own, axis):
    half = own.shape[0] // 2
    left, right = moved(own, axis, 1), moved(own, axis, -1)
    far_low, far_high = moved(left[:half], axis, 1), moved(right[half:], axis, -1)
    return [own, right, far_low, far_high, left]


def plus(a, b):
    return (a.astype(F32) + b.astype(F32)).astype(BF16)


def reduced(own, after, far_low, far_high, before, axis, out=BF16):
    half = far_low.shape[0]
    from_left, from_right = moved(far_low, axis, 1), moved(far_high, axis, -1)
    to_right = jnp.concatenate([plus(after[:half], from_left), after[half:]], axis=0)
    to_left = jnp.concatenate([before[:half], plus(before[half:], from_right)], axis=0)
    got_left = moved(to_right, axis, 1)
    got_right = moved(to_left, axis, -1)
    return (own.astype(F32) + got_left.astype(F32) + got_right.astype(F32)).astype(out)


def in_five(value):
    n = value.shape[0] // 8
    return (value[: 2 * n], value[2 * n : 4 * n], value[4 * n : 5 * n], value[5 * n : 6 * n], value[6 * n :])


def device_at(where, dz, dy):
    return (where[0] + dz) % 4, (where[1] + dy) % 4


def mix(gate, taps):
    lane = lax.broadcasted_iota(jnp.int32, gate.shape, 1)
    before = jnp.where(lane == 0, 0.0, pltpu.roll(gate, 1, 1))
    after = jnp.where(lane == SEQ - 1, 0.0, pltpu.roll(gate, SEQ - 1, 1))
    mixed = taps[:, 0:1] * before + taps[:, 1:2] * gate + taps[:, 2:3] * after
    return before, after, mixed, jax.nn.sigmoid(mixed)


STEP = 88


def hidden_body(gate_ref, value_ref, taps_ref, hidden_ref):
    for u in range(0, UNITS, STEP):
        rows = slice(u, u + STEP)
        taps = taps_ref[rows, :]
        for t in range(0, TOKS, SEQ):
            cols = slice(t, t + SEQ)
            _, _, mixed, sig = mix(gate_ref[rows, cols].astype(F32), taps)
            hidden_ref[rows, cols] = (mixed * sig * value_ref[rows, cols].astype(F32)).astype(BF16)


def arrange_body(where_ref, mine_ref, other_ref, out_ref):
    for c_off, ref in enumerate((mine_ref, other_ref)):
        for x_off in range(4):
            block = (where_ref[2] + x_off) % 4 * 2 + (where_ref[3] + c_off) % 2
            to = pl.multiple_of(block * COLS, COLS)
            out_ref[pl.ds(to, COLS), :] = ref[x_off * COLS : (x_off + 1) * COLS, :]


def back_body(down_ref, grad_ref, gate_ref, value_ref, taps_ref, out_ref, sums_ref, act_ref):
    act_ref[...] = lax.dot_general(
        down_ref[:, :UNITS],
        grad_ref[...],
        (((0,), (0,)), ((), ())),
        preferred_element_type=F32,
    )
    for u in range(0, UNITS, STEP):
        rows = slice(u, u + STEP)
        taps = taps_ref[rows, :]
        sums = [jnp.zeros((STEP, SEQ), F32)] * 3
        for t in range(0, TOKS, SEQ):
            cols = slice(t, t + SEQ)
            gate = gate_ref[rows, cols].astype(F32)
            before, after, mixed, sig = mix(gate, taps)
            grad_act = act_ref[rows, cols]
            out_ref[UNITS + u : UNITS + u + STEP, cols] = (grad_act * (mixed * sig)).astype(BF16)
            inner = (
                grad_act * value_ref[rows, cols].astype(F32) * sig * (1.0 + mixed * (1.0 - sig))
            )
            sums = [s + inner * g for s, g in zip(sums, (before, gate, after))]
            lane = lax.broadcasted_iota(jnp.int32, inner.shape, 1)
            following = jnp.where(lane == SEQ - 1, 0.0, pltpu.roll(inner, SEQ - 1, 1))
            previous = jnp.where(lane == 0, 0.0, pltpu.roll(inner, 1, 1))
            out_ref[rows, cols] = (
                taps[:, 1:2] * inner + taps[:, 0:1] * following + taps[:, 2:3] * previous
            ).astype(BF16)
        for k in range(3):
            sums_ref[rows, k : k + 1] = jnp.sum(sums[k], axis=1, keepdims=True)


def product(left, right):
    return lax.dot_general(
        left, right, (((1,), (1,)), ((), ())), preferred_element_type=F32
    ).astype(BF16)


def outer_body(inputs_ref, grad_ref, both_ref, hidden_ref, out_ref):
    out_ref[:, : 2 * UNITS] = product(inputs_ref[...], both_ref[...])
    out_ref[:, 2 * UNITS :] = product(grad_ref[...], hidden_ref[...])


def block_of(refs, dz, dy):
    def part(five, major, minor):
        ref = five[(0, 1, 2 + minor // 2, 4)[major]]
        at = (minor % 2 if major == 2 else minor) * HALF
        return ref[at : at + HALF, :]

    return jnp.concatenate([part(refs[:5], dz, dy), part(refs[5:], dy, dz)], axis=0)


def input_body(where_ref, right_ref, *rest):
    refs, (kept_ref, sent_ref) = rest[:10], rest[10:]
    where = [where_ref[k] for k in range(4)]
    for dz in range(4):
        for dy in range(4):
            zt, yt = device_at(where, dz, dy)
            at = pl.multiple_of((((zt - where[2] + 4) % 4) * 2 + yt % 2) * ROWS, ROWS)
            near = yt // 2 == where[3]
            block = jnp.dot(
                block_of(refs, dz, dy), right_ref[...], preferred_element_type=F32
            ).astype(BF16)

            @pl.when(near)
            def _():
                kept_ref[pl.ds(at, ROWS), :] = block

            @pl.when(jnp.logical_not(near))
            def _():
                sent_ref[pl.ds(at, ROWS), :] = block


PARAMS = pltpu.CompilerParams(vmem_limit_bytes=50 * 1024 * 1024)


def hidden_of(gate, value, taps):
    return pl.pallas_call(
        hidden_body,
        out_shape=jax.ShapeDtypeStruct((UNITS, TOKS), BF16),
        in_specs=[VMEM] * 3,
        out_specs=VMEM,
        compiler_params=PARAMS,
        name="hidden",
    )(gate, value, taps)


def arranged(where, mine, other):
    return pl.pallas_call(
        arrange_body,
        out_shape=jax.ShapeDtypeStruct((D, TOKS), BF16),
        in_specs=[SMEM, VMEM, VMEM],
        out_specs=VMEM,
        compiler_params=PARAMS,
        name="arrange",
    )(where, mine, other)


def back_of(down, grad, gate, value, taps):
    return pl.pallas_call(
        back_body,
        out_shape=(
            jax.ShapeDtypeStruct((2 * UNITS, TOKS), BF16),
            jax.ShapeDtypeStruct((UNITS, 3), F32),
        ),
        in_specs=[VMEM] * 5,
        out_specs=(VMEM, VMEM),
        scratch_shapes=[pltpu.VMEM((UNITS, TOKS), F32)],
        compiler_params=PARAMS,
        cost_estimate=pl.CostEstimate(
            flops=2 * D * UNITS * TOKS, bytes_accessed=12_000_000, transcendentals=UNITS * TOKS
        ),
        name="back",
    )(down, grad, gate, value, taps)


def outer_of(inputs, grad, both, hidden):
    return pl.pallas_call(
        outer_body,
        out_shape=jax.ShapeDtypeStruct((D, 3 * UNITS), BF16),
        grid=(8,),
        in_specs=[
            pl.BlockSpec((COLS, TOKS), lambda i: (i, 0)),
            pl.BlockSpec((COLS, TOKS), lambda i: (i, 0)),
            VMEM,
            VMEM,
        ],
        out_specs=pl.BlockSpec((COLS, 3 * UNITS), lambda i: (i, 0)),
        compiler_params=PARAMS,
        cost_estimate=pl.CostEstimate(
            flops=6 * D * UNITS * TOKS, bytes_accessed=20_000_000, transcendentals=0
        ),
        name="outer",
    )(inputs, grad, both, hidden)


def input_of(where, right, pieces):
    shape = jax.ShapeDtypeStruct((4 * COLS, TOKS), BF16)
    return pl.pallas_call(
        input_body,
        out_shape=(shape, shape),
        in_specs=[SMEM] + [VMEM] * 11,
        out_specs=(VMEM, VMEM),
        compiler_params=PARAMS,
        cost_estimate=pl.CostEstimate(
            flops=4 * D * UNITS * TOKS, bytes_accessed=15_000_000, transcendentals=0
        ),
        name="grad_input",
    )(where, right, *pieces)


def copy_for_each(value, axis):
    copies = jnp.broadcast_to(value, (lax.axis_size(axis), *value.shape))
    return lax.all_to_all(copies, axis, split_axis=0, concat_axis=0, tiled=True)


def over_features(where, own):
    mine = jnp.concatenate(gathered(own, "x"), axis=0)
    other = swapped(mine)
    return arranged(where, mine, other)


def layer(
    inputs,
    cotangent,
    pre_norm,
    gate_pre,
    value_pre,
    gate_weight,
    value_weight,
    down_weight,
    conv_taps,
    norm_gain,
):
    where = jnp.stack([lax.axis_index(a) for a in ("z", "y", "x", "c")]).astype(jnp.int32)
    down = jnp.pad(down_weight.T, ((0, 0), (0, WIDE - UNITS)))
    down_full = lax.all_gather(down, FS, axis=0, tiled=True)
    inputs_full = over_features(where, inputs.T)
    weights = jnp.concatenate([gate_weight, value_weight], axis=1)
    top = jnp.concatenate(gathered(weights[:HALF], "y"), axis=0)
    low = jnp.concatenate(gathered(weights[HALF:], "z"), axis=0)

    normed = pre_norm.astype(F32)
    cot_float = cotangent.astype(F32)
    scaled = norm_gain[None, :] * cot_float
    sums = jnp.concatenate([jnp.sum(normed * normed, axis=1), jnp.sum(normed * scaled, axis=1)])
    sums = jnp.sum(copy_for_each(sums, TP), axis=0)
    inverse = lax.rsqrt(sums[:TOKS] / D + EPSILON)
    cross = sums[TOKS:] / D
    grad_pre = (inverse[:, None] * (scaled - normed * (inverse * inverse * cross)[:, None])).astype(
        BF16
    )
    gain_local = jnp.sum(cot_float * normed * inverse[:, None], axis=0)

    grad_full = over_features(where, grad_pre.T)

    gate, value, taps = gate_pre.T, value_pre.T, conv_taps.T
    gate, top, low = lax.optimization_barrier((gate, top, low))
    pieces = (*gathered(top, "z"), *gathered(low, "y"))
    hidden = hidden_of(gate, value, taps)
    grads, taps_local = back_of(down_full, grad_full, gate, value, taps)
    terms = outer_of(inputs_full, grad_full, grads, hidden)
    summed = lax.psum_scatter(terms, FS, scatter_dimension=0, tiled=True).astype(F32)

    kept, sent = input_of(where, grads, pieces)
    paired = plus(kept, swapped(sent))
    grad_input = reduced(*in_five(paired), "x", F32).T.astype(BF16)

    small = jnp.concatenate([taps_local.T.ravel(), gain_local])
    small = jnp.sum(copy_for_each(small, FS), axis=0)
    grad_taps = small[: 3 * UNITS].reshape(3, UNITS)
    grad_gain = small[3 * UNITS :]
    return (
        grad_input,
        summed[:, :UNITS],
        summed[:, UNITS : 2 * UNITS],
        summed[:, 2 * UNITS :].T,
        grad_taps,
        grad_gain,
    )


def solution(mesh):
    split = Mesh(mesh.devices.reshape(4, 4, 4, 2), ("z", "y", "x", "c"))
    in_specs = (
        P(FS, TP),
        P(FS, TP),
        P(FS, TP),
        P(FS, TP),
        P(FS, TP),
        P(FS, TP),
        P(FS, TP),
        P(TP, FS),
        P(None, TP),
        P(TP),
    )
    out_specs = (P(FS, TP), P(FS, TP), P(FS, TP), P(TP, FS), P(None, TP), P(TP))
    return jax.shard_map(layer, mesh=split, in_specs=in_specs, out_specs=out_specs, check_vma=False)
```

profile of v0, /device:TPU:1, one launch (start us, length us, event | category | flops | bytes accessed | tf_op | source)
XLA Modules:
  0.0 247.1 jit_solution(4999258512338644371)
XLA Ops:
  7.2 1.8 pad.4
  9.1 1.2 copy.37
  10.3 2.1 collective-permute-start.27
  12.4 1.3 collective-permute-start.26
  14.9 3.9 %collective-permute-start.9 = (bf16[96,1408]{1,0:T(8,128)(2,1)}, bf16[96,1408]{1,0:T(8,128)(2,1)}, u32[]{:S(2)}, u32[]{:S(2)}) collective-permute-start(bf16[96,1408]{1,0:T(8,128)(2,1)} %get-tuple-element.47), channel_id=1, source_target_pairs={{0,96},{32,0},{64,32},{96,64},{1,97},{33,1},{65,33},{97,65},{2,98}... | collective-permute-start | bytes 811016 | tf_op jit(solution)/shard_map/ppermute | solution.py:30
  20.1 5.3 %all-to-all-start = ((f32[8,1,1024]{2,1,0:T(1,128)}), f32[8,1,1024]{2,1,0:T(1,128)}, u32[]{:S(2)}, u32[]{:S(2)}) async-start(f32[8,1,1024]{2,1,0:T(1,128)} %broadcast_in_dim.4), calls=%async_computation | async-start | bytes 65536 | tf_op jit(solution)/shard_map/all_to_all | solution.py:248
  25.4 2.7 %collective-permute-start.5 = (bf16[96,1408]{1,0:T(8,128)(2,1)}, bf16[96,1408]{1,0:T(8,128)(2,1)}, u32[]{:S(2)}, u32[]{:S(2)}) collective-permute-start(bf16[96,1408]{1,0:T(8,128)(2,1)} %get-tuple-element.61), channel_id=1, source_target_pairs={{0,24},{8,0},{16,8},{24,16},{1,25},{9,1},{17,9},{25,17},{2,26},{10... | collective-permute-start | bytes 811016 | tf_op jit(solution)/shard_map/ppermute | solution.py:30
  28.2 2.1 all-to-all-done
  31.1 1.4 collective-permute-start.6
  34.1 3.1 %collective-permute-done.5 = bf16[96,1408]{1,0:T(8,128)(2,1)} collective-permute-done((bf16[96,1408]{1,0:T(8,128)(2,1)}, bf16[96,1408]{1,0:T(8,128)(2,1)}, u32[]{:S(2)}, u32[]{:S(2)}) %collective-permute-start.5) | collective-permute-done | bytes 270368 | tf_op jit(solution)/shard_map/ppermute | solution.py:30
  37.2 2.7 %collective-permute-start = (bf16[384,512]{1,0:T(8,128)(2,1)}, bf16[384,512]{1,0:T(8,128)(2,1)}, u32[]{:S(2)}, u32[]{:S(2)}) collective-permute-start(bf16[384,512]{1,0:T(8,128)(2,1)} %get-tuple-element.51), channel_id=1, source_target_pairs={{0,6},{2,0},{4,2},{6,4},{1,7},{3,1},{5,3},{7,5},{8,14},{10,8},{12,... | collective-permute-start | bytes 1179656 | tf_op jit(solution)/shard_map/ppermute | solution.py:30
  43.6 3.0 %collective-permute-start.12 = (bf16[48,1408]{1,0:T(8,128)(2,1)S(1)}, bf16[48,1408]{1,0:T(8,128)(2,1)S(1)}, u32[]{:S(2)}, u32[]{:S(2)}) collective-permute-start(bf16[48,1408]{1,0:T(8,128)(2,1)S(1)} %slice.125), channel_id=1, source_target_pairs={{0,96},{32,0},{64,32},{96,64},{1,97},{33,1},{65,33},{97,65},{2,98}... | collective-permute-start | bytes 405512 | tf_op jit(solution)/shard_map/ppermute | solution.py:30
  47.6 1.7 constant_dynamic-update-slice_fusion.13
  49.5 3.5 %collective-permute-start.8 = (bf16[48,1408]{1,0:T(8,128)(2,1)S(1)}, bf16[48,1408]{1,0:T(8,128)(2,1)S(1)}, u32[]{:S(2)}, u32[]{:S(2)}) collective-permute-start(bf16[48,1408]{1,0:T(8,128)(2,1)S(1)} %slice.123), channel_id=1, source_target_pairs={{0,24},{8,0},{16,8},{24,16},{1,25},{9,1},{17,9},{25,17},{2,26},{10... | collective-permute-start | bytes 405512 | tf_op jit(solution)/shard_map/ppermute | solution.py:30
  53.0 2.7 %collective-permute-start.29 = (bf16[192,512]{1,0:T(8,128)(2,1)S(1)}, bf16[192,512]{1,0:T(8,128)(2,1)S(1)}, u32[]{:S(2)}, u32[]{:S(2)}) collective-permute-start(bf16[192,512]{1,0:T(8,128)(2,1)S(1)} %slice.138), channel_id=1, source_target_pairs={{0,6},{2,0},{4,2},{6,4},{1,7},{3,1},{5,3},{7,5},{8,14},{10,8},{12,... | collective-permute-start | bytes 589832 | tf_op jit(solution)/shard_map/ppermute | solution.py:30
  58.3 3.5 %collective-permute-start.3 = (bf16[192,512]{1,0:T(8,128)(2,1)S(1)}, bf16[192,512]{1,0:T(8,128)(2,1)S(1)}, u32[]{:S(2)}, u32[]{:S(2)}) collective-permute-start(bf16[192,512]{1,0:T(8,128)(2,1)S(1)} %slice.119), channel_id=1, source_target_pairs={{0,6},{2,0},{4,2},{6,4},{1,7},{3,1},{5,3},{7,5},{8,14},{10,8},{12,... | collective-permute-start | bytes 589832 | tf_op jit(solution)/shard_map/ppermute | solution.py:30
  61.9 2.0 collective-permute-done.2
  63.9 2.7 %collective-permute-start.30 = (bf16[1536,512]{1,0:T(8,128)(2,1)S(1)}, bf16[1536,512]{1,0:T(8,128)(2,1)S(1)}, u32[]{:S(2)}, u32[]{:S(2)}) collective-permute-start(bf16[1536,512]{1,0:T(8,128)(2,1)S(1)} %constant_dynamic-update-slice_fusion.15.mine_ref), channel_id=1, source_target_pairs={{0,1},{1,0},{2,3},{3,2},{4,5},{5,4},{6,7},{7,6},{8,9},{9,8},{10,11... | collective-permute-start | bytes 4718600 | tf_op jit(solution)/shard_map/ppermute | solution.py:34
  66.7 1.1 constant_dynamic-update-slice_fusion.mine_ref
  67.8 1.2 collective-permute-start.4
  71.6 5.0 %collective-permute-done.7 = bf16[48,1408]{1,0:T(8,128)(2,1)S(1)} collective-permute-done((bf16[48,1408]{1,0:T(8,128)(2,1)S(1)}, bf16[48,1408]{1,0:T(8,128)(2,1)S(1)}, u32[]{:S(2)}, u32[]{:S(2)}) %collective-permute-start.7) | collective-permute-done | bytes 135200 | tf_op jit(solution)/shard_map/ppermute | solution.py:30
  76.6 1.7 constant_dynamic-update-slice_fusion.10.rest_5_
  81.3 2.4 arrange.3.inputs_ref
  83.8 2.4 arrange.2.grad_ref
  86.2 9.3 %back.1 = (bf16[1408,512]{1,0:T(8,128)(2,1)S(1)}, f32[704,3]{1,0:T(8,128)S(1)}) custom-call(bf16[3072,768]{1,0:T(8,128)(2,1)} %all-gather.2.cloned.1.call-done.down_ref, bf16[3072,512]{1,0:T(8,128)(2,1)} %arrange.2.grad_ref, bf16[704,512]{1,0:T(8,128)(2,1)S(1)} %bitcast.22, bf16[704,512]{1,0:T(8,128)(2,1)S(1)} %bitcast.24, f32[704,3]{1,0:T(8,128)S(1)} %bitcast.20), custom_call_target="tpu_custom_call" | custom-call | flops 2214592512 | bytes 12000000 | tf_op jit(solution)/shard_map/back/pallas_call | solution.py:194
  95.5 13.3 %outer.1 = bf16[3072,2112]{1,0:T(8,128)(2,1)} custom-call(bf16[3072,512]{1,0:T(8,128)(2,1)} %arrange.3.inputs_ref, bf16[3072,512]{1,0:T(8,128)(2,1)} %arrange.2.grad_ref, bf16[1408,512]{1,0:T(8,128)(2,1)S(1)} %get-tuple-element.14.right_ref.both_ref, bf16[704,512]{1,0:T(8,128)(2,1)S(1)} %copy-done.4), custom_call_target="tpu_custom_call" | custom-call | flops 6643777536 | bytes 20000000 | tf_op jit(solution)/shard_map/outer/pallas_call | solution.py:212
  109.9 1.2 copy-done.7
  111.2 2.9 %collective-permute-start.13 = (bf16[384,1408]{1,0:T(8,128)(2,1)S(1)}, bf16[384,1408]{1,0:T(8,128)(2,1)S(1)}, u32[]{:S(2)}, u32[]{:S(2)}) collective-permute-start(bf16[384,1408]{1,0:T(8,128)(2,1)S(1)} %copy-done.7), channel_id=1, source_target_pairs={{0,96},{32,0},{64,32},{96,64},{1,97},{33,1},{65,33},{97,65},{2,98}... | collective-permute-start | bytes 3244040 | tf_op jit(solution)/shard_map/ppermute | solution.py:30
  114.1 2.7 %collective-permute-start.17 = (bf16[384,1408]{1,0:T(8,128)(2,1)}, bf16[384,1408]{1,0:T(8,128)(2,1)S(1)}, u32[]{:S(2)}, u32[]{:S(2)}) collective-permute-start(bf16[384,1408]{1,0:T(8,128)(2,1)} %constant_dynamic-update-slice_fusion.10.rest_5_), channel_id=1, source_target_pairs={{0,24},{8,0},{16,8},{24,16},{1,25},{9,1},{17,9},{25,17},{2,26},{10... | collective-permute-start | bytes 3244040 | tf_op jit(solution)/shard_map/ppermute | solution.py:30
  116.8 35.4 %collective-permute-done.14.rest_4_ = bf16[384,1408]{1,0:T(8,128)(2,1)S(1)} collective-permute-done((bf16[384,1408]{1,0:T(8,128)(2,1)S(1)}, bf16[384,1408]{1,0:T(8,128)(2,1)S(1)}, u32[]{:S(2)}, u32[]{:S(2)}) %collective-permute-start.14) | collective-permute-done | bytes 1081376 | tf_op jit(solution)/shard_map/ppermute | solution.py:30
  152.3 1.3 collective-permute-done.13.rest_1_
  153.7 3.6 %collective-permute-start.16 = (bf16[192,1408]{1,0:T(8,128)(2,1)S(1)}, bf16[192,1408]{1,0:T(8,128)(2,1)S(1)}, u32[]{:S(2)}, u32[]{:S(2)}) collective-permute-start(bf16[192,1408]{1,0:T(8,128)(2,1)S(1)} %slice.127), channel_id=1, source_target_pairs={{0,96},{32,0},{64,32},{96,64},{1,97},{33,1},{65,33},{97,65},{2,98}... | collective-permute-start | bytes 1622024 | tf_op jit(solution)/shard_map/ppermute | solution.py:30
  157.4 1.5 collective-permute-done.17.rest_6_
  159.0 3.5 %collective-permute-start.20 = (bf16[192,1408]{1,0:T(8,128)(2,1)S(1)}, bf16[192,1408]{1,0:T(8,128)(2,1)S(1)}, u32[]{:S(2)}, u32[]{:S(2)}) collective-permute-start(bf16[192,1408]{1,0:T(8,128)(2,1)S(1)} %slice.129), channel_id=1, source_target_pairs={{0,24},{8,0},{16,8},{24,16},{1,25},{9,1},{17,9},{25,17},{2,26},{10... | collective-permute-start | bytes 1622024 | tf_op jit(solution)/shard_map/ppermute | solution.py:30
  162.5 15.0 %collective-permute-done.15.rest_2_ = bf16[192,1408]{1,0:T(8,128)(2,1)S(1)} collective-permute-done((bf16[192,1408]{1,0:T(8,128)(2,1)S(1)}, bf16[192,1408]{1,0:T(8,128)(2,1)S(1)}, u32[]{:S(2)}, u32[]{:S(2)}) %collective-permute-start.15) | collective-permute-done | bytes 540704 | tf_op jit(solution)/shard_map/ppermute | solution.py:30
  177.5 2.0 collective-permute-done.16.rest_3_
  179.5 3.5 %collective-permute-done.19.rest_7_ = bf16[192,1408]{1,0:T(8,128)(2,1)S(1)} collective-permute-done((bf16[192,1408]{1,0:T(8,128)(2,1)S(1)}, bf16[192,1408]{1,0:T(8,128)(2,1)S(1)}, u32[]{:S(2)}, u32[]{:S(2)}) %collective-permute-start.19) | collective-permute-done | bytes 540704 | tf_op jit(solution)/shard_map/ppermute | solution.py:30
  182.9 1.6 collective-permute-done.20.rest_8_
  184.5 12.8 %grad_input.1 = (bf16[1536,512]{1,0:T(8,128)(2,1)}, bf16[1536,512]{1,0:T(8,128)(2,1)}) custom-call(s32[4]{0:T(128)S(1)} %pad_add_fusion.where_ref, bf16[1408,512]{1,0:T(8,128)(2,1)} %copy-done.8, bf16[384,1408]{1,0:T(8,128)(2,1)S(1)} %copy-done.7, bf16[384,1408]{1,0:T(8,128)(2,1)} %copy-done.20, bf16[192,1408]{1,0:T(8,128)(2,1)S(1)} %collective-permute-done.15.rest_2_, ...), custom_call_target="tpu_custom_call" | custom-call | flops 4429185024 | bytes 15000000 | tf_op jit(solution)/shard_map/grad_input/pallas_call | solution.py:233
  197.3 6.5 %collective-permute-start.21 = (bf16[1536,512]{1,0:T(8,128)(2,1)}, bf16[1536,512]{1,0:T(8,128)(2,1)S(1)}, u32[]{:S(2)}, u32[]{:S(2)}) collective-permute-start(bf16[1536,512]{1,0:T(8,128)(2,1)} %get-tuple-element.18), channel_id=1, source_target_pairs={{0,1},{1,0},{2,3},{3,2},{4,5},{5,4},{6,7},{7,6},{8,9},{9,8},{10,11... | collective-permute-start | bytes 4718600 | tf_op jit(solution)/shard_map/ppermute | solution.py:34
  203.9 3.2 %collective-permute-done.21 = bf16[1536,512]{1,0:T(8,128)(2,1)S(1)} collective-permute-done((bf16[1536,512]{1,0:T(8,128)(2,1)}, bf16[1536,512]{1,0:T(8,128)(2,1)S(1)}, u32[]{:S(2)}, u32[]{:S(2)}) %collective-permute-start.21) | collective-permute-done | bytes 1572896 | tf_op jit(solution)/shard_map/ppermute | solution.py:34
  207.1 1.9 add_convert_fusion
  209.1 4.4 %collective-permute-start.24 = (bf16[192,512]{1,0:T(8,128)(2,1)S(1)}, bf16[192,512]{1,0:T(8,128)(2,1)S(1)}, u32[]{:S(2)}, u32[]{:S(2)}) collective-permute-start(bf16[192,512]{1,0:T(8,128)(2,1)S(1)} %get-tuple-element.55), channel_id=1, source_target_pairs={{0,6},{2,0},{4,2},{6,4},{1,7},{3,1},{5,3},{7,5},{8,14},{10,8},{12,... | collective-permute-start | bytes 589832 | tf_op jit(solution)/shard_map/ppermute | solution.py:30
  213.5 4.8 %collective-permute-done.22 = bf16[192,512]{1,0:T(8,128)(2,1)S(1)} collective-permute-done((bf16[192,512]{1,0:T(8,128)(2,1)S(1)}, bf16[192,512]{1,0:T(8,128)(2,1)S(1)}, u32[]{:S(2)}, u32[]{:S(2)}) %collective-permute-start.22) | collective-permute-done | bytes 196640 | tf_op jit(solution)/shard_map/ppermute | solution.py:30
  218.5 2.5 %collective-permute-start.25 = (bf16[384,512]{1,0:T(8,128)(2,1)S(1)}, bf16[384,512]{1,0:T(8,128)(2,1)S(1)}, u32[]{:S(2)}, u32[]{:S(2)}) collective-permute-start(bf16[384,512]{1,0:T(8,128)(2,1)S(1)} %pad_maximum_fusion.1), channel_id=1, source_target_pairs={{0,6},{2,0},{4,2},{6,4},{1,7},{3,1},{5,3},{7,5},{8,14},{10,8},{12,... | collective-permute-start | bytes 1179656 | tf_op jit(solution)/shard_map/ppermute | solution.py:30
  221.8 13.3 %all_to_all.12 = f32[16,1,2496]{2,1,0:T(1,128)S(1)} all-to-all(f32[16,1,2496]{2,1,0:T(1,128)S(1)} %broadcast_in_dim.5), channel_id=1, replica_groups=mesh['z'=4,'y'=4,'x'=4,'c'=2] {'z','y'}, dimensions={0} | all-to-all | bytes 319488 | tf_op jit(solution)/shard_map/all_to_all | solution.py:248
  237.5 1.3 convert_element_type.73
  238.9 1.3 fusion.13
  (136 shorter events, 23.0 us)
Async XLA Ops:
  7.2 79.0 %all-gather.2.cloned.1.call-start = ((), (), s32[]{:S(2)}) async-start(), calls=%async_computation.3 | async-start | bytes 5013504 | tf_op jit(solution)/shard_map/all_gather | solution.py:271
  7.2 11.5 %copy-start.15 = (bf16[512,384]{1,0:T(8,128)(2,1)S(1)}, bf16[512,384]{1,0:T(8,128)(2,1)}, u32[]{:S(2)}) copy-start(bf16[512,384]{1,0:T(8,128)(2,1)} %param.11) | copy-start | bytes 1179652
  9.0 9.9 %copy-start.16 = (bf16[512,384]{1,0:T(8,128)(2,1)S(1)}, bf16[512,384]{1,0:T(8,128)(2,1)}, u32[]{:S(2)}) copy-start(bf16[512,384]{1,0:T(8,128)(2,1)} %param.12) | copy-start | bytes 1179652
  10.3 39.0 %collective-permute-start.27 = (bf16[384,512]{1,0:T(8,128)(2,1)S(1)}, bf16[384,512]{1,0:T(8,128)(2,1)S(1)}, u32[]{:S(2)}, u32[]{:S(2)}) collective-permute-start(bf16[384,512]{1,0:T(8,128)(2,1)S(1)} %bitcast.26), channel_id=1, source_target_pairs={{0,2},{2,4},{4,6},{6,0},{1,3},{3,5},{5,7},{7,1},{8,10},{10,12},{12... | collective-permute-start | bytes 1179656 | tf_op jit(solution)/shard_map/ppermute | solution.py:30
  12.4 36.9 %collective-permute-start.26 = (bf16[384,512]{1,0:T(8,128)(2,1)S(1)}, bf16[384,512]{1,0:T(8,128)(2,1)S(1)}, u32[]{:S(2)}, u32[]{:S(2)}) collective-permute-start(bf16[384,512]{1,0:T(8,128)(2,1)S(1)} %bitcast.27), channel_id=1, source_target_pairs={{0,6},{2,0},{4,2},{6,4},{1,7},{3,1},{5,3},{7,5},{8,14},{10,8},{12,... | collective-permute-start | bytes 1179656 | tf_op jit(solution)/shard_map/ppermute | solution.py:30
  14.9 16.2 %collective-permute-start.9 = (bf16[96,1408]{1,0:T(8,128)(2,1)}, bf16[96,1408]{1,0:T(8,128)(2,1)}, u32[]{:S(2)}, u32[]{:S(2)}) collective-permute-start(bf16[96,1408]{1,0:T(8,128)(2,1)} %get-tuple-element.47), channel_id=1, source_target_pairs={{0,96},{32,0},{64,32},{96,64},{1,97},{33,1},{65,33},{97,65},{2,98}... | collective-permute-start | bytes 811016 | tf_op jit(solution)/shard_map/ppermute | solution.py:30
  18.7 14.8 %collective-permute-start.10 = (bf16[96,1408]{1,0:T(8,128)(2,1)}, bf16[96,1408]{1,0:T(8,128)(2,1)}, u32[]{:S(2)}, u32[]{:S(2)}) collective-permute-start(bf16[96,1408]{1,0:T(8,128)(2,1)} %get-tuple-element.47), channel_id=1, source_target_pairs={{0,32},{32,64},{64,96},{96,0},{1,33},{33,65},{65,97},{97,1},{2,34}... | collective-permute-start | bytes 811016 | tf_op jit(solution)/shard_map/ppermute | solution.py:30
  19.0 14.5 %copy-start.9 = (bf16[512,384]{0,1:T(8,128)(2,1)}, bf16[512,384]{0,1:T(8,128)(2,1)S(1)}, u32[]{:S(2)}) copy-start(bf16[512,384]{0,1:T(8,128)(2,1)S(1)} %copy.34) | copy-start | bytes 1179652
  19.2 14.3 %copy-start.11 = (bf16[512,384]{0,1:T(8,128)(2,1)}, bf16[512,384]{0,1:T(8,128)(2,1)S(1)}, u32[]{:S(2)}) copy-start(bf16[512,384]{0,1:T(8,128)(2,1)S(1)} %copy.33) | copy-start | bytes 1179652
  20.1 10.2 %all-to-all-start = ((f32[8,1,1024]{2,1,0:T(1,128)}), f32[8,1,1024]{2,1,0:T(1,128)}, u32[]{:S(2)}, u32[]{:S(2)}) async-start(f32[8,1,1024]{2,1,0:T(1,128)} %broadcast_in_dim.4), calls=%async_computation | async-start | bytes 65536 | tf_op jit(solution)/shard_map/all_to_all | solution.py:248
  25.4 212.1 %reduce-scatter.2.cloned.1.call-start = ((), (), s32[]{:S(2)}) async-start(), calls=%async_computation.4 | async-start | bytes 14204928 | tf_op jit(solution)/shard_map/reduce_scatter | solution.py:297
  25.4 11.8 %collective-permute-start.5 = (bf16[96,1408]{1,0:T(8,128)(2,1)}, bf16[96,1408]{1,0:T(8,128)(2,1)}, u32[]{:S(2)}, u32[]{:S(2)}) collective-permute-start(bf16[96,1408]{1,0:T(8,128)(2,1)} %get-tuple-element.61), channel_id=1, source_target_pairs={{0,24},{8,0},{16,8},{24,16},{1,25},{9,1},{17,9},{25,17},{2,26},{10... | collective-permute-start | bytes 811016 | tf_op jit(solution)/shard_map/ppermute | solution.py:30
  31.1 12.6 %collective-permute-start.6 = (bf16[96,1408]{1,0:T(8,128)(2,1)}, bf16[96,1408]{1,0:T(8,128)(2,1)}, u32[]{:S(2)}, u32[]{:S(2)}) collective-permute-start(bf16[96,1408]{1,0:T(8,128)(2,1)} %get-tuple-element.61), channel_id=1, source_target_pairs={{0,8},{8,16},{16,24},{24,0},{1,9},{9,17},{17,25},{25,1},{2,10},{10... | collective-permute-start | bytes 811016 | tf_op jit(solution)/shard_map/ppermute | solution.py:30
  33.5 15.9 %collective-permute-start.1 = (bf16[384,512]{1,0:T(8,128)(2,1)}, bf16[384,512]{1,0:T(8,128)(2,1)S(1)}, u32[]{:S(2)}, u32[]{:S(2)}) collective-permute-start(bf16[384,512]{1,0:T(8,128)(2,1)} %get-tuple-element.51), channel_id=1, source_target_pairs={{0,2},{2,4},{4,6},{6,0},{1,3},{3,5},{5,7},{7,1},{8,10},{10,12},{12... | collective-permute-start | bytes 1179656 | tf_op jit(solution)/shard_map/ppermute | solution.py:30
  37.2 15.8 %collective-permute-start = (bf16[384,512]{1,0:T(8,128)(2,1)}, bf16[384,512]{1,0:T(8,128)(2,1)}, u32[]{:S(2)}, u32[]{:S(2)}) collective-permute-start(bf16[384,512]{1,0:T(8,128)(2,1)} %get-tuple-element.51), channel_id=1, source_target_pairs={{0,6},{2,0},{4,2},{6,4},{1,7},{3,1},{5,3},{7,5},{8,14},{10,8},{12,... | collective-permute-start | bytes 1179656 | tf_op jit(solution)/shard_map/ppermute | solution.py:30
  43.6 13.0 %copy-start.2 = (bf16[1536,512]{1,0:T(8,128)(2,1)S(1)}, bf16[1536,512]{1,0:T(8,128)(2,1)}, u32[]{:S(2)}) copy-start(bf16[1536,512]{1,0:T(8,128)(2,1)} %get-tuple-element.50) | copy-start | bytes 4718596
  43.6 27.3 %collective-permute-start.12 = (bf16[48,1408]{1,0:T(8,128)(2,1)S(1)}, bf16[48,1408]{1,0:T(8,128)(2,1)S(1)}, u32[]{:S(2)}, u32[]{:S(2)}) collective-permute-start(bf16[48,1408]{1,0:T(8,128)(2,1)S(1)} %slice.125), channel_id=1, source_target_pairs={{0,96},{32,0},{64,32},{96,64},{1,97},{33,1},{65,33},{97,65},{2,98}... | collective-permute-start | bytes 405512 | tf_op jit(solution)/shard_map/ppermute | solution.py:30
  49.3 20.7 %collective-permute-start.11 = (bf16[48,1408]{1,0:T(8,128)(2,1)S(1)}, bf16[48,1408]{1,0:T(8,128)(2,1)S(1)}, u32[]{:S(2)}, u32[]{:S(2)}) collective-permute-start(bf16[48,1408]{1,0:T(8,128)(2,1)S(1)} %slice.124), channel_id=1, source_target_pairs={{0,32},{32,64},{64,96},{96,0},{1,33},{33,65},{65,97},{97,1},{2,34}... | collective-permute-start | bytes 405512 | tf_op jit(solution)/shard_map/ppermute | solution.py:30
  49.3 8.4 %collective-permute-start.28 = (bf16[192,512]{1,0:T(8,128)(2,1)S(1)}, bf16[192,512]{1,0:T(8,128)(2,1)S(1)}, u32[]{:S(2)}, u32[]{:S(2)}) collective-permute-start(bf16[192,512]{1,0:T(8,128)(2,1)S(1)} %slice.137), channel_id=1, source_target_pairs={{0,2},{2,4},{4,6},{6,0},{1,3},{3,5},{5,7},{7,1},{8,10},{10,12},{12... | collective-permute-start | bytes 589832 | tf_op jit(solution)/shard_map/ppermute | solution.py:30
  49.4 17.2 %copy-start.14 = (bf16[384,512]{1,0:T(8,128)(2,1)}, bf16[384,512]{1,0:T(8,128)(2,1)S(1)}, u32[]{:S(2)}) copy-start(bf16[384,512]{1,0:T(8,128)(2,1)S(1)} %collective-permute-done.1) | copy-start | bytes 1179652
  49.5 27.1 %collective-permute-start.8 = (bf16[48,1408]{1,0:T(8,128)(2,1)S(1)}, bf16[48,1408]{1,0:T(8,128)(2,1)S(1)}, u32[]{:S(2)}, u32[]{:S(2)}) collective-permute-start(bf16[48,1408]{1,0:T(8,128)(2,1)S(1)} %slice.123), channel_id=1, source_target_pairs={{0,24},{8,0},{16,8},{24,16},{1,25},{9,1},{17,9},{25,17},{2,26},{10... | collective-permute-start | bytes 405512 | tf_op jit(solution)/shard_map/ppermute | solution.py:30
  53.0 5.3 %collective-permute-start.29 = (bf16[192,512]{1,0:T(8,128)(2,1)S(1)}, bf16[192,512]{1,0:T(8,128)(2,1)S(1)}, u32[]{:S(2)}, u32[]{:S(2)}) collective-permute-start(bf16[192,512]{1,0:T(8,128)(2,1)S(1)} %slice.138), channel_id=1, source_target_pairs={{0,6},{2,0},{4,2},{6,4},{1,7},{3,1},{5,3},{7,5},{8,14},{10,8},{12,... | collective-permute-start | bytes 589832 | tf_op jit(solution)/shard_map/ppermute | solution.py:30
  57.7 11.3 %copy-start.5 = (bf16[384,1408]{1,0:T(8,128)(2,1)S(1)}, bf16[384,1408]{1,0:T(8,128)(2,1)}, u32[]{:S(2)}) copy-start(bf16[384,1408]{1,0:T(8,128)(2,1)} %get-tuple-element.60) | copy-start | bytes 3244036
  57.7 6.2 %collective-permute-start.2 = (bf16[192,512]{1,0:T(8,128)(2,1)S(1)}, bf16[192,512]{1,0:T(8,128)(2,1)S(1)}, u32[]{:S(2)}, u32[]{:S(2)}) collective-permute-start(bf16[192,512]{1,0:T(8,128)(2,1)S(1)} %slice.118), channel_id=1, source_target_pairs={{0,2},{2,4},{4,6},{6,0},{1,3},{3,5},{5,7},{7,1},{8,10},{10,12},{12... | collective-permute-start | bytes 589832 | tf_op jit(solution)/shard_map/ppermute | solution.py:30
  58.3 8.3 %collective-permute-start.3 = (bf16[192,512]{1,0:T(8,128)(2,1)S(1)}, bf16[192,512]{1,0:T(8,128)(2,1)S(1)}, u32[]{:S(2)}, u32[]{:S(2)}) collective-permute-start(bf16[192,512]{1,0:T(8,128)(2,1)S(1)} %slice.119), channel_id=1, source_target_pairs={{0,6},{2,0},{4,2},{6,4},{1,7},{3,1},{5,3},{7,5},{8,14},{10,8},{12,... | collective-permute-start | bytes 589832 | tf_op jit(solution)/shard_map/ppermute | solution.py:30
  63.9 17.4 %collective-permute-start.30 = (bf16[1536,512]{1,0:T(8,128)(2,1)S(1)}, bf16[1536,512]{1,0:T(8,128)(2,1)S(1)}, u32[]{:S(2)}, u32[]{:S(2)}) collective-permute-start(bf16[1536,512]{1,0:T(8,128)(2,1)S(1)} %constant_dynamic-update-slice_fusion.15.mine_ref), channel_id=1, source_target_pairs={{0,1},{1,0},{2,3},{3,2},{4,5},{5,4},{6,7},{7,6},{8,9},{9,8},{10,11... | collective-permute-start | bytes 4718600 | tf_op jit(solution)/shard_map/ppermute | solution.py:34
  66.7 13.6 %copy-start = (bf16[512,704]{0,1:T(8,128)(2,1)S(1)}, bf16[512,704]{0,1:T(8,128)(2,1)}, u32[]{:S(2)}) copy-start(bf16[512,704]{0,1:T(8,128)(2,1)} %param.13) | copy-start | bytes 2162692
  66.7 13.6 %copy-start.1 = (bf16[512,704]{0,1:T(8,128)(2,1)S(1)}, bf16[512,704]{0,1:T(8,128)(2,1)}, u32[]{:S(2)}) copy-start(bf16[512,704]{0,1:T(8,128)(2,1)} %param.14) | copy-start | bytes 2162692
  67.8 15.9 %collective-permute-start.4 = (bf16[1536,512]{1,0:T(8,128)(2,1)S(1)}, bf16[1536,512]{1,0:T(8,128)(2,1)S(1)}, u32[]{:S(2)}, u32[]{:S(2)}) collective-permute-start(bf16[1536,512]{1,0:T(8,128)(2,1)S(1)} %constant_dynamic-update-slice_fusion.mine_ref), channel_id=1, source_target_pairs={{0,1},{1,0},{2,3},{3,2},{4,5},{5,4},{6,7},{7,6},{8,9},{9,8},{10,11... | collective-permute-start | bytes 4718600 | tf_op jit(solution)/shard_map/ppermute | solution.py:34
  70.0 6.6 %collective-permute-start.7 = (bf16[48,1408]{1,0:T(8,128)(2,1)S(1)}, bf16[48,1408]{1,0:T(8,128)(2,1)S(1)}, u32[]{:S(2)}, u32[]{:S(2)}) collective-permute-start(bf16[48,1408]{1,0:T(8,128)(2,1)S(1)} %slice.122), channel_id=1, source_target_pairs={{0,8},{8,16},{16,24},{24,0},{1,9},{9,17},{17,25},{25,1},{2,10},{10... | collective-permute-start | bytes 405512 | tf_op jit(solution)/shard_map/ppermute | solution.py:30
  86.2 9.4 %copy-start.4 = (bf16[704,512]{1,0:T(8,128)(2,1)S(1)}, bf16[704,512]{1,0:T(8,128)(2,1)}, u32[]{:S(2)}) copy-start(bf16[704,512]{1,0:T(8,128)(2,1)} %copy-done.3) | copy-start | bytes 2162692
  111.1 41.1 %collective-permute-start.14 = (bf16[384,1408]{1,0:T(8,128)(2,1)S(1)}, bf16[384,1408]{1,0:T(8,128)(2,1)S(1)}, u32[]{:S(2)}, u32[]{:S(2)}) collective-permute-start(bf16[384,1408]{1,0:T(8,128)(2,1)S(1)} %copy-done.7), channel_id=1, source_target_pairs={{0,32},{32,64},{64,96},{96,0},{1,33},{33,65},{65,97},{97,1},{2,34}... | collective-permute-start | bytes 3244040 | tf_op jit(solution)/shard_map/ppermute | solution.py:30
  111.2 42.5 %collective-permute-start.13 = (bf16[384,1408]{1,0:T(8,128)(2,1)S(1)}, bf16[384,1408]{1,0:T(8,128)(2,1)S(1)}, u32[]{:S(2)}, u32[]{:S(2)}) collective-permute-start(bf16[384,1408]{1,0:T(8,128)(2,1)S(1)} %copy-done.7), channel_id=1, source_target_pairs={{0,96},{32,0},{64,32},{96,64},{1,97},{33,1},{65,33},{97,65},{2,98}... | collective-permute-start | bytes 3244040 | tf_op jit(solution)/shard_map/ppermute | solution.py:30
  114.1 43.2 %collective-permute-start.18 = (bf16[384,1408]{1,0:T(8,128)(2,1)}, bf16[384,1408]{1,0:T(8,128)(2,1)S(1)}, u32[]{:S(2)}, u32[]{:S(2)}) collective-permute-start(bf16[384,1408]{1,0:T(8,128)(2,1)} %constant_dynamic-update-slice_fusion.10.rest_5_), channel_id=1, source_target_pairs={{0,8},{8,16},{16,24},{24,0},{1,9},{9,17},{17,25},{25,1},{2,10},{10... | collective-permute-start | bytes 3244040 | tf_op jit(solution)/shard_map/ppermute | solution.py:30
  114.1 44.8 %collective-permute-start.17 = (bf16[384,1408]{1,0:T(8,128)(2,1)}, bf16[384,1408]{1,0:T(8,128)(2,1)S(1)}, u32[]{:S(2)}, u32[]{:S(2)}) collective-permute-start(bf16[384,1408]{1,0:T(8,128)(2,1)} %constant_dynamic-update-slice_fusion.10.rest_5_), channel_id=1, source_target_pairs={{0,24},{8,0},{16,8},{24,16},{1,25},{9,1},{17,9},{25,17},{2,26},{10... | collective-permute-start | bytes 3244040 | tf_op jit(solution)/shard_map/ppermute | solution.py:30
  152.3 25.2 %collective-permute-start.15 = (bf16[192,1408]{1,0:T(8,128)(2,1)S(1)}, bf16[192,1408]{1,0:T(8,128)(2,1)S(1)}, u32[]{:S(2)}, u32[]{:S(2)}) collective-permute-start(bf16[192,1408]{1,0:T(8,128)(2,1)S(1)} %slice.126), channel_id=1, source_target_pairs={{0,32},{32,64},{64,96},{96,0},{1,33},{33,65},{65,97},{97,1},{2,34}... | collective-permute-start | bytes 1622024 | tf_op jit(solution)/shard_map/ppermute | solution.py:30
  153.7 25.8 %collective-permute-start.16 = (bf16[192,1408]{1,0:T(8,128)(2,1)S(1)}, bf16[192,1408]{1,0:T(8,128)(2,1)S(1)}, u32[]{:S(2)}, u32[]{:S(2)}) collective-permute-start(bf16[192,1408]{1,0:T(8,128)(2,1)S(1)} %slice.127), channel_id=1, source_target_pairs={{0,96},{32,0},{64,32},{96,64},{1,97},{33,1},{65,33},{97,65},{2,98}... | collective-permute-start | bytes 1622024 | tf_op jit(solution)/shard_map/ppermute | solution.py:30
  157.3 27.3 %copy-start.21 = (bf16[384,1408]{1,0:T(8,128)(2,1)}, bf16[384,1408]{1,0:T(8,128)(2,1)S(1)}, u32[]{:S(2)}) copy-start(bf16[384,1408]{1,0:T(8,128)(2,1)S(1)} %collective-permute-done.18.rest_9_) | copy-start | bytes 3244036
  157.3 25.6 %collective-permute-start.19 = (bf16[192,1408]{1,0:T(8,128)(2,1)S(1)}, bf16[192,1408]{1,0:T(8,128)(2,1)S(1)}, u32[]{:S(2)}, u32[]{:S(2)}) collective-permute-start(bf16[192,1408]{1,0:T(8,128)(2,1)S(1)} %slice.128), channel_id=1, source_target_pairs={{0,8},{8,16},{16,24},{24,0},{1,9},{9,17},{17,25},{25,1},{2,10},{10... | collective-permute-start | bytes 1622024 | tf_op jit(solution)/shard_map/ppermute | solution.py:30
  158.9 25.6 %copy-start.22 = (bf16[384,1408]{1,0:T(8,128)(2,1)}, bf16[384,1408]{1,0:T(8,128)(2,1)S(1)}, u32[]{:S(2)}) copy-start(bf16[384,1408]{1,0:T(8,128)(2,1)S(1)} %collective-permute-done.17.rest_6_) | copy-start | bytes 3244036
  159.0 25.5 %collective-permute-start.20 = (bf16[192,1408]{1,0:T(8,128)(2,1)S(1)}, bf16[192,1408]{1,0:T(8,128)(2,1)S(1)}, u32[]{:S(2)}, u32[]{:S(2)}) collective-permute-start(bf16[192,1408]{1,0:T(8,128)(2,1)S(1)} %slice.129), channel_id=1, source_target_pairs={{0,24},{8,0},{16,8},{24,16},{1,25},{9,1},{17,9},{25,17},{2,26},{10... | collective-permute-start | bytes 1622024 | tf_op jit(solution)/shard_map/ppermute | solution.py:30
  197.3 9.8 %collective-permute-start.21 = (bf16[1536,512]{1,0:T(8,128)(2,1)}, bf16[1536,512]{1,0:T(8,128)(2,1)S(1)}, u32[]{:S(2)}, u32[]{:S(2)}) collective-permute-start(bf16[1536,512]{1,0:T(8,128)(2,1)} %get-tuple-element.18), channel_id=1, source_target_pairs={{0,1},{1,0},{2,3},{3,2},{4,5},{5,4},{6,7},{7,6},{8,9},{9,8},{10,11... | collective-permute-start | bytes 4718600 | tf_op jit(solution)/shard_map/ppermute | solution.py:34
  209.0 12.1 %copy-start.10 = (bf16[512,384]{0,1:T(8,128)(2,1)S(1)}, bf16[512,384]{0,1:T(8,128)(2,1)}, u32[]{:S(2)}) copy-start(bf16[512,384]{0,1:T(8,128)(2,1)} %copy-done.9) | copy-start | bytes 1179652
  209.0 12.1 %copy-start.12 = (bf16[512,384]{0,1:T(8,128)(2,1)S(1)}, bf16[512,384]{0,1:T(8,128)(2,1)}, u32[]{:S(2)}) copy-start(bf16[512,384]{0,1:T(8,128)(2,1)} %copy-done.11) | copy-start | bytes 1179652
  209.1 9.3 %collective-permute-start.22 = (bf16[192,512]{1,0:T(8,128)(2,1)S(1)}, bf16[192,512]{1,0:T(8,128)(2,1)S(1)}, u32[]{:S(2)}, u32[]{:S(2)}) collective-permute-start(bf16[192,512]{1,0:T(8,128)(2,1)S(1)} %get-tuple-element.54), channel_id=1, source_target_pairs={{0,2},{2,4},{4,6},{6,0},{1,3},{3,5},{5,7},{7,1},{8,10},{10,12},{12... | collective-permute-start | bytes 589832 | tf_op jit(solution)/shard_map/ppermute | solution.py:30
  209.1 9.2 %collective-permute-start.24 = (bf16[192,512]{1,0:T(8,128)(2,1)S(1)}, bf16[192,512]{1,0:T(8,128)(2,1)S(1)}, u32[]{:S(2)}, u32[]{:S(2)}) collective-permute-start(bf16[192,512]{1,0:T(8,128)(2,1)S(1)} %get-tuple-element.55), channel_id=1, source_target_pairs={{0,6},{2,0},{4,2},{6,4},{1,7},{3,1},{5,3},{7,5},{8,14},{10,8},{12,... | collective-permute-start | bytes 589832 | tf_op jit(solution)/shard_map/ppermute | solution.py:30
  218.5 18.0 %collective-permute-start.25 = (bf16[384,512]{1,0:T(8,128)(2,1)S(1)}, bf16[384,512]{1,0:T(8,128)(2,1)S(1)}, u32[]{:S(2)}, u32[]{:S(2)}) collective-permute-start(bf16[384,512]{1,0:T(8,128)(2,1)S(1)} %pad_maximum_fusion.1), channel_id=1, source_target_pairs={{0,6},{2,0},{4,2},{6,4},{1,7},{3,1},{5,3},{7,5},{8,14},{10,8},{12,... | collective-permute-start | bytes 1179656 | tf_op jit(solution)/shard_map/ppermute | solution.py:30
  221.0 15.4 %collective-permute-start.23 = (bf16[384,512]{1,0:T(8,128)(2,1)S(1)}, bf16[384,512]{1,0:T(8,128)(2,1)S(1)}, u32[]{:S(2)}, u32[]{:S(2)}) collective-permute-start(bf16[384,512]{1,0:T(8,128)(2,1)S(1)} %pad_maximum_fusion), channel_id=1, source_target_pairs={{0,2},{2,4},{4,6},{6,0},{1,3},{3,5},{5,7},{7,1},{8,10},{10,12},{12... | collective-permute-start | bytes 1179656 | tf_op jit(solution)/shard_map/ppermute | solution.py:30
  (10 other events, 39.7 us)
Sparse Core Ops, SparseCore 0:
  10.1 61.4 all-gather.1
  110.1 127.2 reduce-scatter.1
where the time goes:
time: 250 us; the launch traced here: 247 us
  waiting for transfers between devices  81.1 us (32%)
  starting transfers between devices  63.5 us (25%)
  Pallas kernels  41.3 us (17%)
  local copies, waits for them, and re-layouts  26.1 us (10%)
  between operations  14.6 us (6%)
  blocking collectives  13.3 us (5%)
  other arithmetic  7.19 us (3%)
    ppermute x28, waiting for transfers between devices, moved(): return lax.ppermute(value, axis, [(i, (i + by) % 4) for i in range(4)])  75.8 us
    ppermute x28, starting transfers between devices, moved(): return lax.ppermute(value, axis, [(i, (i + by) % 4) for i in range(4)])  47.7 us
    pallas_call x1, Pallas kernels, outer_of(): pl.pallas_call(outer_body, out_shape=jax.ShapeDtypeStruct((D, 3 * UNITS),...  13.3 us
    all_to_all x1, blocking collectives, copy_for_each(): return lax.all_to_all(copies, axis, split_axis=0, concat_axis=0, tiled=True)  13.3 us
    pallas_call x1, Pallas kernels, input_of(): pl.pallas_call(input_body, out_shape=(shape, shape), in_specs=[SMEM] + [V...  12.8 us
    unnamed x66, local copies, waits for them, and re-layouts  12 us
    ppermute x3, starting transfers between devices, swapped(): return lax.ppermute(value, 'c', [(0, 1), (1, 0)])  10.4 us
    pallas_call x1, Pallas kernels, back_of(): pl.pallas_call(back_body, out_shape=(jax.ShapeDtypeStruct((2 * UNITS, TOK...  9.35 us
  transfers between devices with their start and end apart: 34, of which 14 were waited for; matrix products, arithmetic and copies ran while one was open for 10% of the time, Pallas kernels for 8%

commit v1 on v0

--- a/solution.py
+++ b/solution.py
@@ -85,12 +85,14 @@
             hidden_ref[rows, cols] = (mixed * sig * value_ref[rows, cols].astype(F32)).astype(BF16)
 
 
-def arrange_body(where_ref, mine_ref, other_ref, out_ref):
+def arrange_body(where_ref, mine_ref, other_ref, grad_ref, inputs_ref):
     for c_off, ref in enumerate((mine_ref, other_ref)):
         for x_off in range(4):
             block = (where_ref[2] + x_off) % 4 * 2 + (where_ref[3] + c_off) % 2
             to = pl.multiple_of(block * COLS, COLS)
-            out_ref[pl.ds(to, COLS), :] = ref[x_off * COLS : (x_off + 1) * COLS, :]
+            at = x_off * COLS
+            grad_ref[pl.ds(to, COLS), :] = ref[at : at + COLS, :TOKS]
+            inputs_ref[pl.ds(to, COLS), :] = ref[at : at + COLS, TOKS:]
 
 
 def back_body(down_ref, grad_ref, gate_ref, value_ref, taps_ref, out_ref, sums_ref, act_ref):
@@ -180,11 +182,12 @@
 
 
 def arranged(where, mine, other):
+    shape = jax.ShapeDtypeStruct((D, TOKS), BF16)
     return pl.pallas_call(
         arrange_body,
-        out_shape=jax.ShapeDtypeStruct((D, TOKS), BF16),
+        out_shape=(shape, shape),
         in_specs=[SMEM, VMEM, VMEM],
-        out_specs=VMEM,
+        out_specs=(VMEM, VMEM),
         compiler_params=PARAMS,
         name="arrange",
     )(where, mine, other)
@@ -269,7 +272,6 @@
     where = jnp.stack([lax.axis_index(a) for a in ("z", "y", "x", "c")]).astype(jnp.int32)
     down = jnp.pad(down_weight.T, ((0, 0), (0, WIDE - UNITS)))
     down_full = lax.all_gather(down, FS, axis=0, tiled=True)
-    inputs_full = over_features(where, inputs.T)
     weights = jnp.concatenate([gate_weight, value_weight], axis=1)
     top = jnp.concatenate(gathered(weights[:HALF], "y"), axis=0)
     low = jnp.concatenate(gathered(weights[HALF:], "z"), axis=0)
@@ -278,7 +280,8 @@
     cot_float = cotangent.astype(F32)
     scaled = norm_gain[None, :] * cot_float
     sums = jnp.concatenate([jnp.sum(normed * normed, axis=1), jnp.sum(normed * scaled, axis=1)])
-    sums = jnp.sum(copy_for_each(sums, TP), axis=0)
+    sums = copy_for_each(sums, TP)
+    sums = jnp.sum(sums, axis=0)
     inverse = lax.rsqrt(sums[:TOKS] / D + EPSILON)
     cross = sums[TOKS:] / D
     grad_pre = (inverse[:, None] * (scaled - normed * (inverse * inverse * cross)[:, None])).astype(
@@ -286,10 +289,10 @@
     )
     gain_local = jnp.sum(cot_float * normed * inverse[:, None], axis=0)
 
-    grad_full = over_features(where, grad_pre.T)
+    both = jnp.concatenate([grad_pre.T, inputs.T], axis=1)
+    grad_full, inputs_full = over_features(where, both)
 
     gate, value, taps = gate_pre.T, value_pre.T, conv_taps.T
-    gate, top, low = lax.optimization_barrier((gate, top, low))
     pieces = (*gathered(top, "z"), *gathered(low, "y"))
     hidden = hidden_of(gate, value, taps)
     grads, taps_local = back_of(down_full, grad_full, gate, value, taps)

time: 250 us -> 252 us (level)
  waiting for transfers between devices: 81.1 us -> 111 us
  starting transfers between devices: 63.5 us -> 51.6 us
  local copies, waits for them, and re-layouts: 26.1 us -> 15.9 us
  blocking collectives: 13.3 us -> 10.6 us
    ppermute x28 -> x24, waiting for transfers between devices: 75.8 us -> 99 us  [moved(): return lax.ppermute(value, axis, [(i, (i + by) % 4) for i in range(4)])]
    ppermute x28 -> x24, starting transfers between devices: 47.7 us -> 37.9 us  [moved(): return lax.ppermute(value, axis, [(i, (i + by) % 4) for i in range(4)])]
    ppermute x3 -> x2, waiting for transfers between devices: 3.25 us -> 7.57 us  [swapped(): return lax.ppermute(value, 'c', [(0, 1), (1, 0)])]
    unnamed x66 -> x46, local copies, waits for them, and re-layouts: 12 us -> 9.16 us
    slice x6 -> x5, local copies, waits for them, and re-layouts: 2.88 us -> 0.13 us  [gathered(): right[half:]]
    all_to_all x1, blocking collectives: 13.3 us -> 10.6 us  [copy_for_each(): return lax.all_to_all(copies, axis, split_axis=0, concat_axis=0, tiled=True)]
    ppermute x3 -> x2, starting transfers between devices: 10.4 us -> 7.88 us  [swapped(): return lax.ppermute(value, 'c', [(0, 1), (1, 0)])]
  transfers between devices with their start and end apart: 34 -> 29, of which waited for: 14 -> 13; matrix products, arithmetic and copies ran while one was open for 10% -> 5% of each run, Pallas kernels for 8% -> 7%
where the time goes in v1:
time: 252 us; the launch traced here: 250 us
  waiting for transfers between devices  111 us (44%)
  starting transfers between devices  51.6 us (20%)
  Pallas kernels  41.1 us (16%)
  local copies, waits for them, and re-layouts  15.9 us (6%)
  between operations  14.4 us (6%)
  blocking collectives  10.6 us (4%)
  other arithmetic  5.66 us (2%)
    ppermute x24, waiting for transfers between devices, moved(): return lax.ppermute(value, axis, [(i, (i + by) % 4) for i in range(4)])  99 us
    ppermute x24, starting transfers between devices, moved(): return lax.ppermute(value, axis, [(i, (i + by) % 4) for i in range(4)])  37.9 us
    pallas_call x1, Pallas kernels, outer_of(): pl.pallas_call(outer_body, out_shape=jax.ShapeDtypeStruct((D, 3 * UNITS),...  13.4 us
    pallas_call x1, Pallas kernels, input_of(): pl.pallas_call(input_body, out_shape=(shape, shape), in_specs=[SMEM] + [V...  12.5 us
    all_to_all x1, blocking collectives, copy_for_each(): return lax.all_to_all(copies, axis, split_axis=0, concat_axis=0, tiled=True)  10.6 us
    pallas_call x1, Pallas kernels, back_of(): pl.pallas_call(back_body, out_shape=(jax.ShapeDtypeStruct((2 * UNITS, TOK...  9.29 us
    unnamed x46, local copies, waits for them, and re-layouts  9.16 us
    ppermute x2, starting transfers between devices, swapped(): return lax.ppermute(value, 'c', [(0, 1), (1, 0)])  7.88 us
  transfers between devices with their start and end apart: 29, of which 13 were waited for; matrix products, arithmetic and copies ran while one was open for 5% of the time, Pallas kernels for 7%

profile of v1, /device:TPU:1, one launch (start us, length us, event | category | flops | bytes accessed | tf_op | source)
XLA Modules:
  0.0 250.4 jit_solution(8987666184031047258)
XLA Ops:
  7.2 1.8 pad.4
  9.0 1.2 copy.33
  11.3 5.8 %all-to-all-start = ((f32[8,1,1024]{2,1,0:T(1,128)}), f32[8,1,1024]{2,1,0:T(1,128)S(1)}, u32[]{:S(2)}, u32[]{:S(2)}) async-start(f32[8,1,1024]{2,1,0:T(1,128)} %broadcast_in_dim.4), calls=%async_computation | async-start | bytes 65536 | tf_op jit(solution)/shard_map/all_to_all | solution.py:251
  17.3 4.5 %all-to-all-done = f32[8,1,1024]{2,1,0:T(1,128)S(1)} async-done(((f32[8,1,1024]{2,1,0:T(1,128)}), f32[8,1,1024]{2,1,0:T(1,128)S(1)}, u32[]{:S(2)}, u32[]{:S(2)}) %all-to-all-start) | async-done | bytes 32800 | tf_op jit(solution)/shard_map/all_to_all | solution.py:251
  22.2 1.1 pad_maximum_fusion
  23.6 2.4 collective-permute-start
  26.0 16.9 %collective-permute-done.1 = bf16[384,1024]{1,0:T(8,128)(2,1)S(1)} collective-permute-done((bf16[384,1024]{1,0:T(8,128)(2,1)S(1)}, bf16[384,1024]{1,0:T(8,128)(2,1)S(1)}, u32[]{:S(2)}, u32[]{:S(2)}) %collective-permute-start.1) | collective-permute-done | bytes 786464 | tf_op jit(solution)/shard_map/ppermute | solution.py:30
  43.0 2.7 %collective-permute-start.3 = (bf16[192,1024]{1,0:T(8,128)(2,1)S(1)}, bf16[192,1024]{1,0:T(8,128)(2,1)S(1)}, u32[]{:S(2)}, u32[]{:S(2)}) collective-permute-start(bf16[192,1024]{1,0:T(8,128)(2,1)S(1)} %slice.111), channel_id=1, source_target_pairs={{0,6},{2,0},{4,2},{6,4},{1,7},{3,1},{5,3},{7,5},{8,14},{10,8},{12,... | collective-permute-start | bytes 1179656 | tf_op jit(solution)/shard_map/ppermute | solution.py:30
  45.7 0.9 constant_dynamic-update-slice_fusion.3
  46.7 6.7 %collective-permute-done.2 = bf16[192,1024]{1,0:T(8,128)(2,1)S(1)} collective-permute-done((bf16[192,1024]{1,0:T(8,128)(2,1)S(1)}, bf16[192,1024]{1,0:T(8,128)(2,1)S(1)}, u32[]{:S(2)}, u32[]{:S(2)}) %collective-permute-start.2) | collective-permute-done | bytes 393248 | tf_op jit(solution)/shard_map/ppermute | solution.py:30
  54.1 0.8 constant_dynamic-update-slice_fusion.1
  54.9 0.9 constant_dynamic-update-slice_fusion.mine_ref
  55.9 2.3 collective-permute-start.4
  58.4 1.0 hidden.1.hidden_ref
  59.5 4.3 %collective-permute-done.4.other_ref = bf16[1536,1024]{1,0:T(8,128)(2,1)} collective-permute-done((bf16[1536,1024]{1,0:T(8,128)(2,1)}, bf16[1536,1024]{1,0:T(8,128)(2,1)}, u32[]{:S(2)}, u32[]{:S(2)}) %collective-permute-start.4) | collective-permute-done | bytes 3145760 | tf_op jit(solution)/shard_map/ppermute | solution.py:34
  63.8 4.9 %arrange.1 = (bf16[3072,512]{1,0:T(8,128)(2,1)S(1)}, bf16[3072,512]{1,0:T(8,128)(2,1)}) custom-call(s32[4]{0:T(128)S(1)} %pad_add_fusion.where_ref, bf16[1536,1024]{1,0:T(8,128)(2,1)} %constant_dynamic-update-slice_fusion.mine_ref, bf16[1536,1024]{1,0:T(8,128)(2,1)} %collective-permute-done.4.other_ref), custom_call_target="tpu_custom_call" | custom-call | tf_op jit(solution)/shard_map/arrange/pallas_call | solution.py:186
  68.7 1.6 copy-done
  70.4 9.3 %back.1 = (bf16[1408,512]{1,0:T(8,128)(2,1)S(1)}, f32[704,3]{1,0:T(8,128)S(1)}) custom-call(bf16[3072,768]{1,0:T(8,128)(2,1)} %all-gather.2.cloned.1.call-done.down_ref, bf16[3072,512]{1,0:T(8,128)(2,1)} %copy-done, bf16[704,512]{1,0:T(8,128)(2,1)S(1)} %bitcast.20, bf16[704,512]{1,0:T(8,128)(2,1)S(1)} %bitcast.22, f32[704,3]{1,0:T(8,128)S(1)} %bitcast.18), custom_call_target="tpu_custom_call" | custom-call | flops 2214592512 | bytes 12000000 | tf_op jit(solution)/shard_map/back/pallas_call | solution.py:197
  79.7 13.4 %outer.1 = bf16[3072,2112]{1,0:T(8,128)(2,1)} custom-call(bf16[3072,512]{1,0:T(8,128)(2,1)} %get-tuple-element.16.inputs_ref, bf16[3072,512]{1,0:T(8,128)(2,1)} %copy-done, bf16[1408,512]{1,0:T(8,128)(2,1)S(1)} %get-tuple-element.13.right_ref.both_ref, bf16[704,512]{1,0:T(8,128)(2,1)S(1)} %hidden.1.hidden_ref), custom_call_target="tpu_custom_call" | custom-call | flops 6643777536 | bytes 20000000 | tf_op jit(solution)/shard_map/outer/pallas_call | solution.py:215
  93.0 1.1 copy-done.3
  94.2 0.9 copy-done.7
  95.4 1.3 collective-permute-start.6
  96.7 1.5 collective-permute-start.5
  98.3 1.6 collective-permute-start.14
  99.9 2.1 collective-permute-start.13
  102.0 2.4 collective-permute-done.6
  104.6 2.7 %collective-permute-start.8 = (bf16[48,1408]{1,0:T(8,128)(2,1)S(1)}, bf16[48,1408]{1,0:T(8,128)(2,1)S(1)}, u32[]{:S(2)}, u32[]{:S(2)}) collective-permute-start(bf16[48,1408]{1,0:T(8,128)(2,1)S(1)} %slice.115), channel_id=1, source_target_pairs={{0,24},{8,0},{16,8},{24,16},{1,25},{9,1},{17,9},{25,17},{2,26},{10... | collective-permute-start | bytes 405512 | tf_op jit(solution)/shard_map/ppermute | solution.py:30
  108.1 0.9 collective-permute-start.15
  109.1 3.6 %collective-permute-start.16 = (bf16[48,1408]{1,0:T(8,128)(2,1)S(1)}, bf16[48,1408]{1,0:T(8,128)(2,1)S(1)}, u32[]{:S(2)}, u32[]{:S(2)}) collective-permute-start(bf16[48,1408]{1,0:T(8,128)(2,1)S(1)} %slice.119), channel_id=1, source_target_pairs={{0,96},{32,0},{64,32},{96,64},{1,97},{33,1},{65,33},{97,65},{2,98}... | collective-permute-start | bytes 405512 | tf_op jit(solution)/shard_map/ppermute | solution.py:30
  113.6 1.7 collective-permute-start.10
  115.3 2.4 collective-permute-start.9
  117.9 2.6 %collective-permute-start.17 = (bf16[384,1408]{1,0:T(8,128)(2,1)S(1)}, bf16[384,1408]{1,0:T(8,128)(2,1)S(1)}, u32[]{:S(2)}, u32[]{:S(2)}) collective-permute-start(bf16[384,1408]{1,0:T(8,128)(2,1)S(1)} %constant_dynamic-update-slice_fusion.10.rest_5_), channel_id=1, source_target_pairs={{0,24},{8,0},{16,8},{24,16},{1,25},{9,1},{17,9},{25,17},{2,26},{10... | collective-permute-start | bytes 3244040 | tf_op jit(solution)/shard_map/ppermute | solution.py:30
  120.5 44.2 %collective-permute-done.10.rest_4_ = bf16[384,1408]{1,0:T(8,128)(2,1)S(1)} collective-permute-done((bf16[384,1408]{1,0:T(8,128)(2,1)S(1)}, bf16[384,1408]{1,0:T(8,128)(2,1)S(1)}, u32[]{:S(2)}, u32[]{:S(2)}) %collective-permute-start.10) | collective-permute-done | bytes 1081376 | tf_op jit(solution)/shard_map/ppermute | solution.py:30
  164.9 3.2 %collective-permute-start.12 = (bf16[192,1408]{1,0:T(8,128)(2,1)S(1)}, bf16[192,1408]{1,0:T(8,128)(2,1)S(1)}, u32[]{:S(2)}, u32[]{:S(2)}) collective-permute-start(bf16[192,1408]{1,0:T(8,128)(2,1)S(1)} %slice.117), channel_id=1, source_target_pairs={{0,96},{32,0},{64,32},{96,64},{1,97},{33,1},{65,33},{97,65},{2,98}... | collective-permute-start | bytes 1622024 | tf_op jit(solution)/shard_map/ppermute | solution.py:30
  168.4 2.7 %collective-permute-start.20 = (bf16[192,1408]{1,0:T(8,128)(2,1)S(1)}, bf16[192,1408]{1,0:T(8,128)(2,1)S(1)}, u32[]{:S(2)}, u32[]{:S(2)}) collective-permute-start(bf16[192,1408]{1,0:T(8,128)(2,1)S(1)} %slice.121), channel_id=1, source_target_pairs={{0,24},{8,0},{16,8},{24,16},{1,25},{9,1},{17,9},{25,17},{2,26},{10... | collective-permute-start | bytes 1622024 | tf_op jit(solution)/shard_map/ppermute | solution.py:30
  171.1 20.0 %collective-permute-done.11.rest_2_ = bf16[192,1408]{1,0:T(8,128)(2,1)S(1)} collective-permute-done((bf16[192,1408]{1,0:T(8,128)(2,1)S(1)}, bf16[192,1408]{1,0:T(8,128)(2,1)S(1)}, u32[]{:S(2)}, u32[]{:S(2)}) %collective-permute-start.11) | collective-permute-done | bytes 540704 | tf_op jit(solution)/shard_map/ppermute | solution.py:30
  191.1 2.4 collective-permute-done.19.rest_7_
  193.5 12.5 %grad_input.1 = (bf16[1536,512]{1,0:T(8,128)(2,1)}, bf16[1536,512]{1,0:T(8,128)(2,1)}) custom-call(s32[4]{0:T(128)S(1)} %pad_add_fusion.where_ref, bf16[1408,512]{1,0:T(8,128)(2,1)} %copy-done.3, bf16[384,1408]{1,0:T(8,128)(2,1)S(1)} %constant_dynamic-update-slice_fusion.5.rest_0_, bf16[384,1408]{1,0:T(8,128)(2,1)} %copy-done.10, ...), custom_call_target="tpu_custom_call" | custom-call | flops 4429185024 | bytes 15000000 | tf_op jit(solution)/shard_map/grad_input/pallas_call | solution.py:236
  206.1 5.5 %collective-permute-start.21 = (bf16[1536,512]{1,0:T(8,128)(2,1)}, bf16[1536,512]{1,0:T(8,128)(2,1)S(1)}, u32[]{:S(2)}, u32[]{:S(2)}) collective-permute-start(bf16[1536,512]{1,0:T(8,128)(2,1)} %get-tuple-element.15), channel_id=1, source_target_pairs={{0,1},{1,0},{2,3},{3,2},{4,5},{5,4},{6,7},{7,6},{8,9},{9,8},{10,11... | collective-permute-start | bytes 4718600 | tf_op jit(solution)/shard_map/ppermute | solution.py:34
  211.6 3.2 %collective-permute-done.21 = bf16[1536,512]{1,0:T(8,128)(2,1)S(1)} collective-permute-done((bf16[1536,512]{1,0:T(8,128)(2,1)}, bf16[1536,512]{1,0:T(8,128)(2,1)S(1)}, u32[]{:S(2)}, u32[]{:S(2)}) %collective-permute-start.21) | collective-permute-done | bytes 1572896 | tf_op jit(solution)/shard_map/ppermute | solution.py:34
  214.9 1.9 add_convert_fusion
  216.9 2.7 %collective-permute-start.24 = (bf16[192,512]{1,0:T(8,128)(2,1)S(1)}, bf16[192,512]{1,0:T(8,128)(2,1)S(1)}, u32[]{:S(2)}, u32[]{:S(2)}) collective-permute-start(bf16[192,512]{1,0:T(8,128)(2,1)S(1)} %get-tuple-element.51), channel_id=1, source_target_pairs={{0,6},{2,0},{4,2},{6,4},{1,7},{3,1},{5,3},{7,5},{8,14},{10,8},{12,... | collective-permute-start | bytes 589832 | tf_op jit(solution)/shard_map/ppermute | solution.py:30
  219.6 4.7 %collective-permute-done.22 = bf16[192,512]{1,0:T(8,128)(2,1)S(1)} collective-permute-done((bf16[192,512]{1,0:T(8,128)(2,1)S(1)}, bf16[192,512]{1,0:T(8,128)(2,1)S(1)}, u32[]{:S(2)}, u32[]{:S(2)}) %collective-permute-start.22) | collective-permute-done | bytes 196640 | tf_op jit(solution)/shard_map/ppermute | solution.py:30
  224.6 2.7 %collective-permute-start.25 = (bf16[384,512]{1,0:T(8,128)(2,1)S(1)}, bf16[384,512]{1,0:T(8,128)(2,1)S(1)}, u32[]{:S(2)}, u32[]{:S(2)}) collective-permute-start(bf16[384,512]{1,0:T(8,128)(2,1)S(1)} %pad_maximum_fusion.2), channel_id=1, source_target_pairs={{0,6},{2,0},{4,2},{6,4},{1,7},{3,1},{5,3},{7,5},{8,14},{10,8},{12,... | collective-permute-start | bytes 1179656 | tf_op jit(solution)/shard_map/ppermute | solution.py:30
  227.7 10.6 %all_to_all.12 = f32[16,1,2496]{2,1,0:T(1,128)S(1)} all-to-all(f32[16,1,2496]{2,1,0:T(1,128)S(1)} %broadcast_in_dim.5), channel_id=1, replica_groups=mesh['z'=4,'y'=4,'x'=4,'c'=2] {'z','y'}, dimensions={0} | all-to-all | bytes 319488 | tf_op jit(solution)/shard_map/all_to_all | solution.py:251
  239.8 0.9 copy.40
  240.8 1.3 convert_element_type.73
  242.2 1.3 fusion.12
  (102 shorter events, 8.3 us)
Async XLA Ops:
  7.2 3.0 %copy-start.5 = (bf16[512,384]{1,0:T(8,128)(2,1)S(1)}, bf16[512,384]{1,0:T(8,128)(2,1)}, u32[]{:S(2)}) copy-start(bf16[512,384]{1,0:T(8,128)(2,1)} %param.11) | copy-start | bytes 1179652
  7.2 3.2 %copy-start.15 = (f32[384]{0:T(512)S(1)}, f32[384]{0:T(512)}, u32[]{:S(2)}) copy-start(f32[384]{0:T(512)} %param.19) | copy-start | bytes 4612
  7.2 63.2 %all-gather.2.cloned.1.call-start = ((), (), s32[]{:S(2)}) async-start(), calls=%async_computation.3 | async-start | bytes 5013504 | tf_op jit(solution)/shard_map/all_gather | solution.py:274
  7.2 9.8 %copy-start.6 = (bf16[512,384]{1,0:T(8,128)(2,1)S(1)}, bf16[512,384]{1,0:T(8,128)(2,1)}, u32[]{:S(2)}) copy-start(bf16[512,384]{1,0:T(8,128)(2,1)} %param.10) | copy-start | bytes 1179652
  11.3 10.5 %all-to-all-start = ((f32[8,1,1024]{2,1,0:T(1,128)}), f32[8,1,1024]{2,1,0:T(1,128)S(1)}, u32[]{:S(2)}, u32[]{:S(2)}) async-start(f32[8,1,1024]{2,1,0:T(1,128)} %broadcast_in_dim.4), calls=%async_computation | async-start | bytes 65536 | tf_op jit(solution)/shard_map/all_to_all | solution.py:251
  17.1 223.7 %reduce-scatter.2.cloned.1.call-start = ((), (), s32[]{:S(2)}) async-start(), calls=%async_computation.4 | async-start | bytes 14204928 | tf_op jit(solution)/shard_map/reduce_scatter | solution.py:300
  23.3 19.6 %collective-permute-start.1 = (bf16[384,1024]{1,0:T(8,128)(2,1)S(1)}, bf16[384,1024]{1,0:T(8,128)(2,1)S(1)}, u32[]{:S(2)}, u32[]{:S(2)}) collective-permute-start(bf16[384,1024]{1,0:T(8,128)(2,1)S(1)} %get-tuple-element.58), channel_id=1, source_target_pairs={{0,2},{2,4},{4,6},{6,0},{1,3},{3,5},{5,7},{7,1},{8,10},{10,12},{12... | collective-permute-start | bytes 2359304 | tf_op jit(solution)/shard_map/ppermute | solution.py:30
  23.6 19.4 %collective-permute-start = (bf16[384,1024]{1,0:T(8,128)(2,1)S(1)}, bf16[384,1024]{1,0:T(8,128)(2,1)S(1)}, u32[]{:S(2)}, u32[]{:S(2)}) collective-permute-start(bf16[384,1024]{1,0:T(8,128)(2,1)S(1)} %get-tuple-element.58), channel_id=1, source_target_pairs={{0,6},{2,0},{4,2},{6,4},{1,7},{3,1},{5,3},{7,5},{8,14},{10,8},{12,... | collective-permute-start | bytes 2359304 | tf_op jit(solution)/shard_map/ppermute | solution.py:30
  42.9 10.5 %collective-permute-start.2 = (bf16[192,1024]{1,0:T(8,128)(2,1)S(1)}, bf16[192,1024]{1,0:T(8,128)(2,1)S(1)}, u32[]{:S(2)}, u32[]{:S(2)}) collective-permute-start(bf16[192,1024]{1,0:T(8,128)(2,1)S(1)} %slice.110), channel_id=1, source_target_pairs={{0,2},{2,4},{4,6},{6,0},{1,3},{3,5},{5,7},{7,1},{8,10},{10,12},{12... | collective-permute-start | bytes 1179656 | tf_op jit(solution)/shard_map/ppermute | solution.py:30
  43.0 11.1 %collective-permute-start.3 = (bf16[192,1024]{1,0:T(8,128)(2,1)S(1)}, bf16[192,1024]{1,0:T(8,128)(2,1)S(1)}, u32[]{:S(2)}, u32[]{:S(2)}) collective-permute-start(bf16[192,1024]{1,0:T(8,128)(2,1)S(1)} %slice.111), channel_id=1, source_target_pairs={{0,6},{2,0},{4,2},{6,4},{1,7},{3,1},{5,3},{7,5},{8,14},{10,8},{12,... | collective-permute-start | bytes 1179656 | tf_op jit(solution)/shard_map/ppermute | solution.py:30
  46.7 11.5 %copy-start.14 = (f32[3,704]{1,0:T(4,128)S(1)}, f32[3,704]{1,0:T(4,128)}, u32[]{:S(2)}) copy-start(f32[3,704]{1,0:T(4,128)} %param.18) | copy-start | bytes 25348
  54.1 4.3 %copy-start.1 = (bf16[512,704]{0,1:T(8,128)(2,1)S(1)}, bf16[512,704]{0,1:T(8,128)(2,1)}, u32[]{:S(2)}) copy-start(bf16[512,704]{0,1:T(8,128)(2,1)} %param.13) | copy-start | bytes 2162692
  54.1 4.3 %copy-start.2 = (bf16[512,704]{0,1:T(8,128)(2,1)S(1)}, bf16[512,704]{0,1:T(8,128)(2,1)}, u32[]{:S(2)}) copy-start(bf16[512,704]{0,1:T(8,128)(2,1)} %param.14) | copy-start | bytes 2162692
  55.9 8.0 %collective-permute-start.4 = (bf16[1536,1024]{1,0:T(8,128)(2,1)}, bf16[1536,1024]{1,0:T(8,128)(2,1)}, u32[]{:S(2)}, u32[]{:S(2)}) collective-permute-start(bf16[1536,1024]{1,0:T(8,128)(2,1)} %constant_dynamic-update-slice_fusion.mine_ref), channel_id=1, source_target_pairs={{0,1},{1,0},{2,3},{3,2},{4,5},{5,4},{6,7},{7,6},{8,9},{9,8},{10,11... | collective-permute-start | bytes 9437192 | tf_op jit(solution)/shard_map/ppermute | solution.py:34
  68.7 1.6 copy-start
  93.0 1.1 copy-start.3
  94.2 1.0 copy-start.7
  94.2 1.0 copy-start.8
  95.4 9.1 %collective-permute-start.6 = (bf16[96,1408]{1,0:T(8,128)(2,1)S(1)}, bf16[96,1408]{1,0:T(8,128)(2,1)S(1)}, u32[]{:S(2)}, u32[]{:S(2)}) collective-permute-start(bf16[96,1408]{1,0:T(8,128)(2,1)S(1)} %get-tuple-element.61), channel_id=1, source_target_pairs={{0,8},{8,16},{16,24},{24,0},{1,9},{9,17},{17,25},{25,1},{2,10},{10... | collective-permute-start | bytes 811016 | tf_op jit(solution)/shard_map/ppermute | solution.py:30
  96.7 7.8 %collective-permute-start.5 = (bf16[96,1408]{1,0:T(8,128)(2,1)S(1)}, bf16[96,1408]{1,0:T(8,128)(2,1)S(1)}, u32[]{:S(2)}, u32[]{:S(2)}) collective-permute-start(bf16[96,1408]{1,0:T(8,128)(2,1)S(1)} %get-tuple-element.61), channel_id=1, source_target_pairs={{0,24},{8,0},{16,8},{24,16},{1,25},{9,1},{17,9},{25,17},{2,26},{10... | collective-permute-start | bytes 811016 | tf_op jit(solution)/shard_map/ppermute | solution.py:30
  98.3 9.8 %collective-permute-start.14 = (bf16[96,1408]{1,0:T(8,128)(2,1)S(1)}, bf16[96,1408]{1,0:T(8,128)(2,1)S(1)}, u32[]{:S(2)}, u32[]{:S(2)}) collective-permute-start(bf16[96,1408]{1,0:T(8,128)(2,1)S(1)} %get-tuple-element.45), channel_id=1, source_target_pairs={{0,32},{32,64},{64,96},{96,0},{1,33},{33,65},{65,97},{97,1},{2,34}... | collective-permute-start | bytes 811016 | tf_op jit(solution)/shard_map/ppermute | solution.py:30
  99.9 9.2 %collective-permute-start.13 = (bf16[96,1408]{1,0:T(8,128)(2,1)S(1)}, bf16[96,1408]{1,0:T(8,128)(2,1)S(1)}, u32[]{:S(2)}, u32[]{:S(2)}) collective-permute-start(bf16[96,1408]{1,0:T(8,128)(2,1)S(1)} %get-tuple-element.45), channel_id=1, source_target_pairs={{0,96},{32,0},{64,32},{96,64},{1,97},{33,1},{65,33},{97,65},{2,98}... | collective-permute-start | bytes 811016 | tf_op jit(solution)/shard_map/ppermute | solution.py:30
  104.5 9.1 %collective-permute-start.7 = (bf16[48,1408]{1,0:T(8,128)(2,1)S(1)}, bf16[48,1408]{1,0:T(8,128)(2,1)S(1)}, u32[]{:S(2)}, u32[]{:S(2)}) collective-permute-start(bf16[48,1408]{1,0:T(8,128)(2,1)S(1)} %slice.114), channel_id=1, source_target_pairs={{0,8},{8,16},{16,24},{24,0},{1,9},{9,17},{17,25},{25,1},{2,10},{10... | collective-permute-start | bytes 405512 | tf_op jit(solution)/shard_map/ppermute | solution.py:30
  104.6 9.0 %collective-permute-start.8 = (bf16[48,1408]{1,0:T(8,128)(2,1)S(1)}, bf16[48,1408]{1,0:T(8,128)(2,1)S(1)}, u32[]{:S(2)}, u32[]{:S(2)}) collective-permute-start(bf16[48,1408]{1,0:T(8,128)(2,1)S(1)} %slice.115), channel_id=1, source_target_pairs={{0,24},{8,0},{16,8},{24,16},{1,25},{9,1},{17,9},{25,17},{2,26},{10... | collective-permute-start | bytes 405512 | tf_op jit(solution)/shard_map/ppermute | solution.py:30
  108.1 9.6 %collective-permute-start.15 = (bf16[48,1408]{1,0:T(8,128)(2,1)S(1)}, bf16[48,1408]{1,0:T(8,128)(2,1)S(1)}, u32[]{:S(2)}, u32[]{:S(2)}) collective-permute-start(bf16[48,1408]{1,0:T(8,128)(2,1)S(1)} %slice.118), channel_id=1, source_target_pairs={{0,32},{32,64},{64,96},{96,0},{1,33},{33,65},{65,97},{97,1},{2,34}... | collective-permute-start | bytes 405512 | tf_op jit(solution)/shard_map/ppermute | solution.py:30
  109.1 8.6 %collective-permute-start.16 = (bf16[48,1408]{1,0:T(8,128)(2,1)S(1)}, bf16[48,1408]{1,0:T(8,128)(2,1)S(1)}, u32[]{:S(2)}, u32[]{:S(2)}) collective-permute-start(bf16[48,1408]{1,0:T(8,128)(2,1)S(1)} %slice.119), channel_id=1, source_target_pairs={{0,96},{32,0},{64,32},{96,64},{1,97},{33,1},{65,33},{97,65},{2,98}... | collective-permute-start | bytes 405512 | tf_op jit(solution)/shard_map/ppermute | solution.py:30
  113.6 51.1 %collective-permute-start.10 = (bf16[384,1408]{1,0:T(8,128)(2,1)S(1)}, bf16[384,1408]{1,0:T(8,128)(2,1)S(1)}, u32[]{:S(2)}, u32[]{:S(2)}) collective-permute-start(bf16[384,1408]{1,0:T(8,128)(2,1)S(1)} %constant_dynamic-update-slice_fusion.5.rest_0_), channel_id=1, source_target_pairs={{0,32},{32,64},{64,96},{96,0},{1,33},{33,65},{65,97},{97,1},{2,34}... | collective-permute-start | bytes 3244040 | tf_op jit(solution)/shard_map/ppermute | solution.py:30
  115.3 49.6 %collective-permute-start.9 = (bf16[384,1408]{1,0:T(8,128)(2,1)S(1)}, bf16[384,1408]{1,0:T(8,128)(2,1)S(1)}, u32[]{:S(2)}, u32[]{:S(2)}) collective-permute-start(bf16[384,1408]{1,0:T(8,128)(2,1)S(1)} %constant_dynamic-update-slice_fusion.5.rest_0_), channel_id=1, source_target_pairs={{0,96},{32,0},{64,32},{96,64},{1,97},{33,1},{65,33},{97,65},{2,98}... | collective-permute-start | bytes 3244040 | tf_op jit(solution)/shard_map/ppermute | solution.py:30
  117.8 75.7 %copy-start.13 = (bf16[384,1408]{1,0:T(8,128)(2,1)}, bf16[384,1408]{1,0:T(8,128)(2,1)S(1)}, u32[]{:S(2)}) copy-start(bf16[384,1408]{1,0:T(8,128)(2,1)S(1)} %constant_dynamic-update-slice_fusion.10.rest_5_) | copy-start | bytes 3244036
  117.8 50.4 %collective-permute-start.18 = (bf16[384,1408]{1,0:T(8,128)(2,1)S(1)}, bf16[384,1408]{1,0:T(8,128)(2,1)S(1)}, u32[]{:S(2)}, u32[]{:S(2)}) collective-permute-start(bf16[384,1408]{1,0:T(8,128)(2,1)S(1)} %constant_dynamic-update-slice_fusion.10.rest_5_), channel_id=1, source_target_pairs={{0,8},{8,16},{16,24},{24,0},{1,9},{9,17},{17,25},{25,1},{2,10},{10... | collective-permute-start | bytes 3244040 | tf_op jit(solution)/shard_map/ppermute | solution.py:30
  117.9 50.4 %collective-permute-start.17 = (bf16[384,1408]{1,0:T(8,128)(2,1)S(1)}, bf16[384,1408]{1,0:T(8,128)(2,1)S(1)}, u32[]{:S(2)}, u32[]{:S(2)}) collective-permute-start(bf16[384,1408]{1,0:T(8,128)(2,1)S(1)} %constant_dynamic-update-slice_fusion.10.rest_5_), channel_id=1, source_target_pairs={{0,24},{8,0},{16,8},{24,16},{1,25},{9,1},{17,9},{25,17},{2,26},{10... | collective-permute-start | bytes 3244040 | tf_op jit(solution)/shard_map/ppermute | solution.py:30
  164.7 3.5 %copy-start.9 = (bf16[384,1408]{1,0:T(8,128)(2,1)}, bf16[384,1408]{1,0:T(8,128)(2,1)S(1)}, u32[]{:S(2)}) copy-start(bf16[384,1408]{1,0:T(8,128)(2,1)S(1)} %collective-permute-done.10.rest_4_) | copy-start | bytes 3244036
  164.8 26.3 %collective-permute-start.11 = (bf16[192,1408]{1,0:T(8,128)(2,1)S(1)}, bf16[192,1408]{1,0:T(8,128)(2,1)S(1)}, u32[]{:S(2)}, u32[]{:S(2)}) collective-permute-start(bf16[192,1408]{1,0:T(8,128)(2,1)S(1)} %slice.116), channel_id=1, source_target_pairs={{0,32},{32,64},{64,96},{96,0},{1,33},{33,65},{65,97},{97,1},{2,34}... | collective-permute-start | bytes 1622024 | tf_op jit(solution)/shard_map/ppermute | solution.py:30
  164.9 3.5 %copy-start.10 = (bf16[384,1408]{1,0:T(8,128)(2,1)}, bf16[384,1408]{1,0:T(8,128)(2,1)S(1)}, u32[]{:S(2)}) copy-start(bf16[384,1408]{1,0:T(8,128)(2,1)S(1)} %collective-permute-done.9.rest_1_) | copy-start | bytes 3244036
  164.9 26.2 %collective-permute-start.12 = (bf16[192,1408]{1,0:T(8,128)(2,1)S(1)}, bf16[192,1408]{1,0:T(8,128)(2,1)S(1)}, u32[]{:S(2)}, u32[]{:S(2)}) collective-permute-start(bf16[192,1408]{1,0:T(8,128)(2,1)S(1)} %slice.117), channel_id=1, source_target_pairs={{0,96},{32,0},{64,32},{96,64},{1,97},{33,1},{65,33},{97,65},{2,98}... | collective-permute-start | bytes 1622024 | tf_op jit(solution)/shard_map/ppermute | solution.py:30
  168.2 25.3 %copy-start.11 = (bf16[384,1408]{1,0:T(8,128)(2,1)}, bf16[384,1408]{1,0:T(8,128)(2,1)S(1)}, u32[]{:S(2)}) copy-start(bf16[384,1408]{1,0:T(8,128)(2,1)S(1)} %collective-permute-done.18.rest_9_) | copy-start | bytes 3244036
  168.2 25.3 %collective-permute-start.19 = (bf16[192,1408]{1,0:T(8,128)(2,1)S(1)}, bf16[192,1408]{1,0:T(8,128)(2,1)S(1)}, u32[]{:S(2)}, u32[]{:S(2)}) collective-permute-start(bf16[192,1408]{1,0:T(8,128)(2,1)S(1)} %slice.120), channel_id=1, source_target_pairs={{0,8},{8,16},{16,24},{24,0},{1,9},{9,17},{17,25},{25,1},{2,10},{10... | collective-permute-start | bytes 1622024 | tf_op jit(solution)/shard_map/ppermute | solution.py:30
  168.4 25.2 %copy-start.12 = (bf16[384,1408]{1,0:T(8,128)(2,1)}, bf16[384,1408]{1,0:T(8,128)(2,1)S(1)}, u32[]{:S(2)}) copy-start(bf16[384,1408]{1,0:T(8,128)(2,1)S(1)} %collective-permute-done.17.rest_6_) | copy-start | bytes 3244036
  168.4 25.1 %collective-permute-start.20 = (bf16[192,1408]{1,0:T(8,128)(2,1)S(1)}, bf16[192,1408]{1,0:T(8,128)(2,1)S(1)}, u32[]{:S(2)}, u32[]{:S(2)}) collective-permute-start(bf16[192,1408]{1,0:T(8,128)(2,1)S(1)} %slice.121), channel_id=1, source_target_pairs={{0,24},{8,0},{16,8},{24,16},{1,25},{9,1},{17,9},{25,17},{2,26},{10... | collective-permute-start | bytes 1622024 | tf_op jit(solution)/shard_map/ppermute | solution.py:30
  206.1 8.8 %collective-permute-start.21 = (bf16[1536,512]{1,0:T(8,128)(2,1)}, bf16[1536,512]{1,0:T(8,128)(2,1)S(1)}, u32[]{:S(2)}, u32[]{:S(2)}) collective-permute-start(bf16[1536,512]{1,0:T(8,128)(2,1)} %get-tuple-element.15), channel_id=1, source_target_pairs={{0,1},{1,0},{2,3},{3,2},{4,5},{5,4},{6,7},{7,6},{8,9},{9,8},{10,11... | collective-permute-start | bytes 4718600 | tf_op jit(solution)/shard_map/ppermute | solution.py:34
  216.8 7.5 %collective-permute-start.22 = (bf16[192,512]{1,0:T(8,128)(2,1)S(1)}, bf16[192,512]{1,0:T(8,128)(2,1)S(1)}, u32[]{:S(2)}, u32[]{:S(2)}) collective-permute-start(bf16[192,512]{1,0:T(8,128)(2,1)S(1)} %get-tuple-element.50), channel_id=1, source_target_pairs={{0,2},{2,4},{4,6},{6,0},{1,3},{3,5},{5,7},{7,1},{8,10},{10,12},{12... | collective-permute-start | bytes 589832 | tf_op jit(solution)/shard_map/ppermute | solution.py:30
  216.9 7.4 %collective-permute-start.24 = (bf16[192,512]{1,0:T(8,128)(2,1)S(1)}, bf16[192,512]{1,0:T(8,128)(2,1)S(1)}, u32[]{:S(2)}, u32[]{:S(2)}) collective-permute-start(bf16[192,512]{1,0:T(8,128)(2,1)S(1)} %get-tuple-element.51), channel_id=1, source_target_pairs={{0,6},{2,0},{4,2},{6,4},{1,7},{3,1},{5,3},{7,5},{8,14},{10,8},{12,... | collective-permute-start | bytes 589832 | tf_op jit(solution)/shard_map/ppermute | solution.py:30
  224.4 15.3 %collective-permute-start.23 = (bf16[384,512]{1,0:T(8,128)(2,1)S(1)}, bf16[384,512]{1,0:T(8,128)(2,1)S(1)}, u32[]{:S(2)}, u32[]{:S(2)}) collective-permute-start(bf16[384,512]{1,0:T(8,128)(2,1)S(1)} %pad_maximum_fusion.1), channel_id=1, source_target_pairs={{0,2},{2,4},{4,6},{6,0},{1,3},{3,5},{5,7},{7,1},{8,10},{10,12},{12... | collective-permute-start | bytes 1179656 | tf_op jit(solution)/shard_map/ppermute | solution.py:30
  224.6 15.1 %collective-permute-start.25 = (bf16[384,512]{1,0:T(8,128)(2,1)S(1)}, bf16[384,512]{1,0:T(8,128)(2,1)S(1)}, u32[]{:S(2)}, u32[]{:S(2)}) collective-permute-start(bf16[384,512]{1,0:T(8,128)(2,1)S(1)} %pad_maximum_fusion.2), channel_id=1, source_target_pairs={{0,6},{2,0},{4,2},{6,4},{1,7},{3,1},{5,3},{7,5},{8,14},{10,8},{12,... | collective-permute-start | bytes 1179656 | tf_op jit(solution)/shard_map/ppermute | solution.py:30
  240.8 1.4 copy-start.4
Sparse Core Ops, SparseCore 0:
  10.7 56.9 all-gather.1
  94.3 133.1 reduce-scatter.1

commit v2 on v1

--- a/solution.py
+++ b/solution.py
@@ -85,14 +85,26 @@
             hidden_ref[rows, cols] = (mixed * sig * value_ref[rows, cols].astype(F32)).astype(BF16)
 
 
-def arrange_body(where_ref, mine_ref, other_ref, grad_ref, inputs_ref):
-    for c_off, ref in enumerate((mine_ref, other_ref)):
-        for x_off in range(4):
-            block = (where_ref[2] + x_off) % 4 * 2 + (where_ref[3] + c_off) % 2
-            to = pl.multiple_of(block * COLS, COLS)
-            at = x_off * COLS
-            grad_ref[pl.ds(to, COLS), :] = ref[at : at + COLS, :TOKS]
-            inputs_ref[pl.ds(to, COLS), :] = ref[at : at + COLS, TOKS:]
+def arrange_body(where_ref, *rest):
+    refs, (grad_ref, inputs_ref) = rest[:10], rest[10:]
+    for c_off in range(2):
+        at = 0
+        for ref in refs[c_off * 5 : c_off * 5 + 5]:
+            rows = ref.shape[0]
+            block = (where_ref[2] + at // COLS) % 4 * 2 + (where_ref[3] + c_off) % 2
+            to = pl.multiple_of(block * COLS + at % COLS, ROWS)
+            grad_ref[pl.ds(to, rows), :] = ref[:, :TOKS]
+            inputs_ref[pl.ds(to, rows), :] = ref[:, TOKS:]
+            at += rows
+
+
+def join_body(*refs):
+    for k in range(2):
+        at = 0
+        for ref in refs[k * 5 : k * 5 + 5]:
+            rows = ref.shape[0]
+            refs[10 + k][at : at + rows, :] = ref[...]
+            at += rows
 
 
 def back_body(down_ref, grad_ref, gate_ref, value_ref, taps_ref, out_ref, sums_ref, act_ref):
@@ -181,16 +193,28 @@
     )(gate, value, taps)
 
 
-def arranged(where, mine, other):
+def arranged(where, *pieces):
     shape = jax.ShapeDtypeStruct((D, TOKS), BF16)
     return pl.pallas_call(
         arrange_body,
         out_shape=(shape, shape),
-        in_specs=[SMEM, VMEM, VMEM],
+        in_specs=[SMEM] + [VMEM] * 10,
         out_specs=(VMEM, VMEM),
         compiler_params=PARAMS,
         name="arrange",
-    )(where, mine, other)
+    )(where, *pieces)
+
+
+def joined(*pieces):
+    shape = jax.ShapeDtypeStruct((4 * HALF, 2 * UNITS), BF16)
+    return pl.pallas_call(
+        join_body,
+        out_shape=(shape, shape),
+        in_specs=[VMEM] * 10,
+        out_specs=(VMEM, VMEM),
+        compiler_params=PARAMS,
+        name="join",
+    )(*pieces)
 
 
 def back_of(down, grad, gate, value, taps):
@@ -252,9 +276,12 @@
 
 
 def over_features(where, own):
-    mine = jnp.concatenate(gathered(own, "x"), axis=0)
-    other = swapped(mine)
-    return arranged(where, mine, other)
+    mine = gathered(own, "x")
+    other = [None] * 5
+    for picks in ((0,), (1, 4), (2, 3)):
+        for k in picks:
+            other[k] = swapped(mine[k])
+    return arranged(where, *mine, *other)
 
 
 def layer(
@@ -273,8 +300,7 @@
     down = jnp.pad(down_weight.T, ((0, 0), (0, WIDE - UNITS)))
     down_full = lax.all_gather(down, FS, axis=0, tiled=True)
     weights = jnp.concatenate([gate_weight, value_weight], axis=1)
-    top = jnp.concatenate(gathered(weights[:HALF], "y"), axis=0)
-    low = jnp.concatenate(gathered(weights[HALF:], "z"), axis=0)
+    top, low = joined(*gathered(weights[:HALF], "y"), *gathered(weights[HALF:], "z"))
 
     normed = pre_norm.astype(F32)
     cot_float = cotangent.astype(F32)

time: 252 us -> 253 us (level)
  starting transfers between devices: 51.6 us -> 55.1 us
  local copies, waits for them, and re-layouts: 15.9 us -> 12.5 us
  waiting for transfers between devices: 111 us -> 108 us
    ppermute x2 -> x6, starting transfers between devices: 7.88 us -> 14 us  [swapped(): return lax.ppermute(value, 'c', [(0, 1), (1, 0)])]
    all_gather x1, waiting for transfers between devices: 0.01 us -> 4.75 us  [layer(): down_full = lax.all_gather(down, FS, axis=0, tiled=True)]
    ppermute x2 -> x6, waiting for transfers between devices: 7.57 us -> 3.26 us  [swapped(): return lax.ppermute(value, 'c', [(0, 1), (1, 0)])]
    unnamed x46 -> x37, local copies, waits for them, and re-layouts: 9.16 us -> 5.82 us
    ppermute x24, waiting for transfers between devices: 99 us -> 95.7 us  [moved(): return lax.ppermute(value, axis, [(i, (i + by) % 4) for i in range(4)])]
    ppermute x24, starting transfers between devices: 37.9 us -> 35.3 us  [moved(): return lax.ppermute(value, axis, [(i, (i + by) % 4) for i in range(4)])]
    pallas_call x1 -> x2, Pallas kernels: 4.89 us -> 6.65 us  [the longest x1 5.51 us: arranged(): pl.pallas_call(arrange_body, out_shape=(shape, shape), in_specs=[SMEM] +...]
  transfers between devices with their start and end apart: 29 -> 33, of which waited for: 13 -> 13; matrix products, arithmetic and copies ran while one was open for 5% -> 4% of each run, Pallas kernels for 7% -> 8%
where the time goes in v2:
time: 253 us; the launch traced here: 250 us
  waiting for transfers between devices  108 us (43%)
  starting transfers between devices  55.1 us (22%)
  Pallas kernels  42.6 us (17%)
  between operations  14.4 us (6%)
  local copies, waits for them, and re-layouts  12.5 us (5%)
  blocking collectives  11.7 us (5%)
  other arithmetic  5.79 us (2%)
    ppermute x24, waiting for transfers between devices, moved(): return lax.ppermute(value, axis, [(i, (i + by) % 4) for i in range(4)])  95.7 us
    ppermute x24, starting transfers between devices, moved(): return lax.ppermute(value, axis, [(i, (i + by) % 4) for i in range(4)])  35.3 us
    ppermute x6, starting transfers between devices, swapped(): return lax.ppermute(value, 'c', [(0, 1), (1, 0)])  14 us
    pallas_call x1, Pallas kernels, outer_of(): pl.pallas_call(outer_body, out_shape=jax.ShapeDtypeStruct((D, 3 * UNITS),...  13.2 us
    pallas_call x1, Pallas kernels, input_of(): pl.pallas_call(input_body, out_shape=(shape, shape), in_specs=[SMEM] + [V...  12.5 us
    all_to_all x1, blocking collectives, copy_for_each(): return lax.all_to_all(copies, axis, split_axis=0, concat_axis=0, tiled=True)  11.7 us
    pallas_call x1, Pallas kernels, back_of(): pl.pallas_call(back_body, out_shape=(jax.ShapeDtypeStruct((2 * UNITS, TOK...  9.3 us
    unnamed x37, local copies, waits for them, and re-layouts  5.82 us
  transfers between devices with their start and end apart: 33, of which 13 were waited for; matrix products, arithmetic and copies ran while one was open for 4% of the time, Pallas kernels for 8%

profile of v2, /device:TPU:1, one launch (start us, length us, event | category | flops | bytes accessed | tf_op | source)
XLA Modules:
  0.0 250.5 jit_solution(18257314833023595387)
XLA Ops:
  7.2 1.8 pad.4
  9.0 1.2 copy.33
  11.3 5.8 %all-to-all-start = ((f32[8,1,1024]{2,1,0:T(1,128)}), f32[8,1,1024]{2,1,0:T(1,128)S(1)}, u32[]{:S(2)}, u32[]{:S(2)}) async-start(f32[8,1,1024]{2,1,0:T(1,128)} %broadcast_in_dim.4), calls=%async_computation | async-start | bytes 65536 | tf_op jit(solution)/shard_map/all_to_all | solution.py:275
  17.3 4.5 %all-to-all-done = f32[8,1,1024]{2,1,0:T(1,128)S(1)} async-done(((f32[8,1,1024]{2,1,0:T(1,128)}), f32[8,1,1024]{2,1,0:T(1,128)S(1)}, u32[]{:S(2)}, u32[]{:S(2)}) %all-to-all-start) | async-done | bytes 32800 | tf_op jit(solution)/shard_map/all_to_all | solution.py:275
  22.7 2.4 collective-permute-start
  25.1 1.3 collective-permute-start.4
  26.4 15.6 %collective-permute-done.1.rest_4_ = bf16[384,1024]{1,0:T(8,128)(2,1)S(1)} collective-permute-done((bf16[384,1024]{1,0:T(8,128)(2,1)S(1)}, bf16[384,1024]{1,0:T(8,128)(2,1)S(1)}, u32[]{:S(2)}, u32[]{:S(2)}) %collective-permute-start.1) | collective-permute-done | bytes 786464 | tf_op jit(solution)/shard_map/ppermute | solution.py:30
  42.1 1.0 slice.111
  43.1 2.7 %collective-permute-start.3 = (bf16[192,1024]{1,0:T(8,128)(2,1)S(1)}, bf16[192,1024]{1,0:T(8,128)(2,1)}, u32[]{:S(2)}, u32[]{:S(2)}) collective-permute-start(bf16[192,1024]{1,0:T(8,128)(2,1)S(1)} %slice.111), channel_id=1, source_target_pairs={{0,6},{2,0},{4,2},{6,4},{1,7},{3,1},{5,3},{7,5},{8,14},{10,8},{12,... | collective-permute-start | bytes 1179656 | tf_op jit(solution)/shard_map/ppermute | solution.py:30
  45.9 2.2 collective-permute-start.5
  48.0 4.5 %collective-permute-done.2.rest_2_ = bf16[192,1024]{1,0:T(8,128)(2,1)} collective-permute-done((bf16[192,1024]{1,0:T(8,128)(2,1)S(1)}, bf16[192,1024]{1,0:T(8,128)(2,1)}, u32[]{:S(2)}, u32[]{:S(2)}) %collective-permute-start.2) | collective-permute-done | bytes 393248 | tf_op jit(solution)/shard_map/ppermute | solution.py:30
  52.5 2.4 collective-permute-start.6
  55.4 1.0 hidden.1.hidden_ref
  57.4 5.5 %arrange.1 = (bf16[3072,512]{1,0:T(8,128)(2,1)}, bf16[3072,512]{1,0:T(8,128)(2,1)}) custom-call(s32[4]{0:T(128)S(1)} %pad_add_fusion.where_ref, bf16[384,1024]{1,0:T(8,128)(2,1)S(1)} %pad_maximum_fusion.rest_0_, bf16[384,1024]{1,0:T(8,128)(2,1)} %collective-permute-done.rest_1_, bf16[192,1024]{1,0:T(8,128)(2,1)} %collective-permute-done.2.rest_2_, ...), custom_call_target="tpu_custom_call" | custom-call | tf_op jit(solution)/shard_map/arrange/pallas_call | solution.py:198
  62.9 4.8 %all-gather.2.cloned.1.call-done.down_ref = bf16[3072,768]{1,0:T(8,128)(2,1)} async-done(((bf16[192,768]{1,0:T(8,128)(2,1)}), bf16[3072,768]{1,0:T(8,128)(2,1)}) %all-gather.2.cloned.1.call-update) | async-done | bytes 4718608 | tf_op jit(solution)/shard_map/all_gather | solution.py:301
  67.7 9.3 %back.1 = (bf16[1408,512]{1,0:T(8,128)(2,1)S(1)}, f32[704,3]{1,0:T(8,128)S(1)}) custom-call(bf16[3072,768]{1,0:T(8,128)(2,1)} %all-gather.2.cloned.1.call-done.down_ref, bf16[3072,512]{1,0:T(8,128)(2,1)} %get-tuple-element.14.grad_ref, bf16[704,512]{1,0:T(8,128)(2,1)S(1)} %bitcast.20, bf16[704,512]{1,0:T(8,128)(2,1)S(1)} %bitcast.22, f32[704,3]{1,0:T(8,128)S(1)} %bitcast.18), custom_call_target="tpu_custom_call" | custom-call | flops 2214592512 | bytes 12000000 | tf_op jit(solution)/shard_map/back/pallas_call | solution.py:221
  77.0 13.2 %outer.1 = bf16[3072,2112]{1,0:T(8,128)(2,1)} custom-call(bf16[3072,512]{1,0:T(8,128)(2,1)} %get-tuple-element.20.inputs_ref, bf16[3072,512]{1,0:T(8,128)(2,1)} %get-tuple-element.14.grad_ref, bf16[1408,512]{1,0:T(8,128)(2,1)S(1)} %get-tuple-element.15.right_ref.both_ref, bf16[704,512]{1,0:T(8,128)(2,1)S(1)} %copy-done.3), custom_call_target="tpu_custom_call" | custom-call | flops 6643777536 | bytes 20000000 | tf_op jit(solution)/shard_map/outer/pallas_call | solution.py:239
  90.2 1.1 copy-done.4
  92.6 1.3 collective-permute-start.10
  93.8 1.5 collective-permute-start.9
  95.3 1.1 collective-permute-start.14
  96.4 1.6 collective-permute-start.13
  98.0 3.1 %collective-permute-done.10.refs_4_ = bf16[96,1408]{1,0:T(8,128)(2,1)S(1)} collective-permute-done((bf16[96,1408]{1,0:T(8,128)(2,1)S(1)}, bf16[96,1408]{1,0:T(8,128)(2,1)S(1)}, u32[]{:S(2)}, u32[]{:S(2)}) %collective-permute-start.10) | collective-permute-done | bytes 270368 | tf_op jit(solution)/shard_map/ppermute | solution.py:30
  101.2 2.7 %collective-permute-start.12 = (bf16[48,1408]{1,0:T(8,128)(2,1)S(1)}, bf16[48,1408]{1,0:T(8,128)(2,1)S(1)}, u32[]{:S(2)}, u32[]{:S(2)}) collective-permute-start(bf16[48,1408]{1,0:T(8,128)(2,1)S(1)} %slice.115), channel_id=1, source_target_pairs={{0,24},{8,0},{16,8},{24,16},{1,25},{9,1},{17,9},{25,17},{2,26},{10... | collective-permute-start | bytes 405512 | tf_op jit(solution)/shard_map/ppermute | solution.py:30
  103.9 1.1 collective-permute-start.15
  105.1 2.5 collective-permute-start.16
  107.5 2.6 %collective-permute-done.11.refs_2_ = bf16[48,1408]{1,0:T(8,128)(2,1)S(1)} collective-permute-done((bf16[48,1408]{1,0:T(8,128)(2,1)S(1)}, bf16[48,1408]{1,0:T(8,128)(2,1)S(1)}, u32[]{:S(2)}, u32[]{:S(2)}) %collective-permute-start.11) | collective-permute-done | bytes 135200 | tf_op jit(solution)/shard_map/ppermute | solution.py:30
  110.1 2.2 collective-permute-done.15.refs_7_
  113.0 1.1 join.1
  115.1 2.6 %collective-permute-start.17 = (bf16[384,1408]{1,0:T(8,128)(2,1)S(1)}, bf16[384,1408]{1,0:T(8,128)(2,1)S(1)}, u32[]{:S(2)}, u32[]{:S(2)}) collective-permute-start(bf16[384,1408]{1,0:T(8,128)(2,1)S(1)} %get-tuple-element.16.rest_0_), channel_id=1, source_target_pairs={{0,96},{32,0},{64,32},{96,64},{1,97},{33,1},{65,33},{97,65},{2,98}... | collective-permute-start | bytes 3244040 | tf_op jit(solution)/shard_map/ppermute | solution.py:30
  117.7 2.7 %collective-permute-start.21 = (bf16[384,1408]{1,0:T(8,128)(2,1)}, bf16[384,1408]{1,0:T(8,128)(2,1)S(1)}, u32[]{:S(2)}, u32[]{:S(2)}) collective-permute-start(bf16[384,1408]{1,0:T(8,128)(2,1)} %get-tuple-element.17.rest_5_), channel_id=1, source_target_pairs={{0,24},{8,0},{16,8},{24,16},{1,25},{9,1},{17,9},{25,17},{2,26},{10... | collective-permute-start | bytes 3244040 | tf_op jit(solution)/shard_map/ppermute | solution.py:30
  120.4 42.0 %collective-permute-done.18.rest_4_ = bf16[384,1408]{1,0:T(8,128)(2,1)S(1)} collective-permute-done((bf16[384,1408]{1,0:T(8,128)(2,1)S(1)}, bf16[384,1408]{1,0:T(8,128)(2,1)S(1)}, u32[]{:S(2)}, u32[]{:S(2)}) %collective-permute-start.18) | collective-permute-done | bytes 1081376 | tf_op jit(solution)/shard_map/ppermute | solution.py:30
  162.6 3.3 %collective-permute-start.20 = (bf16[192,1408]{1,0:T(8,128)(2,1)S(1)}, bf16[192,1408]{1,0:T(8,128)(2,1)S(1)}, u32[]{:S(2)}, u32[]{:S(2)}) collective-permute-start(bf16[192,1408]{1,0:T(8,128)(2,1)S(1)} %slice.119), channel_id=1, source_target_pairs={{0,96},{32,0},{64,32},{96,64},{1,97},{33,1},{65,33},{97,65},{2,98}... | collective-permute-start | bytes 1622024 | tf_op jit(solution)/shard_map/ppermute | solution.py:30
  166.2 2.7 %collective-permute-start.24 = (bf16[192,1408]{1,0:T(8,128)(2,1)S(1)}, bf16[192,1408]{1,0:T(8,128)(2,1)S(1)}, u32[]{:S(2)}, u32[]{:S(2)}) collective-permute-start(bf16[192,1408]{1,0:T(8,128)(2,1)S(1)} %slice.121), channel_id=1, source_target_pairs={{0,24},{8,0},{16,8},{24,16},{1,25},{9,1},{17,9},{25,17},{2,26},{10... | collective-permute-start | bytes 1622024 | tf_op jit(solution)/shard_map/ppermute | solution.py:30
  168.9 19.2 %collective-permute-done.19.rest_2_ = bf16[192,1408]{1,0:T(8,128)(2,1)S(1)} collective-permute-done((bf16[192,1408]{1,0:T(8,128)(2,1)S(1)}, bf16[192,1408]{1,0:T(8,128)(2,1)S(1)}, u32[]{:S(2)}, u32[]{:S(2)}) %collective-permute-start.19) | collective-permute-done | bytes 540704 | tf_op jit(solution)/shard_map/ppermute | solution.py:30
  188.1 1.1 collective-permute-done.23.rest_7_
  189.2 12.5 %grad_input.1 = (bf16[1536,512]{1,0:T(8,128)(2,1)}, bf16[1536,512]{1,0:T(8,128)(2,1)}) custom-call(s32[4]{0:T(128)S(1)} %pad_add_fusion.where_ref, bf16[1408,512]{1,0:T(8,128)(2,1)} %copy-done.4, bf16[384,1408]{1,0:T(8,128)(2,1)S(1)} %get-tuple-element.16.rest_0_, bf16[384,1408]{1,0:T(8,128)(2,1)} %copy-done.11, ...), custom_call_target="tpu_custom_call" | custom-call | flops 4429185024 | bytes 15000000 | tf_op jit(solution)/shard_map/grad_input/pallas_call | solution.py:260
  201.7 7.8 %collective-permute-start.25 = (bf16[1536,512]{1,0:T(8,128)(2,1)}, bf16[1536,512]{1,0:T(8,128)(2,1)S(1)}, u32[]{:S(2)}, u32[]{:S(2)}) collective-permute-start(bf16[1536,512]{1,0:T(8,128)(2,1)} %get-tuple-element.19), channel_id=1, source_target_pairs={{0,1},{1,0},{2,3},{3,2},{4,5},{5,4},{6,7},{7,6},{8,9},{9,8},{10,11... | collective-permute-start | bytes 4718600 | tf_op jit(solution)/shard_map/ppermute | solution.py:34
  209.5 3.2 %collective-permute-done.25 = bf16[1536,512]{1,0:T(8,128)(2,1)S(1)} collective-permute-done((bf16[1536,512]{1,0:T(8,128)(2,1)}, bf16[1536,512]{1,0:T(8,128)(2,1)S(1)}, u32[]{:S(2)}, u32[]{:S(2)}) %collective-permute-start.25) | collective-permute-done | bytes 1572896 | tf_op jit(solution)/shard_map/ppermute | solution.py:34
  212.7 1.9 add_convert_fusion
  214.7 1.3 collective-permute-start.26
  215.9 1.5 collective-permute-start.28
  217.4 4.7 %collective-permute-done.26 = bf16[192,512]{1,0:T(8,128)(2,1)S(1)} collective-permute-done((bf16[192,512]{1,0:T(8,128)(2,1)S(1)}, bf16[192,512]{1,0:T(8,128)(2,1)S(1)}, u32[]{:S(2)}, u32[]{:S(2)}) %collective-permute-start.26) | collective-permute-done | bytes 196640 | tf_op jit(solution)/shard_map/ppermute | solution.py:30
  223.3 1.9 collective-permute-start.29
  225.6 11.7 %all_to_all.12 = f32[16,1,2496]{2,1,0:T(1,128)S(1)} all-to-all(f32[16,1,2496]{2,1,0:T(1,128)S(1)} %broadcast_in_dim.5), channel_id=1, replica_groups=mesh['z'=4,'y'=4,'x'=4,'c'=2] {'z','y'}, dimensions={0} | all-to-all | bytes 319488 | tf_op jit(solution)/shard_map/all_to_all | solution.py:275
  238.7 1.3 fusion.7
  240.9 1.3 convert_element_type.73
  242.3 1.3 fusion.11
  (99 shorter events, 11.0 us)
Async XLA Ops:
  7.2 3.0 %copy-start.6 = (bf16[512,384]{1,0:T(8,128)(2,1)S(1)}, bf16[512,384]{1,0:T(8,128)(2,1)}, u32[]{:S(2)}) copy-start(bf16[512,384]{1,0:T(8,128)(2,1)} %param.11) | copy-start | bytes 1179652
  7.2 3.2 %copy-start.15 = (f32[384]{0:T(512)S(1)}, f32[384]{0:T(512)}, u32[]{:S(2)}) copy-start(f32[384]{0:T(512)} %param.19) | copy-start | bytes 4612
  7.2 60.5 %all-gather.2.cloned.1.call-start = ((), (), s32[]{:S(2)}) async-start(), calls=%async_computation.3 | async-start | bytes 5013504 | tf_op jit(solution)/shard_map/all_gather | solution.py:301
  7.2 9.8 %copy-start.7 = (bf16[512,384]{1,0:T(8,128)(2,1)S(1)}, bf16[512,384]{1,0:T(8,128)(2,1)}, u32[]{:S(2)}) copy-start(bf16[512,384]{1,0:T(8,128)(2,1)} %param.10) | copy-start | bytes 1179652
  11.3 10.5 %all-to-all-start = ((f32[8,1,1024]{2,1,0:T(1,128)}), f32[8,1,1024]{2,1,0:T(1,128)S(1)}, u32[]{:S(2)}, u32[]{:S(2)}) async-start(f32[8,1,1024]{2,1,0:T(1,128)} %broadcast_in_dim.4), calls=%async_computation | async-start | bytes 65536 | tf_op jit(solution)/shard_map/all_to_all | solution.py:275
  17.1 223.8 %reduce-scatter.2.cloned.1.call-start = ((), (), s32[]{:S(2)}) async-start(), calls=%async_computation.4 | async-start | bytes 14204928 | tf_op jit(solution)/shard_map/reduce_scatter | solution.py:326
  22.2 33.0 %copy-start.14 = (f32[3,704]{1,0:T(4,128)S(1)}, f32[3,704]{1,0:T(4,128)}, u32[]{:S(2)}) copy-start(f32[3,704]{1,0:T(4,128)} %param.18) | copy-start | bytes 25348
  22.2 33.2 %copy-start = (bf16[512,704]{0,1:T(8,128)(2,1)S(1)}, bf16[512,704]{0,1:T(8,128)(2,1)}, u32[]{:S(2)}) copy-start(bf16[512,704]{0,1:T(8,128)(2,1)} %param.13) | copy-start | bytes 2162692
  22.2 33.2 %copy-start.1 = (bf16[512,704]{0,1:T(8,128)(2,1)S(1)}, bf16[512,704]{0,1:T(8,128)(2,1)}, u32[]{:S(2)}) copy-start(bf16[512,704]{0,1:T(8,128)(2,1)} %param.14) | copy-start | bytes 2162692
  22.4 19.6 %collective-permute-start.1 = (bf16[384,1024]{1,0:T(8,128)(2,1)S(1)}, bf16[384,1024]{1,0:T(8,128)(2,1)S(1)}, u32[]{:S(2)}, u32[]{:S(2)}) collective-permute-start(bf16[384,1024]{1,0:T(8,128)(2,1)S(1)} %pad_maximum_fusion.rest_0_), channel_id=1, source_target_pairs={{0,2},{2,4},{4,6},{6,0},{1,3},{3,5},{5,7},{7,1},{8,10},{10,12},{12... | collective-permute-start | bytes 2359304 | tf_op jit(solution)/shard_map/ppermute | solution.py:30
  22.7 19.4 %collective-permute-start = (bf16[384,1024]{1,0:T(8,128)(2,1)S(1)}, bf16[384,1024]{1,0:T(8,128)(2,1)}, u32[]{:S(2)}, u32[]{:S(2)}) collective-permute-start(bf16[384,1024]{1,0:T(8,128)(2,1)S(1)} %pad_maximum_fusion.rest_0_), channel_id=1, source_target_pairs={{0,6},{2,0},{4,2},{6,4},{1,7},{3,1},{5,3},{7,5},{8,14},{10,8},{12,... | collective-permute-start | bytes 2359304 | tf_op jit(solution)/shard_map/ppermute | solution.py:30
  25.1 32.3 %collective-permute-start.4 = (bf16[384,1024]{1,0:T(8,128)(2,1)S(1)}, bf16[384,1024]{1,0:T(8,128)(2,1)}, u32[]{:S(2)}, u32[]{:S(2)}) collective-permute-start(bf16[384,1024]{1,0:T(8,128)(2,1)S(1)} %pad_maximum_fusion.rest_0_), channel_id=1, source_target_pairs={{0,1},{1,0},{2,3},{3,2},{4,5},{5,4},{6,7},{7,6},{8,9},{9,8},{10,11... | collective-permute-start | bytes 2359304 | tf_op jit(solution)/shard_map/ppermute | solution.py:34
  42.0 10.5 %collective-permute-start.2 = (bf16[192,1024]{1,0:T(8,128)(2,1)S(1)}, bf16[192,1024]{1,0:T(8,128)(2,1)}, u32[]{:S(2)}, u32[]{:S(2)}) collective-permute-start(bf16[192,1024]{1,0:T(8,128)(2,1)S(1)} %slice.110), channel_id=1, source_target_pairs={{0,2},{2,4},{4,6},{6,0},{1,3},{3,5},{5,7},{7,1},{8,10},{10,12},{12... | collective-permute-start | bytes 1179656 | tf_op jit(solution)/shard_map/ppermute | solution.py:30
  43.1 11.8 %collective-permute-start.3 = (bf16[192,1024]{1,0:T(8,128)(2,1)S(1)}, bf16[192,1024]{1,0:T(8,128)(2,1)}, u32[]{:S(2)}, u32[]{:S(2)}) collective-permute-start(bf16[192,1024]{1,0:T(8,128)(2,1)S(1)} %slice.111), channel_id=1, source_target_pairs={{0,6},{2,0},{4,2},{6,4},{1,7},{3,1},{5,3},{7,5},{8,14},{10,8},{12,... | collective-permute-start | bytes 1179656 | tf_op jit(solution)/shard_map/ppermute | solution.py:30
  45.9 11.5 %collective-permute-start.5 = (bf16[384,1024]{1,0:T(8,128)(2,1)}, bf16[384,1024]{1,0:T(8,128)(2,1)}, u32[]{:S(2)}, u32[]{:S(2)}) collective-permute-start(bf16[384,1024]{1,0:T(8,128)(2,1)} %collective-permute-done.rest_1_), channel_id=1, source_target_pairs={{0,1},{1,0},{2,3},{3,2},{4,5},{5,4},{6,7},{7,6},{8,9},{9,8},{10,11... | collective-permute-start | bytes 2359304 | tf_op jit(solution)/shard_map/ppermute | solution.py:34
  48.0 9.4 %collective-permute-start.8 = (bf16[384,1024]{1,0:T(8,128)(2,1)S(1)}, bf16[384,1024]{1,0:T(8,128)(2,1)}, u32[]{:S(2)}, u32[]{:S(2)}) collective-permute-start(bf16[384,1024]{1,0:T(8,128)(2,1)S(1)} %collective-permute-done.1.rest_4_), channel_id=1, source_target_pairs={{0,1},{1,0},{2,3},{3,2},{4,5},{5,4},{6,7},{7,6},{8,9},{9,8},{10,11... | collective-permute-start | bytes 2359304 | tf_op jit(solution)/shard_map/ppermute | solution.py:34
  52.5 4.9 %collective-permute-start.6 = (bf16[192,1024]{1,0:T(8,128)(2,1)}, bf16[192,1024]{1,0:T(8,128)(2,1)}, u32[]{:S(2)}, u32[]{:S(2)}) collective-permute-start(bf16[192,1024]{1,0:T(8,128)(2,1)} %collective-permute-done.2.rest_2_), channel_id=1, source_target_pairs={{0,1},{1,0},{2,3},{3,2},{4,5},{5,4},{6,7},{7,6},{8,9},{9,8},{10,11... | collective-permute-start | bytes 1179656 | tf_op jit(solution)/shard_map/ppermute | solution.py:34
  54.9 2.5 collective-permute-start.7
  67.7 9.3 %copy-start.3 = (bf16[704,512]{1,0:T(8,128)(2,1)S(1)}, bf16[704,512]{1,0:T(8,128)(2,1)}, u32[]{:S(2)}) copy-start(bf16[704,512]{1,0:T(8,128)(2,1)} %copy-done.2) | copy-start | bytes 2162692
  90.2 1.1 copy-start.4
  91.4 1.0 copy-start.8
  91.4 1.0 copy-start.9
  92.6 8.5 %collective-permute-start.10 = (bf16[96,1408]{1,0:T(8,128)(2,1)S(1)}, bf16[96,1408]{1,0:T(8,128)(2,1)S(1)}, u32[]{:S(2)}, u32[]{:S(2)}) collective-permute-start(bf16[96,1408]{1,0:T(8,128)(2,1)S(1)} %get-tuple-element.59.refs_0_), channel_id=1, source_target_pairs={{0,8},{8,16},{16,24},{24,0},{1,9},{9,17},{17,25},{25,1},{2,10},{10... | collective-permute-start | bytes 811016 | tf_op jit(solution)/shard_map/ppermute | solution.py:30
  93.8 7.3 %collective-permute-start.9 = (bf16[96,1408]{1,0:T(8,128)(2,1)S(1)}, bf16[96,1408]{1,0:T(8,128)(2,1)S(1)}, u32[]{:S(2)}, u32[]{:S(2)}) collective-permute-start(bf16[96,1408]{1,0:T(8,128)(2,1)S(1)} %get-tuple-element.59.refs_0_), channel_id=1, source_target_pairs={{0,24},{8,0},{16,8},{24,16},{1,25},{9,1},{17,9},{25,17},{2,26},{10... | collective-permute-start | bytes 811016 | tf_op jit(solution)/shard_map/ppermute | solution.py:30
  95.3 8.6 %collective-permute-start.14 = (bf16[96,1408]{1,0:T(8,128)(2,1)S(1)}, bf16[96,1408]{1,0:T(8,128)(2,1)S(1)}, u32[]{:S(2)}, u32[]{:S(2)}) collective-permute-start(bf16[96,1408]{1,0:T(8,128)(2,1)S(1)} %get-tuple-element.58.refs_5_), channel_id=1, source_target_pairs={{0,32},{32,64},{64,96},{96,0},{1,33},{33,65},{65,97},{97,1},{2,34}... | collective-permute-start | bytes 811016 | tf_op jit(solution)/shard_map/ppermute | solution.py:30
  96.4 8.7 %collective-permute-start.13 = (bf16[96,1408]{1,0:T(8,128)(2,1)S(1)}, bf16[96,1408]{1,0:T(8,128)(2,1)S(1)}, u32[]{:S(2)}, u32[]{:S(2)}) collective-permute-start(bf16[96,1408]{1,0:T(8,128)(2,1)S(1)} %get-tuple-element.58.refs_5_), channel_id=1, source_target_pairs={{0,96},{32,0},{64,32},{96,64},{1,97},{33,1},{65,33},{97,65},{2,98}... | collective-permute-start | bytes 811016 | tf_op jit(solution)/shard_map/ppermute | solution.py:30
  101.1 9.1 %collective-permute-start.11 = (bf16[48,1408]{1,0:T(8,128)(2,1)S(1)}, bf16[48,1408]{1,0:T(8,128)(2,1)S(1)}, u32[]{:S(2)}, u32[]{:S(2)}) collective-permute-start(bf16[48,1408]{1,0:T(8,128)(2,1)S(1)} %slice.114), channel_id=1, source_target_pairs={{0,8},{8,16},{16,24},{24,0},{1,9},{9,17},{17,25},{25,1},{2,10},{10... | collective-permute-start | bytes 405512 | tf_op jit(solution)/shard_map/ppermute | solution.py:30
  101.2 9.0 %collective-permute-start.12 = (bf16[48,1408]{1,0:T(8,128)(2,1)S(1)}, bf16[48,1408]{1,0:T(8,128)(2,1)S(1)}, u32[]{:S(2)}, u32[]{:S(2)}) collective-permute-start(bf16[48,1408]{1,0:T(8,128)(2,1)S(1)} %slice.115), channel_id=1, source_target_pairs={{0,24},{8,0},{16,8},{24,16},{1,25},{9,1},{17,9},{25,17},{2,26},{10... | collective-permute-start | bytes 405512 | tf_op jit(solution)/shard_map/ppermute | solution.py:30
  103.9 8.4 %collective-permute-start.15 = (bf16[48,1408]{1,0:T(8,128)(2,1)S(1)}, bf16[48,1408]{1,0:T(8,128)(2,1)S(1)}, u32[]{:S(2)}, u32[]{:S(2)}) collective-permute-start(bf16[48,1408]{1,0:T(8,128)(2,1)S(1)} %slice.116), channel_id=1, source_target_pairs={{0,32},{32,64},{64,96},{96,0},{1,33},{33,65},{65,97},{97,1},{2,34}... | collective-permute-start | bytes 405512 | tf_op jit(solution)/shard_map/ppermute | solution.py:30
  105.1 7.9 %collective-permute-start.16 = (bf16[48,1408]{1,0:T(8,128)(2,1)S(1)}, bf16[48,1408]{1,0:T(8,128)(2,1)S(1)}, u32[]{:S(2)}, u32[]{:S(2)}) collective-permute-start(bf16[48,1408]{1,0:T(8,128)(2,1)S(1)} %slice.117), channel_id=1, source_target_pairs={{0,96},{32,0},{64,32},{96,64},{1,97},{33,1},{65,33},{97,65},{2,98}... | collective-permute-start | bytes 405512 | tf_op jit(solution)/shard_map/ppermute | solution.py:30
  114.2 48.2 %collective-permute-start.18 = (bf16[384,1408]{1,0:T(8,128)(2,1)S(1)}, bf16[384,1408]{1,0:T(8,128)(2,1)S(1)}, u32[]{:S(2)}, u32[]{:S(2)}) collective-permute-start(bf16[384,1408]{1,0:T(8,128)(2,1)S(1)} %get-tuple-element.16.rest_0_), channel_id=1, source_target_pairs={{0,32},{32,64},{64,96},{96,0},{1,33},{33,65},{65,97},{97,1},{2,34}... | collective-permute-start | bytes 3244040 | tf_op jit(solution)/shard_map/ppermute | solution.py:30
  115.1 47.4 %collective-permute-start.17 = (bf16[384,1408]{1,0:T(8,128)(2,1)S(1)}, bf16[384,1408]{1,0:T(8,128)(2,1)S(1)}, u32[]{:S(2)}, u32[]{:S(2)}) collective-permute-start(bf16[384,1408]{1,0:T(8,128)(2,1)S(1)} %get-tuple-element.16.rest_0_), channel_id=1, source_target_pairs={{0,96},{32,0},{64,32},{96,64},{1,97},{33,1},{65,33},{97,65},{2,98}... | collective-permute-start | bytes 3244040 | tf_op jit(solution)/shard_map/ppermute | solution.py:30
  117.7 48.2 %collective-permute-start.22 = (bf16[384,1408]{1,0:T(8,128)(2,1)}, bf16[384,1408]{1,0:T(8,128)(2,1)S(1)}, u32[]{:S(2)}, u32[]{:S(2)}) collective-permute-start(bf16[384,1408]{1,0:T(8,128)(2,1)} %get-tuple-element.17.rest_5_), channel_id=1, source_target_pairs={{0,8},{8,16},{16,24},{24,0},{1,9},{9,17},{17,25},{25,1},{2,10},{10... | collective-permute-start | bytes 3244040 | tf_op jit(solution)/shard_map/ppermute | solution.py:30
  117.7 48.4 %collective-permute-start.21 = (bf16[384,1408]{1,0:T(8,128)(2,1)}, bf16[384,1408]{1,0:T(8,128)(2,1)S(1)}, u32[]{:S(2)}, u32[]{:S(2)}) collective-permute-start(bf16[384,1408]{1,0:T(8,128)(2,1)} %get-tuple-element.17.rest_5_), channel_id=1, source_target_pairs={{0,24},{8,0},{16,8},{24,16},{1,25},{9,1},{17,9},{25,17},{2,26},{10... | collective-permute-start | bytes 3244040 | tf_op jit(solution)/shard_map/ppermute | solution.py:30
  162.4 3.6 %copy-start.10 = (bf16[384,1408]{1,0:T(8,128)(2,1)}, bf16[384,1408]{1,0:T(8,128)(2,1)S(1)}, u32[]{:S(2)}) copy-start(bf16[384,1408]{1,0:T(8,128)(2,1)S(1)} %collective-permute-done.18.rest_4_) | copy-start | bytes 3244036
  162.4 25.6 %collective-permute-start.19 = (bf16[192,1408]{1,0:T(8,128)(2,1)S(1)}, bf16[192,1408]{1,0:T(8,128)(2,1)S(1)}, u32[]{:S(2)}, u32[]{:S(2)}) collective-permute-start(bf16[192,1408]{1,0:T(8,128)(2,1)S(1)} %slice.118), channel_id=1, source_target_pairs={{0,32},{32,64},{64,96},{96,0},{1,33},{33,65},{65,97},{97,1},{2,34}... | collective-permute-start | bytes 1622024 | tf_op jit(solution)/shard_map/ppermute | solution.py:30
  162.5 3.6 %copy-start.11 = (bf16[384,1408]{1,0:T(8,128)(2,1)}, bf16[384,1408]{1,0:T(8,128)(2,1)S(1)}, u32[]{:S(2)}) copy-start(bf16[384,1408]{1,0:T(8,128)(2,1)S(1)} %collective-permute-done.17.rest_1_) | copy-start | bytes 3244036
  162.6 25.5 %collective-permute-start.20 = (bf16[192,1408]{1,0:T(8,128)(2,1)S(1)}, bf16[192,1408]{1,0:T(8,128)(2,1)S(1)}, u32[]{:S(2)}, u32[]{:S(2)}) collective-permute-start(bf16[192,1408]{1,0:T(8,128)(2,1)S(1)} %slice.119), channel_id=1, source_target_pairs={{0,96},{32,0},{64,32},{96,64},{1,97},{33,1},{65,33},{97,65},{2,98}... | collective-permute-start | bytes 1622024 | tf_op jit(solution)/shard_map/ppermute | solution.py:30
  165.9 23.2 %copy-start.12 = (bf16[384,1408]{1,0:T(8,128)(2,1)}, bf16[384,1408]{1,0:T(8,128)(2,1)S(1)}, u32[]{:S(2)}) copy-start(bf16[384,1408]{1,0:T(8,128)(2,1)S(1)} %collective-permute-done.22.rest_9_) | copy-start | bytes 3244036
  166.0 23.2 %collective-permute-start.23 = (bf16[192,1408]{1,0:T(8,128)(2,1)S(1)}, bf16[192,1408]{1,0:T(8,128)(2,1)S(1)}, u32[]{:S(2)}, u32[]{:S(2)}) collective-permute-start(bf16[192,1408]{1,0:T(8,128)(2,1)S(1)} %slice.120), channel_id=1, source_target_pairs={{0,8},{8,16},{16,24},{24,0},{1,9},{9,17},{17,25},{25,1},{2,10},{10... | collective-permute-start | bytes 1622024 | tf_op jit(solution)/shard_map/ppermute | solution.py:30
  166.1 23.1 %copy-start.13 = (bf16[384,1408]{1,0:T(8,128)(2,1)}, bf16[384,1408]{1,0:T(8,128)(2,1)S(1)}, u32[]{:S(2)}) copy-start(bf16[384,1408]{1,0:T(8,128)(2,1)S(1)} %collective-permute-done.21.rest_6_) | copy-start | bytes 3244036
  166.2 23.0 %collective-permute-start.24 = (bf16[192,1408]{1,0:T(8,128)(2,1)S(1)}, bf16[192,1408]{1,0:T(8,128)(2,1)S(1)}, u32[]{:S(2)}, u32[]{:S(2)}) collective-permute-start(bf16[192,1408]{1,0:T(8,128)(2,1)S(1)} %slice.121), channel_id=1, source_target_pairs={{0,24},{8,0},{16,8},{24,16},{1,25},{9,1},{17,9},{25,17},{2,26},{10... | collective-permute-start | bytes 1622024 | tf_op jit(solution)/shard_map/ppermute | solution.py:30
  201.7 11.1 %collective-permute-start.25 = (bf16[1536,512]{1,0:T(8,128)(2,1)}, bf16[1536,512]{1,0:T(8,128)(2,1)S(1)}, u32[]{:S(2)}, u32[]{:S(2)}) collective-permute-start(bf16[1536,512]{1,0:T(8,128)(2,1)} %get-tuple-element.19), channel_id=1, source_target_pairs={{0,1},{1,0},{2,3},{3,2},{4,5},{5,4},{6,7},{7,6},{8,9},{9,8},{10,11... | collective-permute-start | bytes 4718600 | tf_op jit(solution)/shard_map/ppermute | solution.py:34
  214.7 7.5 %collective-permute-start.26 = (bf16[192,512]{1,0:T(8,128)(2,1)S(1)}, bf16[192,512]{1,0:T(8,128)(2,1)S(1)}, u32[]{:S(2)}, u32[]{:S(2)}) collective-permute-start(bf16[192,512]{1,0:T(8,128)(2,1)S(1)} %get-tuple-element.50), channel_id=1, source_target_pairs={{0,2},{2,4},{4,6},{6,0},{1,3},{3,5},{5,7},{7,1},{8,10},{10,12},{12... | collective-permute-start | bytes 589832 | tf_op jit(solution)/shard_map/ppermute | solution.py:30
  215.9 6.2 %collective-permute-start.28 = (bf16[192,512]{1,0:T(8,128)(2,1)S(1)}, bf16[192,512]{1,0:T(8,128)(2,1)S(1)}, u32[]{:S(2)}, u32[]{:S(2)}) collective-permute-start(bf16[192,512]{1,0:T(8,128)(2,1)S(1)} %get-tuple-element.51), channel_id=1, source_target_pairs={{0,6},{2,0},{4,2},{6,4},{1,7},{3,1},{5,3},{7,5},{8,14},{10,8},{12,... | collective-permute-start | bytes 589832 | tf_op jit(solution)/shard_map/ppermute | solution.py:30
  222.3 16.4 %collective-permute-start.27 = (bf16[384,512]{1,0:T(8,128)(2,1)S(1)}, bf16[384,512]{1,0:T(8,128)(2,1)}, u32[]{:S(2)}, u32[]{:S(2)}) collective-permute-start(bf16[384,512]{1,0:T(8,128)(2,1)S(1)} %pad_maximum_fusion.1), channel_id=1, source_target_pairs={{0,2},{2,4},{4,6},{6,0},{1,3},{3,5},{5,7},{7,1},{8,10},{10,12},{12... | collective-permute-start | bytes 1179656 | tf_op jit(solution)/shard_map/ppermute | solution.py:30
  223.3 15.4 %collective-permute-start.29 = (bf16[384,512]{1,0:T(8,128)(2,1)S(1)}, bf16[384,512]{1,0:T(8,128)(2,1)}, u32[]{:S(2)}, u32[]{:S(2)}) collective-permute-start(bf16[384,512]{1,0:T(8,128)(2,1)S(1)} %pad_maximum_fusion.2), channel_id=1, source_target_pairs={{0,6},{2,0},{4,2},{6,4},{1,7},{3,1},{5,3},{7,5},{8,14},{10,8},{12,... | collective-permute-start | bytes 1179656 | tf_op jit(solution)/shard_map/ppermute | solution.py:30
  240.9 1.4 copy-start.5
  (1 other events, 0.9 us)
Sparse Core Ops, SparseCore 0:
  10.7 56.9 all-gather.1
  91.5 132.4 reduce-scatter.1

commit v3 on v2

--- a/solution.py
+++ b/solution.py
@@ -73,6 +73,7 @@
 
 
 STEP = 88
+BACK_STEPS = 4
 
 
 def hidden_body(gate_ref, value_ref, taps_ref, hidden_ref):
@@ -108,12 +109,28 @@
 
 
 def back_body(down_ref, grad_ref, gate_ref, value_ref, taps_ref, out_ref, sums_ref, act_ref):
-    act_ref[...] = lax.dot_general(
+    step = pl.program_id(0)
+    part = lax.dot_general(
         down_ref[:, :UNITS],
         grad_ref[...],
         (((0,), (0,)), ((), ())),
         preferred_element_type=F32,
     )
+
+    @pl.when(step == 0)
+    def _():
+        act_ref[...] = part
+
+    @pl.when(step > 0)
+    def _():
+        act_ref[...] += part
+
+    @pl.when(step == BACK_STEPS - 1)
+    def _():
+        finish_back(gate_ref, value_ref, taps_ref, out_ref, sums_ref, act_ref)
+
+
+def finish_back(gate_ref, value_ref, taps_ref, out_ref, sums_ref, act_ref):
     for u in range(0, UNITS, STEP):
         rows = slice(u, u + STEP)
         taps = taps_ref[rows, :]
@@ -218,13 +235,21 @@
 
 
 def back_of(down, grad, gate, value, taps):
+    rows = D // BACK_STEPS
     return pl.pallas_call(
         back_body,
         out_shape=(
             jax.ShapeDtypeStruct((2 * UNITS, TOKS), BF16),
             jax.ShapeDtypeStruct((UNITS, 3), F32),
         ),
-        in_specs=[VMEM] * 5,
+        grid=(BACK_STEPS,),
+        in_specs=[
+            pl.BlockSpec((rows, WIDE), lambda i: (i, 0)),
+            pl.BlockSpec((rows, TOKS), lambda i: (i, 0)),
+            VMEM,
+            VMEM,
+            VMEM,
+        ],
         out_specs=(VMEM, VMEM),
         scratch_shapes=[pltpu.VMEM((UNITS, TOKS), F32)],
         compiler_params=PARAMS,

time: 253 us -> 254 us (level)
  no operation moved by 1% of the time
where the time goes in v3:
time: 254 us; the launch traced here: 251 us
  waiting for transfers between devices  108 us (43%)
  starting transfers between devices  55 us (22%)
  Pallas kernels  43.5 us (17%)
  between operations  14.4 us (6%)
  local copies, waits for them, and re-layouts  12.5 us (5%)
  blocking collectives  11.7 us (5%)
  other arithmetic  5.79 us (2%)
    ppermute x24, waiting for transfers between devices, moved(): return lax.ppermute(value, axis, [(i, (i + by) % 4) for i in range(4)])  95.8 us
    ppermute x24, starting transfers between devices, moved(): return lax.ppermute(value, axis, [(i, (i + by) % 4) for i in range(4)])  35.4 us
    ppermute x6, starting transfers between devices, swapped(): return lax.ppermute(value, 'c', [(0, 1), (1, 0)])  13.8 us
    pallas_call x1, Pallas kernels, outer_of(): pl.pallas_call(outer_body, out_shape=jax.ShapeDtypeStruct((D, 3 * UNITS),...  13.2 us
    pallas_call x1, Pallas kernels, input_of(): pl.pallas_call(input_body, out_shape=(shape, shape), in_specs=[SMEM] + [V...  12.5 us
    all_to_all x1, blocking collectives, copy_for_each(): return lax.all_to_all(copies, axis, split_axis=0, concat_axis=0, tiled=True)  11.7 us
    pallas_call x1, Pallas kernels, back_of(): pl.pallas_call(back_body, out_shape=(jax.ShapeDtypeStruct((2 * UNITS, TOK...  10.2 us
    unnamed x37, local copies, waits for them, and re-layouts  5.82 us
  transfers between devices with their start and end apart: 33, of which 13 were waited for; matrix products, arithmetic and copies ran while one was open for 4% of the time, Pallas kernels for 8%

profile of v3, /device:TPU:1, one launch (start us, length us, event | category | flops | bytes accessed | tf_op | source)
XLA Modules:
  0.0 251.4 jit_solution(7832838339866686695)
XLA Ops:
  7.2 1.8 pad.4
  9.0 1.2 copy.33
  11.3 5.8 %all-to-all-start = ((f32[8,1,1024]{2,1,0:T(1,128)}), f32[8,1,1024]{2,1,0:T(1,128)S(1)}, u32[]{:S(2)}, u32[]{:S(2)}) async-start(f32[8,1,1024]{2,1,0:T(1,128)} %broadcast_in_dim.4), calls=%async_computation | async-start | bytes 65536 | tf_op jit(solution)/shard_map/all_to_all | solution.py:300
  17.3 4.5 %all-to-all-done = f32[8,1,1024]{2,1,0:T(1,128)S(1)} async-done(((f32[8,1,1024]{2,1,0:T(1,128)}), f32[8,1,1024]{2,1,0:T(1,128)S(1)}, u32[]{:S(2)}, u32[]{:S(2)}) %all-to-all-start) | async-done | bytes 32800 | tf_op jit(solution)/shard_map/all_to_all | solution.py:300
  22.7 2.4 collective-permute-start
  25.1 1.3 collective-permute-start.4
  26.4 15.6 %collective-permute-done.1.rest_4_ = bf16[384,1024]{1,0:T(8,128)(2,1)S(1)} collective-permute-done((bf16[384,1024]{1,0:T(8,128)(2,1)S(1)}, bf16[384,1024]{1,0:T(8,128)(2,1)S(1)}, u32[]{:S(2)}, u32[]{:S(2)}) %collective-permute-start.1) | collective-permute-done | bytes 786464 | tf_op jit(solution)/shard_map/ppermute | solution.py:30
  42.1 1.0 slice.111
  43.1 2.7 %collective-permute-start.3 = (bf16[192,1024]{1,0:T(8,128)(2,1)S(1)}, bf16[192,1024]{1,0:T(8,128)(2,1)}, u32[]{:S(2)}, u32[]{:S(2)}) collective-permute-start(bf16[192,1024]{1,0:T(8,128)(2,1)S(1)} %slice.111), channel_id=1, source_target_pairs={{0,6},{2,0},{4,2},{6,4},{1,7},{3,1},{5,3},{7,5},{8,14},{10,8},{12,... | collective-permute-start | bytes 1179656 | tf_op jit(solution)/shard_map/ppermute | solution.py:30
  45.9 2.2 collective-permute-start.5
  48.0 4.5 %collective-permute-done.2.rest_2_ = bf16[192,1024]{1,0:T(8,128)(2,1)} collective-permute-done((bf16[192,1024]{1,0:T(8,128)(2,1)S(1)}, bf16[192,1024]{1,0:T(8,128)(2,1)}, u32[]{:S(2)}, u32[]{:S(2)}) %collective-permute-start.2) | collective-permute-done | bytes 393248 | tf_op jit(solution)/shard_map/ppermute | solution.py:30
  52.5 2.4 collective-permute-start.6
  57.4 5.5 %arrange.1 = (bf16[3072,512]{1,0:T(8,128)(2,1)}, bf16[3072,512]{1,0:T(8,128)(2,1)}) custom-call(s32[4]{0:T(128)S(1)} %pad_add_fusion.where_ref, bf16[384,1024]{1,0:T(8,128)(2,1)S(1)} %pad_maximum_fusion.rest_0_, bf16[384,1024]{1,0:T(8,128)(2,1)} %collective-permute-done.rest_1_, bf16[192,1024]{1,0:T(8,128)(2,1)} %collective-permute-done.2.rest_2_, ...), custom_call_target="tpu_custom_call" | custom-call | tf_op jit(solution)/shard_map/arrange/pallas_call | solution.py:215
  62.9 4.8 %all-gather.2.cloned.1.call-done.down_ref = bf16[3072,768]{1,0:T(8,128)(2,1)} async-done(((bf16[192,768]{1,0:T(8,128)(2,1)}), bf16[3072,768]{1,0:T(8,128)(2,1)}) %all-gather.2.cloned.1.call-update) | async-done | bytes 4718608 | tf_op jit(solution)/shard_map/all_gather | solution.py:326
  67.7 10.2 %back.1 = (bf16[1408,512]{1,0:T(8,128)(2,1)S(1)}, f32[704,3]{1,0:T(8,128)S(1)}) custom-call(bf16[3072,768]{1,0:T(8,128)(2,1)} %all-gather.2.cloned.1.call-done.down_ref, bf16[3072,512]{1,0:T(8,128)(2,1)} %get-tuple-element.14.grad_ref, bf16[704,512]{1,0:T(8,128)(2,1)S(1)} %bitcast.20, bf16[704,512]{1,0:T(8,128)(2,1)S(1)} %bitcast.22, f32[704,3]{1,0:T(8,128)S(1)} %bitcast.18), custom_call_target="tpu_custom_call" | custom-call | flops 2214592512 | bytes 12000000 | tf_op jit(solution)/shard_map/back/pallas_call | solution.py:239
  77.9 13.2 %outer.1 = bf16[3072,2112]{1,0:T(8,128)(2,1)} custom-call(bf16[3072,512]{1,0:T(8,128)(2,1)} %get-tuple-element.20.inputs_ref, bf16[3072,512]{1,0:T(8,128)(2,1)} %get-tuple-element.14.grad_ref, bf16[1408,512]{1,0:T(8,128)(2,1)S(1)} %get-tuple-element.15.right_ref.both_ref, bf16[704,512]{1,0:T(8,128)(2,1)S(1)} %copy-done.3), custom_call_target="tpu_custom_call" | custom-call | flops 6643777536 | bytes 20000000 | tf_op jit(solution)/shard_map/outer/pallas_call | solution.py:264
  91.1 1.1 copy-done.4
  93.5 1.2 collective-permute-start.10
  94.7 1.5 collective-permute-start.9
  96.2 1.1 collective-permute-start.14
  97.3 1.6 collective-permute-start.13
  98.9 3.1 %collective-permute-done.10.refs_4_ = bf16[96,1408]{1,0:T(8,128)(2,1)S(1)} collective-permute-done((bf16[96,1408]{1,0:T(8,128)(2,1)S(1)}, bf16[96,1408]{1,0:T(8,128)(2,1)S(1)}, u32[]{:S(2)}, u32[]{:S(2)}) %collective-permute-start.10) | collective-permute-done | bytes 270368 | tf_op jit(solution)/shard_map/ppermute | solution.py:30
  102.1 2.7 %collective-permute-start.12 = (bf16[48,1408]{1,0:T(8,128)(2,1)S(1)}, bf16[48,1408]{1,0:T(8,128)(2,1)S(1)}, u32[]{:S(2)}, u32[]{:S(2)}) collective-permute-start(bf16[48,1408]{1,0:T(8,128)(2,1)S(1)} %slice.115), channel_id=1, source_target_pairs={{0,24},{8,0},{16,8},{24,16},{1,25},{9,1},{17,9},{25,17},{2,26},{10... | collective-permute-start | bytes 405512 | tf_op jit(solution)/shard_map/ppermute | solution.py:30
  104.8 1.1 collective-permute-start.15
  105.9 2.6 %collective-permute-start.16 = (bf16[48,1408]{1,0:T(8,128)(2,1)S(1)}, bf16[48,1408]{1,0:T(8,128)(2,1)S(1)}, u32[]{:S(2)}, u32[]{:S(2)}) collective-permute-start(bf16[48,1408]{1,0:T(8,128)(2,1)S(1)} %slice.117), channel_id=1, source_target_pairs={{0,96},{32,0},{64,32},{96,64},{1,97},{33,1},{65,33},{97,65},{2,98}... | collective-permute-start | bytes 405512 | tf_op jit(solution)/shard_map/ppermute | solution.py:30
  108.5 2.5 collective-permute-done.11.refs_2_
  111.0 2.3 collective-permute-done.15.refs_7_
  114.0 1.1 join.1
  116.0 2.6 %collective-permute-start.17 = (bf16[384,1408]{1,0:T(8,128)(2,1)S(1)}, bf16[384,1408]{1,0:T(8,128)(2,1)S(1)}, u32[]{:S(2)}, u32[]{:S(2)}) collective-permute-start(bf16[384,1408]{1,0:T(8,128)(2,1)S(1)} %get-tuple-element.16.rest_0_), channel_id=1, source_target_pairs={{0,96},{32,0},{64,32},{96,64},{1,97},{33,1},{65,33},{97,65},{2,98}... | collective-permute-start | bytes 3244040 | tf_op jit(solution)/shard_map/ppermute | solution.py:30
  118.6 2.7 %collective-permute-start.21 = (bf16[384,1408]{1,0:T(8,128)(2,1)}, bf16[384,1408]{1,0:T(8,128)(2,1)S(1)}, u32[]{:S(2)}, u32[]{:S(2)}) collective-permute-start(bf16[384,1408]{1,0:T(8,128)(2,1)} %get-tuple-element.17.rest_5_), channel_id=1, source_target_pairs={{0,24},{8,0},{16,8},{24,16},{1,25},{9,1},{17,9},{25,17},{2,26},{10... | collective-permute-start | bytes 3244040 | tf_op jit(solution)/shard_map/ppermute | solution.py:30
  121.3 42.1 %collective-permute-done.18.rest_4_ = bf16[384,1408]{1,0:T(8,128)(2,1)S(1)} collective-permute-done((bf16[384,1408]{1,0:T(8,128)(2,1)S(1)}, bf16[384,1408]{1,0:T(8,128)(2,1)S(1)}, u32[]{:S(2)}, u32[]{:S(2)}) %collective-permute-start.18) | collective-permute-done | bytes 1081376 | tf_op jit(solution)/shard_map/ppermute | solution.py:30
  163.6 3.3 %collective-permute-start.20 = (bf16[192,1408]{1,0:T(8,128)(2,1)S(1)}, bf16[192,1408]{1,0:T(8,128)(2,1)S(1)}, u32[]{:S(2)}, u32[]{:S(2)}) collective-permute-start(bf16[192,1408]{1,0:T(8,128)(2,1)S(1)} %slice.119), channel_id=1, source_target_pairs={{0,96},{32,0},{64,32},{96,64},{1,97},{33,1},{65,33},{97,65},{2,98}... | collective-permute-start | bytes 1622024 | tf_op jit(solution)/shard_map/ppermute | solution.py:30
  167.1 2.7 %collective-permute-start.24 = (bf16[192,1408]{1,0:T(8,128)(2,1)S(1)}, bf16[192,1408]{1,0:T(8,128)(2,1)S(1)}, u32[]{:S(2)}, u32[]{:S(2)}) collective-permute-start(bf16[192,1408]{1,0:T(8,128)(2,1)S(1)} %slice.121), channel_id=1, source_target_pairs={{0,24},{8,0},{16,8},{24,16},{1,25},{9,1},{17,9},{25,17},{2,26},{10... | collective-permute-start | bytes 1622024 | tf_op jit(solution)/shard_map/ppermute | solution.py:30
  169.8 19.2 %collective-permute-done.19.rest_2_ = bf16[192,1408]{1,0:T(8,128)(2,1)S(1)} collective-permute-done((bf16[192,1408]{1,0:T(8,128)(2,1)S(1)}, bf16[192,1408]{1,0:T(8,128)(2,1)S(1)}, u32[]{:S(2)}, u32[]{:S(2)}) %collective-permute-start.19) | collective-permute-done | bytes 540704 | tf_op jit(solution)/shard_map/ppermute | solution.py:30
  189.1 1.2 collective-permute-done.23.rest_7_
  190.2 12.5 %grad_input.1 = (bf16[1536,512]{1,0:T(8,128)(2,1)}, bf16[1536,512]{1,0:T(8,128)(2,1)}) custom-call(s32[4]{0:T(128)S(1)} %pad_add_fusion.where_ref, bf16[1408,512]{1,0:T(8,128)(2,1)} %copy-done.4, bf16[384,1408]{1,0:T(8,128)(2,1)S(1)} %get-tuple-element.16.rest_0_, bf16[384,1408]{1,0:T(8,128)(2,1)} %copy-done.11, ...), custom_call_target="tpu_custom_call" | custom-call | flops 4429185024 | bytes 15000000 | tf_op jit(solution)/shard_map/grad_input/pallas_call | solution.py:285
  202.7 7.7 %collective-permute-start.25 = (bf16[1536,512]{1,0:T(8,128)(2,1)}, bf16[1536,512]{1,0:T(8,128)(2,1)S(1)}, u32[]{:S(2)}, u32[]{:S(2)}) collective-permute-start(bf16[1536,512]{1,0:T(8,128)(2,1)} %get-tuple-element.19), channel_id=1, source_target_pairs={{0,1},{1,0},{2,3},{3,2},{4,5},{5,4},{6,7},{7,6},{8,9},{9,8},{10,11... | collective-permute-start | bytes 4718600 | tf_op jit(solution)/shard_map/ppermute | solution.py:34
  210.4 3.2 %collective-permute-done.25 = bf16[1536,512]{1,0:T(8,128)(2,1)S(1)} collective-permute-done((bf16[1536,512]{1,0:T(8,128)(2,1)}, bf16[1536,512]{1,0:T(8,128)(2,1)S(1)}, u32[]{:S(2)}, u32[]{:S(2)}) %collective-permute-start.25) | collective-permute-done | bytes 1572896 | tf_op jit(solution)/shard_map/ppermute | solution.py:34
  213.6 1.9 add_convert_fusion
  215.6 1.3 collective-permute-start.26
  216.9 1.5 collective-permute-start.28
  218.3 4.7 %collective-permute-done.26 = bf16[192,512]{1,0:T(8,128)(2,1)S(1)} collective-permute-done((bf16[192,512]{1,0:T(8,128)(2,1)S(1)}, bf16[192,512]{1,0:T(8,128)(2,1)S(1)}, u32[]{:S(2)}, u32[]{:S(2)}) %collective-permute-start.26) | collective-permute-done | bytes 196640 | tf_op jit(solution)/shard_map/ppermute | solution.py:30
  223.2 1.0 collective-permute-start.27
  224.2 1.8 collective-permute-start.29
  226.5 11.7 %all_to_all.12 = f32[16,1,2496]{2,1,0:T(1,128)S(1)} all-to-all(f32[16,1,2496]{2,1,0:T(1,128)S(1)} %broadcast_in_dim.5), channel_id=1, replica_groups=mesh['z'=4,'y'=4,'x'=4,'c'=2] {'z','y'}, dimensions={0} | all-to-all | bytes 319488 | tf_op jit(solution)/shard_map/all_to_all | solution.py:300
  239.6 1.3 fusion.7
  241.8 1.3 convert_element_type.73
  243.2 1.3 fusion.11
  (99 shorter events, 11.0 us)
Async XLA Ops:
  7.2 3.0 %copy-start.6 = (bf16[512,384]{1,0:T(8,128)(2,1)S(1)}, bf16[512,384]{1,0:T(8,128)(2,1)}, u32[]{:S(2)}) copy-start(bf16[512,384]{1,0:T(8,128)(2,1)} %param.11) | copy-start | bytes 1179652
  7.2 3.2 %copy-start.15 = (f32[384]{0:T(512)S(1)}, f32[384]{0:T(512)}, u32[]{:S(2)}) copy-start(f32[384]{0:T(512)} %param.19) | copy-start | bytes 4612
  7.2 60.5 %all-gather.2.cloned.1.call-start = ((), (), s32[]{:S(2)}) async-start(), calls=%async_computation.3 | async-start | bytes 5013504 | tf_op jit(solution)/shard_map/all_gather | solution.py:326
  7.2 9.8 %copy-start.7 = (bf16[512,384]{1,0:T(8,128)(2,1)S(1)}, bf16[512,384]{1,0:T(8,128)(2,1)}, u32[]{:S(2)}) copy-start(bf16[512,384]{1,0:T(8,128)(2,1)} %param.10) | copy-start | bytes 1179652
  11.3 10.5 %all-to-all-start = ((f32[8,1,1024]{2,1,0:T(1,128)}), f32[8,1,1024]{2,1,0:T(1,128)S(1)}, u32[]{:S(2)}, u32[]{:S(2)}) async-start(f32[8,1,1024]{2,1,0:T(1,128)} %broadcast_in_dim.4), calls=%async_computation | async-start | bytes 65536 | tf_op jit(solution)/shard_map/all_to_all | solution.py:300
  17.1 224.7 %reduce-scatter.2.cloned.1.call-start = ((), (), s32[]{:S(2)}) async-start(), calls=%async_computation.4 | async-start | bytes 14204928 | tf_op jit(solution)/shard_map/reduce_scatter | solution.py:351
  22.2 33.0 %copy-start.14 = (f32[3,704]{1,0:T(4,128)S(1)}, f32[3,704]{1,0:T(4,128)}, u32[]{:S(2)}) copy-start(f32[3,704]{1,0:T(4,128)} %param.18) | copy-start | bytes 25348
  22.2 33.2 %copy-start = (bf16[512,704]{0,1:T(8,128)(2,1)S(1)}, bf16[512,704]{0,1:T(8,128)(2,1)}, u32[]{:S(2)}) copy-start(bf16[512,704]{0,1:T(8,128)(2,1)} %param.13) | copy-start | bytes 2162692
  22.2 33.2 %copy-start.1 = (bf16[512,704]{0,1:T(8,128)(2,1)S(1)}, bf16[512,704]{0,1:T(8,128)(2,1)}, u32[]{:S(2)}) copy-start(bf16[512,704]{0,1:T(8,128)(2,1)} %param.14) | copy-start | bytes 2162692
  22.4 19.6 %collective-permute-start.1 = (bf16[384,1024]{1,0:T(8,128)(2,1)S(1)}, bf16[384,1024]{1,0:T(8,128)(2,1)S(1)}, u32[]{:S(2)}, u32[]{:S(2)}) collective-permute-start(bf16[384,1024]{1,0:T(8,128)(2,1)S(1)} %pad_maximum_fusion.rest_0_), channel_id=1, source_target_pairs={{0,2},{2,4},{4,6},{6,0},{1,3},{3,5},{5,7},{7,1},{8,10},{10,12},{12... | collective-permute-start | bytes 2359304 | tf_op jit(solution)/shard_map/ppermute | solution.py:30
  22.7 19.4 %collective-permute-start = (bf16[384,1024]{1,0:T(8,128)(2,1)S(1)}, bf16[384,1024]{1,0:T(8,128)(2,1)}, u32[]{:S(2)}, u32[]{:S(2)}) collective-permute-start(bf16[384,1024]{1,0:T(8,128)(2,1)S(1)} %pad_maximum_fusion.rest_0_), channel_id=1, source_target_pairs={{0,6},{2,0},{4,2},{6,4},{1,7},{3,1},{5,3},{7,5},{8,14},{10,8},{12,... | collective-permute-start | bytes 2359304 | tf_op jit(solution)/shard_map/ppermute | solution.py:30
  25.1 32.3 %collective-permute-start.4 = (bf16[384,1024]{1,0:T(8,128)(2,1)S(1)}, bf16[384,1024]{1,0:T(8,128)(2,1)}, u32[]{:S(2)}, u32[]{:S(2)}) collective-permute-start(bf16[384,1024]{1,0:T(8,128)(2,1)S(1)} %pad_maximum_fusion.rest_0_), channel_id=1, source_target_pairs={{0,1},{1,0},{2,3},{3,2},{4,5},{5,4},{6,7},{7,6},{8,9},{9,8},{10,11... | collective-permute-start | bytes 2359304 | tf_op jit(solution)/shard_map/ppermute | solution.py:34
  42.0 10.5 %collective-permute-start.2 = (bf16[192,1024]{1,0:T(8,128)(2,1)S(1)}, bf16[192,1024]{1,0:T(8,128)(2,1)}, u32[]{:S(2)}, u32[]{:S(2)}) collective-permute-start(bf16[192,1024]{1,0:T(8,128)(2,1)S(1)} %slice.110), channel_id=1, source_target_pairs={{0,2},{2,4},{4,6},{6,0},{1,3},{3,5},{5,7},{7,1},{8,10},{10,12},{12... | collective-permute-start | bytes 1179656 | tf_op jit(solution)/shard_map/ppermute | solution.py:30
  43.1 11.8 %collective-permute-start.3 = (bf16[192,1024]{1,0:T(8,128)(2,1)S(1)}, bf16[192,1024]{1,0:T(8,128)(2,1)}, u32[]{:S(2)}, u32[]{:S(2)}) collective-permute-start(bf16[192,1024]{1,0:T(8,128)(2,1)S(1)} %slice.111), channel_id=1, source_target_pairs={{0,6},{2,0},{4,2},{6,4},{1,7},{3,1},{5,3},{7,5},{8,14},{10,8},{12,... | collective-permute-start | bytes 1179656 | tf_op jit(solution)/shard_map/ppermute | solution.py:30
  45.9 11.5 %collective-permute-start.5 = (bf16[384,1024]{1,0:T(8,128)(2,1)}, bf16[384,1024]{1,0:T(8,128)(2,1)}, u32[]{:S(2)}, u32[]{:S(2)}) collective-permute-start(bf16[384,1024]{1,0:T(8,128)(2,1)} %collective-permute-done.rest_1_), channel_id=1, source_target_pairs={{0,1},{1,0},{2,3},{3,2},{4,5},{5,4},{6,7},{7,6},{8,9},{9,8},{10,11... | collective-permute-start | bytes 2359304 | tf_op jit(solution)/shard_map/ppermute | solution.py:34
  48.0 9.4 %collective-permute-start.8 = (bf16[384,1024]{1,0:T(8,128)(2,1)S(1)}, bf16[384,1024]{1,0:T(8,128)(2,1)}, u32[]{:S(2)}, u32[]{:S(2)}) collective-permute-start(bf16[384,1024]{1,0:T(8,128)(2,1)S(1)} %collective-permute-done.1.rest_4_), channel_id=1, source_target_pairs={{0,1},{1,0},{2,3},{3,2},{4,5},{5,4},{6,7},{7,6},{8,9},{9,8},{10,11... | collective-permute-start | bytes 2359304 | tf_op jit(solution)/shard_map/ppermute | solution.py:34
  52.5 4.9 %collective-permute-start.6 = (bf16[192,1024]{1,0:T(8,128)(2,1)}, bf16[192,1024]{1,0:T(8,128)(2,1)}, u32[]{:S(2)}, u32[]{:S(2)}) collective-permute-start(bf16[192,1024]{1,0:T(8,128)(2,1)} %collective-permute-done.2.rest_2_), channel_id=1, source_target_pairs={{0,1},{1,0},{2,3},{3,2},{4,5},{5,4},{6,7},{7,6},{8,9},{9,8},{10,11... | collective-permute-start | bytes 1179656 | tf_op jit(solution)/shard_map/ppermute | solution.py:34
  54.9 2.5 collective-permute-start.7
  67.7 10.2 %copy-start.3 = (bf16[704,512]{1,0:T(8,128)(2,1)S(1)}, bf16[704,512]{1,0:T(8,128)(2,1)}, u32[]{:S(2)}) copy-start(bf16[704,512]{1,0:T(8,128)(2,1)} %copy-done.2) | copy-start | bytes 2162692
  91.1 1.1 copy-start.4
  92.3 1.0 copy-start.8
  92.3 1.0 copy-start.9
  93.5 8.5 %collective-permute-start.10 = (bf16[96,1408]{1,0:T(8,128)(2,1)S(1)}, bf16[96,1408]{1,0:T(8,128)(2,1)S(1)}, u32[]{:S(2)}, u32[]{:S(2)}) collective-permute-start(bf16[96,1408]{1,0:T(8,128)(2,1)S(1)} %get-tuple-element.59.refs_0_), channel_id=1, source_target_pairs={{0,8},{8,16},{16,24},{24,0},{1,9},{9,17},{17,25},{25,1},{2,10},{10... | collective-permute-start | bytes 811016 | tf_op jit(solution)/shard_map/ppermute | solution.py:30
  94.7 7.3 %collective-permute-start.9 = (bf16[96,1408]{1,0:T(8,128)(2,1)S(1)}, bf16[96,1408]{1,0:T(8,128)(2,1)S(1)}, u32[]{:S(2)}, u32[]{:S(2)}) collective-permute-start(bf16[96,1408]{1,0:T(8,128)(2,1)S(1)} %get-tuple-element.59.refs_0_), channel_id=1, source_target_pairs={{0,24},{8,0},{16,8},{24,16},{1,25},{9,1},{17,9},{25,17},{2,26},{10... | collective-permute-start | bytes 811016 | tf_op jit(solution)/shard_map/ppermute | solution.py:30
  96.2 8.6 %collective-permute-start.14 = (bf16[96,1408]{1,0:T(8,128)(2,1)S(1)}, bf16[96,1408]{1,0:T(8,128)(2,1)S(1)}, u32[]{:S(2)}, u32[]{:S(2)}) collective-permute-start(bf16[96,1408]{1,0:T(8,128)(2,1)S(1)} %get-tuple-element.58.refs_5_), channel_id=1, source_target_pairs={{0,32},{32,64},{64,96},{96,0},{1,33},{33,65},{65,97},{97,1},{2,34}... | collective-permute-start | bytes 811016 | tf_op jit(solution)/shard_map/ppermute | solution.py:30
  97.3 8.7 %collective-permute-start.13 = (bf16[96,1408]{1,0:T(8,128)(2,1)S(1)}, bf16[96,1408]{1,0:T(8,128)(2,1)S(1)}, u32[]{:S(2)}, u32[]{:S(2)}) collective-permute-start(bf16[96,1408]{1,0:T(8,128)(2,1)S(1)} %get-tuple-element.58.refs_5_), channel_id=1, source_target_pairs={{0,96},{32,0},{64,32},{96,64},{1,97},{33,1},{65,33},{97,65},{2,98}... | collective-permute-start | bytes 811016 | tf_op jit(solution)/shard_map/ppermute | solution.py:30
  102.0 9.1 %collective-permute-start.11 = (bf16[48,1408]{1,0:T(8,128)(2,1)S(1)}, bf16[48,1408]{1,0:T(8,128)(2,1)S(1)}, u32[]{:S(2)}, u32[]{:S(2)}) collective-permute-start(bf16[48,1408]{1,0:T(8,128)(2,1)S(1)} %slice.114), channel_id=1, source_target_pairs={{0,8},{8,16},{16,24},{24,0},{1,9},{9,17},{17,25},{25,1},{2,10},{10... | collective-permute-start | bytes 405512 | tf_op jit(solution)/shard_map/ppermute | solution.py:30
  102.1 8.9 %collective-permute-start.12 = (bf16[48,1408]{1,0:T(8,128)(2,1)S(1)}, bf16[48,1408]{1,0:T(8,128)(2,1)S(1)}, u32[]{:S(2)}, u32[]{:S(2)}) collective-permute-start(bf16[48,1408]{1,0:T(8,128)(2,1)S(1)} %slice.115), channel_id=1, source_target_pairs={{0,24},{8,0},{16,8},{24,16},{1,25},{9,1},{17,9},{25,17},{2,26},{10... | collective-permute-start | bytes 405512 | tf_op jit(solution)/shard_map/ppermute | solution.py:30
  104.8 8.5 %collective-permute-start.15 = (bf16[48,1408]{1,0:T(8,128)(2,1)S(1)}, bf16[48,1408]{1,0:T(8,128)(2,1)S(1)}, u32[]{:S(2)}, u32[]{:S(2)}) collective-permute-start(bf16[48,1408]{1,0:T(8,128)(2,1)S(1)} %slice.116), channel_id=1, source_target_pairs={{0,32},{32,64},{64,96},{96,0},{1,33},{33,65},{65,97},{97,1},{2,34}... | collective-permute-start | bytes 405512 | tf_op jit(solution)/shard_map/ppermute | solution.py:30
  105.9 8.0 %collective-permute-start.16 = (bf16[48,1408]{1,0:T(8,128)(2,1)S(1)}, bf16[48,1408]{1,0:T(8,128)(2,1)S(1)}, u32[]{:S(2)}, u32[]{:S(2)}) collective-permute-start(bf16[48,1408]{1,0:T(8,128)(2,1)S(1)} %slice.117), channel_id=1, source_target_pairs={{0,96},{32,0},{64,32},{96,64},{1,97},{33,1},{65,33},{97,65},{2,98}... | collective-permute-start | bytes 405512 | tf_op jit(solution)/shard_map/ppermute | solution.py:30
  115.1 48.3 %collective-permute-start.18 = (bf16[384,1408]{1,0:T(8,128)(2,1)S(1)}, bf16[384,1408]{1,0:T(8,128)(2,1)S(1)}, u32[]{:S(2)}, u32[]{:S(2)}) collective-permute-start(bf16[384,1408]{1,0:T(8,128)(2,1)S(1)} %get-tuple-element.16.rest_0_), channel_id=1, source_target_pairs={{0,32},{32,64},{64,96},{96,0},{1,33},{33,65},{65,97},{97,1},{2,34}... | collective-permute-start | bytes 3244040 | tf_op jit(solution)/shard_map/ppermute | solution.py:30
  116.0 47.5 %collective-permute-start.17 = (bf16[384,1408]{1,0:T(8,128)(2,1)S(1)}, bf16[384,1408]{1,0:T(8,128)(2,1)S(1)}, u32[]{:S(2)}, u32[]{:S(2)}) collective-permute-start(bf16[384,1408]{1,0:T(8,128)(2,1)S(1)} %get-tuple-element.16.rest_0_), channel_id=1, source_target_pairs={{0,96},{32,0},{64,32},{96,64},{1,97},{33,1},{65,33},{97,65},{2,98}... | collective-permute-start | bytes 3244040 | tf_op jit(solution)/shard_map/ppermute | solution.py:30
  118.6 48.2 %collective-permute-start.22 = (bf16[384,1408]{1,0:T(8,128)(2,1)}, bf16[384,1408]{1,0:T(8,128)(2,1)S(1)}, u32[]{:S(2)}, u32[]{:S(2)}) collective-permute-start(bf16[384,1408]{1,0:T(8,128)(2,1)} %get-tuple-element.17.rest_5_), channel_id=1, source_target_pairs={{0,8},{8,16},{16,24},{24,0},{1,9},{9,17},{17,25},{25,1},{2,10},{10... | collective-permute-start | bytes 3244040 | tf_op jit(solution)/shard_map/ppermute | solution.py:30
  118.6 48.4 %collective-permute-start.21 = (bf16[384,1408]{1,0:T(8,128)(2,1)}, bf16[384,1408]{1,0:T(8,128)(2,1)S(1)}, u32[]{:S(2)}, u32[]{:S(2)}) collective-permute-start(bf16[384,1408]{1,0:T(8,128)(2,1)} %get-tuple-element.17.rest_5_), channel_id=1, source_target_pairs={{0,24},{8,0},{16,8},{24,16},{1,25},{9,1},{17,9},{25,17},{2,26},{10... | collective-permute-start | bytes 3244040 | tf_op jit(solution)/shard_map/ppermute | solution.py:30
  163.4 3.6 %copy-start.10 = (bf16[384,1408]{1,0:T(8,128)(2,1)}, bf16[384,1408]{1,0:T(8,128)(2,1)S(1)}, u32[]{:S(2)}) copy-start(bf16[384,1408]{1,0:T(8,128)(2,1)S(1)} %collective-permute-done.18.rest_4_) | copy-start | bytes 3244036
  163.4 25.6 %collective-permute-start.19 = (bf16[192,1408]{1,0:T(8,128)(2,1)S(1)}, bf16[192,1408]{1,0:T(8,128)(2,1)S(1)}, u32[]{:S(2)}, u32[]{:S(2)}) collective-permute-start(bf16[192,1408]{1,0:T(8,128)(2,1)S(1)} %slice.118), channel_id=1, source_target_pairs={{0,32},{32,64},{64,96},{96,0},{1,33},{33,65},{65,97},{97,1},{2,34}... | collective-permute-start | bytes 1622024 | tf_op jit(solution)/shard_map/ppermute | solution.py:30
  163.5 3.6 %copy-start.11 = (bf16[384,1408]{1,0:T(8,128)(2,1)}, bf16[384,1408]{1,0:T(8,128)(2,1)S(1)}, u32[]{:S(2)}) copy-start(bf16[384,1408]{1,0:T(8,128)(2,1)S(1)} %collective-permute-done.17.rest_1_) | copy-start | bytes 3244036
  163.6 25.5 %collective-permute-start.20 = (bf16[192,1408]{1,0:T(8,128)(2,1)S(1)}, bf16[192,1408]{1,0:T(8,128)(2,1)S(1)}, u32[]{:S(2)}, u32[]{:S(2)}) collective-permute-start(bf16[192,1408]{1,0:T(8,128)(2,1)S(1)} %slice.119), channel_id=1, source_target_pairs={{0,96},{32,0},{64,32},{96,64},{1,97},{33,1},{65,33},{97,65},{2,98}... | collective-permute-start | bytes 1622024 | tf_op jit(solution)/shard_map/ppermute | solution.py:30
  166.9 23.4 %copy-start.12 = (bf16[384,1408]{1,0:T(8,128)(2,1)}, bf16[384,1408]{1,0:T(8,128)(2,1)S(1)}, u32[]{:S(2)}) copy-start(bf16[384,1408]{1,0:T(8,128)(2,1)S(1)} %collective-permute-done.22.rest_9_) | copy-start | bytes 3244036
  166.9 23.3 %collective-permute-start.23 = (bf16[192,1408]{1,0:T(8,128)(2,1)S(1)}, bf16[192,1408]{1,0:T(8,128)(2,1)S(1)}, u32[]{:S(2)}, u32[]{:S(2)}) collective-permute-start(bf16[192,1408]{1,0:T(8,128)(2,1)S(1)} %slice.120), channel_id=1, source_target_pairs={{0,8},{8,16},{16,24},{24,0},{1,9},{9,17},{17,25},{25,1},{2,10},{10... | collective-permute-start | bytes 1622024 | tf_op jit(solution)/shard_map/ppermute | solution.py:30
  167.0 23.2 %copy-start.13 = (bf16[384,1408]{1,0:T(8,128)(2,1)}, bf16[384,1408]{1,0:T(8,128)(2,1)S(1)}, u32[]{:S(2)}) copy-start(bf16[384,1408]{1,0:T(8,128)(2,1)S(1)} %collective-permute-done.21.rest_6_) | copy-start | bytes 3244036
  167.1 23.1 %collective-permute-start.24 = (bf16[192,1408]{1,0:T(8,128)(2,1)S(1)}, bf16[192,1408]{1,0:T(8,128)(2,1)S(1)}, u32[]{:S(2)}, u32[]{:S(2)}) collective-permute-start(bf16[192,1408]{1,0:T(8,128)(2,1)S(1)} %slice.121), channel_id=1, source_target_pairs={{0,24},{8,0},{16,8},{24,16},{1,25},{9,1},{17,9},{25,17},{2,26},{10... | collective-permute-start | bytes 1622024 | tf_op jit(solution)/shard_map/ppermute | solution.py:30
  202.7 10.9 %collective-permute-start.25 = (bf16[1536,512]{1,0:T(8,128)(2,1)}, bf16[1536,512]{1,0:T(8,128)(2,1)S(1)}, u32[]{:S(2)}, u32[]{:S(2)}) collective-permute-start(bf16[1536,512]{1,0:T(8,128)(2,1)} %get-tuple-element.19), channel_id=1, source_target_pairs={{0,1},{1,0},{2,3},{3,2},{4,5},{5,4},{6,7},{7,6},{8,9},{9,8},{10,11... | collective-permute-start | bytes 4718600 | tf_op jit(solution)/shard_map/ppermute | solution.py:34
  215.6 7.5 %collective-permute-start.26 = (bf16[192,512]{1,0:T(8,128)(2,1)S(1)}, bf16[192,512]{1,0:T(8,128)(2,1)S(1)}, u32[]{:S(2)}, u32[]{:S(2)}) collective-permute-start(bf16[192,512]{1,0:T(8,128)(2,1)S(1)} %get-tuple-element.50), channel_id=1, source_target_pairs={{0,2},{2,4},{4,6},{6,0},{1,3},{3,5},{5,7},{7,1},{8,10},{10,12},{12... | collective-permute-start | bytes 589832 | tf_op jit(solution)/shard_map/ppermute | solution.py:30
  216.9 6.2 %collective-permute-start.28 = (bf16[192,512]{1,0:T(8,128)(2,1)S(1)}, bf16[192,512]{1,0:T(8,128)(2,1)S(1)}, u32[]{:S(2)}, u32[]{:S(2)}) collective-permute-start(bf16[192,512]{1,0:T(8,128)(2,1)S(1)} %get-tuple-element.51), channel_id=1, source_target_pairs={{0,6},{2,0},{4,2},{6,4},{1,7},{3,1},{5,3},{7,5},{8,14},{10,8},{12,... | collective-permute-start | bytes 589832 | tf_op jit(solution)/shard_map/ppermute | solution.py:30
  223.2 16.4 %collective-permute-start.27 = (bf16[384,512]{1,0:T(8,128)(2,1)S(1)}, bf16[384,512]{1,0:T(8,128)(2,1)}, u32[]{:S(2)}, u32[]{:S(2)}) collective-permute-start(bf16[384,512]{1,0:T(8,128)(2,1)S(1)} %pad_maximum_fusion.1), channel_id=1, source_target_pairs={{0,2},{2,4},{4,6},{6,0},{1,3},{3,5},{5,7},{7,1},{8,10},{10,12},{12... | collective-permute-start | bytes 1179656 | tf_op jit(solution)/shard_map/ppermute | solution.py:30
  224.2 15.3 %collective-permute-start.29 = (bf16[384,512]{1,0:T(8,128)(2,1)S(1)}, bf16[384,512]{1,0:T(8,128)(2,1)}, u32[]{:S(2)}, u32[]{:S(2)}) collective-permute-start(bf16[384,512]{1,0:T(8,128)(2,1)S(1)} %pad_maximum_fusion.2), channel_id=1, source_target_pairs={{0,6},{2,0},{4,2},{6,4},{1,7},{3,1},{5,3},{7,5},{8,14},{10,8},{12,... | collective-permute-start | bytes 1179656 | tf_op jit(solution)/shard_map/ppermute | solution.py:30
  241.8 1.4 copy-start.5
  (1 other events, 0.9 us)
Sparse Core Ops, SparseCore 0:
  10.7 56.9 all-gather.1
  92.4 132.3 reduce-scatter.1

commit v4 on v3

--- a/solution.py
+++ b/solution.py
@@ -73,7 +73,8 @@
 
 
 STEP = 88
-BACK_STEPS = 4
+BACK_STEPS = 2
+OUTER_STEPS = 4
 
 
 def hidden_body(gate_ref, value_ref, taps_ref, hidden_ref):
@@ -261,23 +262,44 @@
 
 
 def outer_of(inputs, grad, both, hidden):
+    rows = D // OUTER_STEPS
     return pl.pallas_call(
         outer_body,
         out_shape=jax.ShapeDtypeStruct((D, 3 * UNITS), BF16),
-        grid=(8,),
+        grid=(OUTER_STEPS,),
         in_specs=[
-            pl.BlockSpec((COLS, TOKS), lambda i: (i, 0)),
-            pl.BlockSpec((COLS, TOKS), lambda i: (i, 0)),
+            pl.BlockSpec((rows, TOKS), lambda i: (i, 0)),
+            pl.BlockSpec((rows, TOKS), lambda i: (i, 0)),
             VMEM,
             VMEM,
         ],
-        out_specs=pl.BlockSpec((COLS, 3 * UNITS), lambda i: (i, 0)),
+        out_specs=pl.BlockSpec((rows, 3 * UNITS), lambda i: (i, 0)),
         compiler_params=PARAMS,
         cost_estimate=pl.CostEstimate(
             flops=6 * D * UNITS * TOKS, bytes_accessed=20_000_000, transcendentals=0
         ),
         name="outer",
     )(inputs, grad, both, hidden)
+
+
+def widen_body(summed_ref, *outs):
+    whole = summed_ref[...].astype(F32)
+    for k, out_ref in enumerate(outs):
+        out_ref[...] = whole[:, k * UNITS : (k + 1) * UNITS]
+
+
+def widened(summed):
+    rows = ROWS // 2
+    shape = jax.ShapeDtypeStruct((ROWS, UNITS), F32)
+    return pl.pallas_call(
+        widen_body,
+        out_shape=(shape,) * 3,
+        grid=(2,),
+        in_specs=[pl.BlockSpec((rows, 3 * UNITS), lambda i: (i, 0))],
+        out_specs=(pl.BlockSpec((rows, UNITS), lambda i: (i, 0)),) * 3,
+        compiler_params=PARAMS,
+        name="widen",
+    )(summed)
 
 
 def input_of(where, right, pieces):
@@ -348,7 +370,8 @@
     hidden = hidden_of(gate, value, taps)
     grads, taps_local = back_of(down_full, grad_full, gate, value, taps)
     terms = outer_of(inputs_full, grad_full, grads, hidden)
-    summed = lax.psum_scatter(terms, FS, scatter_dimension=0, tiled=True).astype(F32)
+    summed = lax.psum_scatter(terms, FS, scatter_dimension=0, tiled=True)
+    grad_gate, grad_value, grad_down = widened(summed)
 
     kept, sent = input_of(where, grads, pieces)
     paired = plus(kept, swapped(sent))
@@ -360,9 +383,9 @@
     grad_gain = small[3 * UNITS :]
     return (
         grad_input,
-        summed[:, :UNITS],
-        summed[:, UNITS : 2 * UNITS],
-        summed[:, 2 * UNITS :].T,
+        grad_gate,
+        grad_value,
+        grad_down.T,
         grad_taps,
         grad_gain,
     )

time: 254 us -> 251 us (0.988)
  no operation moved by 1% of the time
where the time goes in v4:
time: 251 us; the launch traced here: 249 us
  waiting for transfers between devices  108 us (43%)
  starting transfers between devices  55.1 us (22%)
  Pallas kernels  42.6 us (17%)
  between operations  14.4 us (6%)
  local copies, waits for them, and re-layouts  12.3 us (5%)
  blocking collectives  11.7 us (5%)
  other arithmetic  4.46 us (2%)
    ppermute x24, waiting for transfers between devices, moved(): return lax.ppermute(value, axis, [(i, (i + by) % 4) for i in range(4)])  95.8 us
    ppermute x24, starting transfers between devices, moved(): return lax.ppermute(value, axis, [(i, (i + by) % 4) for i in range(4)])  35.3 us
    ppermute x6, starting transfers between devices, swapped(): return lax.ppermute(value, 'c', [(0, 1), (1, 0)])  13.9 us
    pallas_call x1, Pallas kernels, input_of(): pl.pallas_call(input_body, out_shape=(shape, shape), in_specs=[SMEM] + [V...  12.5 us
    pallas_call x1, Pallas kernels, outer_of(): pl.pallas_call(outer_body, out_shape=jax.ShapeDtypeStruct((D, 3 * UNITS),...  11.9 us
    all_to_all x1, blocking collectives, copy_for_each(): return lax.all_to_all(copies, axis, split_axis=0, concat_axis=0, tiled=True)  11.7 us
    pallas_call x1, Pallas kernels, back_of(): pl.pallas_call(back_body, out_shape=(jax.ShapeDtypeStruct((2 * UNITS, TOK...  9.4 us
    unnamed x37, local copies, waits for them, and re-layouts  6.91 us
  transfers between devices with their start and end apart: 33, of which 13 were waited for; matrix products, arithmetic and copies ran while one was open for 4% of the time, Pallas kernels for 8%

profile of v4, /device:TPU:1, one launch (start us, length us, event | category | flops | bytes accessed | tf_op | source)
XLA Modules:
  0.0 248.9 jit_solution(7684291181704279519)
XLA Ops:
  7.2 1.8 pad.4
  9.0 1.2 copy.33
  11.3 5.8 %all-to-all-start = ((f32[8,1,1024]{2,1,0:T(1,128)}), f32[8,1,1024]{2,1,0:T(1,128)S(1)}, u32[]{:S(2)}, u32[]{:S(2)}) async-start(f32[8,1,1024]{2,1,0:T(1,128)} %broadcast_in_dim.4), calls=%async_computation | async-start | bytes 65536 | tf_op jit(solution)/shard_map/all_to_all | solution.py:322
  17.3 4.5 %all-to-all-done = f32[8,1,1024]{2,1,0:T(1,128)S(1)} async-done(((f32[8,1,1024]{2,1,0:T(1,128)}), f32[8,1,1024]{2,1,0:T(1,128)S(1)}, u32[]{:S(2)}, u32[]{:S(2)}) %all-to-all-start) | async-done | bytes 32800 | tf_op jit(solution)/shard_map/all_to_all | solution.py:322
  22.7 2.4 collective-permute-start
  25.1 1.3 collective-permute-start.4
  26.4 15.6 %collective-permute-done.1.rest_4_ = bf16[384,1024]{1,0:T(8,128)(2,1)S(1)} collective-permute-done((bf16[384,1024]{1,0:T(8,128)(2,1)S(1)}, bf16[384,1024]{1,0:T(8,128)(2,1)S(1)}, u32[]{:S(2)}, u32[]{:S(2)}) %collective-permute-start.1) | collective-permute-done | bytes 786464 | tf_op jit(solution)/shard_map/ppermute | solution.py:30
  42.1 1.0 slice.99
  43.1 2.7 %collective-permute-start.3 = (bf16[192,1024]{1,0:T(8,128)(2,1)S(1)}, bf16[192,1024]{1,0:T(8,128)(2,1)}, u32[]{:S(2)}, u32[]{:S(2)}) collective-permute-start(bf16[192,1024]{1,0:T(8,128)(2,1)S(1)} %slice.99), channel_id=1, source_target_pairs={{0,6},{2,0},{4,2},{6,4},{1,7},{3,1},{5,3},{7,5},{8,14},{10,8},{12,... | collective-permute-start | bytes 1179656 | tf_op jit(solution)/shard_map/ppermute | solution.py:30
  45.9 2.2 collective-permute-start.5
  48.0 4.5 %collective-permute-done.2.rest_2_ = bf16[192,1024]{1,0:T(8,128)(2,1)} collective-permute-done((bf16[192,1024]{1,0:T(8,128)(2,1)S(1)}, bf16[192,1024]{1,0:T(8,128)(2,1)}, u32[]{:S(2)}, u32[]{:S(2)}) %collective-permute-start.2) | collective-permute-done | bytes 393248 | tf_op jit(solution)/shard_map/ppermute | solution.py:30
  52.5 2.4 collective-permute-start.6
  55.4 1.0 hidden.1.hidden_ref
  57.4 5.5 %arrange.1 = (bf16[3072,512]{1,0:T(8,128)(2,1)}, bf16[3072,512]{1,0:T(8,128)(2,1)}) custom-call(s32[4]{0:T(128)S(1)} %pad_add_fusion.where_ref, bf16[384,1024]{1,0:T(8,128)(2,1)S(1)} %pad_maximum_fusion.rest_0_, bf16[384,1024]{1,0:T(8,128)(2,1)} %collective-permute-done.rest_1_, bf16[192,1024]{1,0:T(8,128)(2,1)} %collective-permute-done.2.rest_2_, ...), custom_call_target="tpu_custom_call" | custom-call | tf_op jit(solution)/shard_map/arrange/pallas_call | solution.py:216
  62.9 4.8 %all-gather.2.cloned.1.call-done.down_ref = bf16[3072,768]{1,0:T(8,128)(2,1)} async-done(((bf16[192,768]{1,0:T(8,128)(2,1)}), bf16[3072,768]{1,0:T(8,128)(2,1)}) %all-gather.2.cloned.1.call-update) | async-done | bytes 4718608 | tf_op jit(solution)/shard_map/all_gather | solution.py:348
  67.7 9.4 %back.1 = (bf16[1408,512]{1,0:T(8,128)(2,1)S(1)}, f32[704,3]{1,0:T(8,128)S(1)}) custom-call(bf16[3072,768]{1,0:T(8,128)(2,1)} %all-gather.2.cloned.1.call-done.down_ref, bf16[3072,512]{1,0:T(8,128)(2,1)} %get-tuple-element.17.grad_ref, bf16[704,512]{1,0:T(8,128)(2,1)S(1)} %bitcast.19, bf16[704,512]{1,0:T(8,128)(2,1)S(1)} %bitcast.21, f32[704,3]{1,0:T(8,128)S(1)} %bitcast.17), custom_call_target="tpu_custom_call" | custom-call | flops 2214592512 | bytes 12000000 | tf_op jit(solution)/shard_map/back/pallas_call | solution.py:240
  77.1 11.9 %outer.1 = bf16[3072,2112]{1,0:T(8,128)(2,1)} custom-call(bf16[3072,512]{1,0:T(8,128)(2,1)} %get-tuple-element.23.inputs_ref, bf16[3072,512]{1,0:T(8,128)(2,1)} %get-tuple-element.17.grad_ref, bf16[1408,512]{1,0:T(8,128)(2,1)S(1)} %get-tuple-element.18.right_ref.both_ref, bf16[704,512]{1,0:T(8,128)(2,1)S(1)} %copy-done.4), custom_call_target="tpu_custom_call" | custom-call | flops 6643777536 | bytes 20000000 | tf_op jit(solution)/shard_map/outer/pallas_call | solution.py:266
  89.0 1.1 copy-done.5
  91.3 1.2 collective-permute-start.10
  92.6 1.5 collective-permute-start.9
  94.1 1.1 collective-permute-start.14
  95.2 1.6 collective-permute-start.13
  96.8 3.0 %collective-permute-done.10.refs_4_ = bf16[96,1408]{1,0:T(8,128)(2,1)S(1)} collective-permute-done((bf16[96,1408]{1,0:T(8,128)(2,1)S(1)}, bf16[96,1408]{1,0:T(8,128)(2,1)S(1)}, u32[]{:S(2)}, u32[]{:S(2)}) %collective-permute-start.10) | collective-permute-done | bytes 270368 | tf_op jit(solution)/shard_map/ppermute | solution.py:30
  99.9 2.7 %collective-permute-start.12 = (bf16[48,1408]{1,0:T(8,128)(2,1)S(1)}, bf16[48,1408]{1,0:T(8,128)(2,1)S(1)}, u32[]{:S(2)}, u32[]{:S(2)}) collective-permute-start(bf16[48,1408]{1,0:T(8,128)(2,1)S(1)} %slice.103), channel_id=1, source_target_pairs={{0,24},{8,0},{16,8},{24,16},{1,25},{9,1},{17,9},{25,17},{2,26},{10... | collective-permute-start | bytes 405512 | tf_op jit(solution)/shard_map/ppermute | solution.py:30
  102.7 1.2 collective-permute-start.15
  103.9 2.4 collective-permute-start.16
  106.3 2.5 %collective-permute-done.11.refs_2_ = bf16[48,1408]{1,0:T(8,128)(2,1)S(1)} collective-permute-done((bf16[48,1408]{1,0:T(8,128)(2,1)S(1)}, bf16[48,1408]{1,0:T(8,128)(2,1)S(1)}, u32[]{:S(2)}, u32[]{:S(2)}) %collective-permute-start.11) | collective-permute-done | bytes 135200 | tf_op jit(solution)/shard_map/ppermute | solution.py:30
  108.9 2.2 collective-permute-done.15.refs_7_
  111.8 1.1 join.1
  113.9 2.6 %collective-permute-start.17 = (bf16[384,1408]{1,0:T(8,128)(2,1)S(1)}, bf16[384,1408]{1,0:T(8,128)(2,1)S(1)}, u32[]{:S(2)}, u32[]{:S(2)}) collective-permute-start(bf16[384,1408]{1,0:T(8,128)(2,1)S(1)} %get-tuple-element.19.rest_0_), channel_id=1, source_target_pairs={{0,96},{32,0},{64,32},{96,64},{1,97},{33,1},{65,33},{97,65},{2,98}... | collective-permute-start | bytes 3244040 | tf_op jit(solution)/shard_map/ppermute | solution.py:30
  116.5 2.7 %collective-permute-start.21 = (bf16[384,1408]{1,0:T(8,128)(2,1)}, bf16[384,1408]{1,0:T(8,128)(2,1)S(1)}, u32[]{:S(2)}, u32[]{:S(2)}) collective-permute-start(bf16[384,1408]{1,0:T(8,128)(2,1)} %get-tuple-element.20.rest_5_), channel_id=1, source_target_pairs={{0,24},{8,0},{16,8},{24,16},{1,25},{9,1},{17,9},{25,17},{2,26},{10... | collective-permute-start | bytes 3244040 | tf_op jit(solution)/shard_map/ppermute | solution.py:30
  119.1 42.0 %collective-permute-done.18.rest_4_ = bf16[384,1408]{1,0:T(8,128)(2,1)S(1)} collective-permute-done((bf16[384,1408]{1,0:T(8,128)(2,1)S(1)}, bf16[384,1408]{1,0:T(8,128)(2,1)S(1)}, u32[]{:S(2)}, u32[]{:S(2)}) %collective-permute-start.18) | collective-permute-done | bytes 1081376 | tf_op jit(solution)/shard_map/ppermute | solution.py:30
  161.3 3.3 %collective-permute-start.20 = (bf16[192,1408]{1,0:T(8,128)(2,1)S(1)}, bf16[192,1408]{1,0:T(8,128)(2,1)S(1)}, u32[]{:S(2)}, u32[]{:S(2)}) collective-permute-start(bf16[192,1408]{1,0:T(8,128)(2,1)S(1)} %slice.107), channel_id=1, source_target_pairs={{0,96},{32,0},{64,32},{96,64},{1,97},{33,1},{65,33},{97,65},{2,98}... | collective-permute-start | bytes 1622024 | tf_op jit(solution)/shard_map/ppermute | solution.py:30
  164.9 2.7 %collective-permute-start.24 = (bf16[192,1408]{1,0:T(8,128)(2,1)S(1)}, bf16[192,1408]{1,0:T(8,128)(2,1)S(1)}, u32[]{:S(2)}, u32[]{:S(2)}) collective-permute-start(bf16[192,1408]{1,0:T(8,128)(2,1)S(1)} %slice.109), channel_id=1, source_target_pairs={{0,24},{8,0},{16,8},{24,16},{1,25},{9,1},{17,9},{25,17},{2,26},{10... | collective-permute-start | bytes 1622024 | tf_op jit(solution)/shard_map/ppermute | solution.py:30
  167.6 19.2 %collective-permute-done.19.rest_2_ = bf16[192,1408]{1,0:T(8,128)(2,1)S(1)} collective-permute-done((bf16[192,1408]{1,0:T(8,128)(2,1)S(1)}, bf16[192,1408]{1,0:T(8,128)(2,1)S(1)}, u32[]{:S(2)}, u32[]{:S(2)}) %collective-permute-start.19) | collective-permute-done | bytes 540704 | tf_op jit(solution)/shard_map/ppermute | solution.py:30
  186.8 1.2 collective-permute-done.23.rest_7_
  188.0 12.5 %grad_input.1 = (bf16[1536,512]{1,0:T(8,128)(2,1)}, bf16[1536,512]{1,0:T(8,128)(2,1)}) custom-call(s32[4]{0:T(128)S(1)} %pad_add_fusion.where_ref, bf16[1408,512]{1,0:T(8,128)(2,1)} %copy-done.5, bf16[384,1408]{1,0:T(8,128)(2,1)S(1)} %get-tuple-element.19.rest_0_, bf16[384,1408]{1,0:T(8,128)(2,1)} %copy-done.11, ...), custom_call_target="tpu_custom_call" | custom-call | flops 4429185024 | bytes 15000000 | tf_op jit(solution)/shard_map/grad_input/pallas_call | solution.py:307
  200.5 7.8 %collective-permute-start.25 = (bf16[1536,512]{1,0:T(8,128)(2,1)}, bf16[1536,512]{1,0:T(8,128)(2,1)S(1)}, u32[]{:S(2)}, u32[]{:S(2)}) collective-permute-start(bf16[1536,512]{1,0:T(8,128)(2,1)} %get-tuple-element.22), channel_id=1, source_target_pairs={{0,1},{1,0},{2,3},{3,2},{4,5},{5,4},{6,7},{7,6},{8,9},{9,8},{10,11... | collective-permute-start | bytes 4718600 | tf_op jit(solution)/shard_map/ppermute | solution.py:34
  208.3 3.2 %collective-permute-done.25 = bf16[1536,512]{1,0:T(8,128)(2,1)S(1)} collective-permute-done((bf16[1536,512]{1,0:T(8,128)(2,1)}, bf16[1536,512]{1,0:T(8,128)(2,1)S(1)}, u32[]{:S(2)}, u32[]{:S(2)}) %collective-permute-start.25) | collective-permute-done | bytes 1572896 | tf_op jit(solution)/shard_map/ppermute | solution.py:34
  211.5 1.9 add_convert_fusion
  213.5 1.2 collective-permute-start.26
  214.7 1.5 collective-permute-start.28
  216.2 4.7 %collective-permute-done.26 = bf16[192,512]{1,0:T(8,128)(2,1)S(1)} collective-permute-done((bf16[192,512]{1,0:T(8,128)(2,1)S(1)}, bf16[192,512]{1,0:T(8,128)(2,1)S(1)}, u32[]{:S(2)}, u32[]{:S(2)}) %collective-permute-start.26) | collective-permute-done | bytes 196640 | tf_op jit(solution)/shard_map/ppermute | solution.py:30
  222.1 1.9 collective-permute-start.29
  224.4 11.7 %all_to_all.12 = f32[16,1,2496]{2,1,0:T(1,128)S(1)} all-to-all(f32[16,1,2496]{2,1,0:T(1,128)S(1)} %broadcast_in_dim.5), channel_id=1, replica_groups=mesh['z'=4,'y'=4,'x'=4,'c'=2] {'z','y'}, dimensions={0} | all-to-all | bytes 319488 | tf_op jit(solution)/shard_map/all_to_all | solution.py:322
  237.5 1.3 fusion.7
  239.7 1.1 copy-done.2
  240.8 1.2 widen.1
  (98 shorter events, 11.0 us)
Async XLA Ops:
  7.2 3.0 %copy-start.6 = (bf16[512,384]{1,0:T(8,128)(2,1)S(1)}, bf16[512,384]{1,0:T(8,128)(2,1)}, u32[]{:S(2)}) copy-start(bf16[512,384]{1,0:T(8,128)(2,1)} %param.11) | copy-start | bytes 1179652
  7.2 3.2 %copy-start.15 = (f32[384]{0:T(512)S(1)}, f32[384]{0:T(512)}, u32[]{:S(2)}) copy-start(f32[384]{0:T(512)} %param.19) | copy-start | bytes 4612
  7.2 60.5 %all-gather.2.cloned.1.call-start = ((), (), s32[]{:S(2)}) async-start(), calls=%async_computation.3 | async-start | bytes 5013504 | tf_op jit(solution)/shard_map/all_gather | solution.py:348
  7.2 9.8 %copy-start.7 = (bf16[512,384]{1,0:T(8,128)(2,1)S(1)}, bf16[512,384]{1,0:T(8,128)(2,1)}, u32[]{:S(2)}) copy-start(bf16[512,384]{1,0:T(8,128)(2,1)} %param.10) | copy-start | bytes 1179652
  11.3 10.5 %all-to-all-start = ((f32[8,1,1024]{2,1,0:T(1,128)}), f32[8,1,1024]{2,1,0:T(1,128)S(1)}, u32[]{:S(2)}, u32[]{:S(2)}) async-start(f32[8,1,1024]{2,1,0:T(1,128)} %broadcast_in_dim.4), calls=%async_computation | async-start | bytes 65536 | tf_op jit(solution)/shard_map/all_to_all | solution.py:322
  17.1 222.6 %reduce-scatter.2.cloned.1.call-start = ((), (), s32[]{:S(2)}) async-start(), calls=%async_computation.4 | async-start | bytes 14204928 | tf_op jit(solution)/shard_map/reduce_scatter | solution.py:373
  22.2 33.0 %copy-start.14 = (f32[3,704]{1,0:T(4,128)S(1)}, f32[3,704]{1,0:T(4,128)}, u32[]{:S(2)}) copy-start(f32[3,704]{1,0:T(4,128)} %param.18) | copy-start | bytes 25348
  22.2 33.2 %copy-start = (bf16[512,704]{0,1:T(8,128)(2,1)S(1)}, bf16[512,704]{0,1:T(8,128)(2,1)}, u32[]{:S(2)}) copy-start(bf16[512,704]{0,1:T(8,128)(2,1)} %param.13) | copy-start | bytes 2162692
  22.2 33.2 %copy-start.1 = (bf16[512,704]{0,1:T(8,128)(2,1)S(1)}, bf16[512,704]{0,1:T(8,128)(2,1)}, u32[]{:S(2)}) copy-start(bf16[512,704]{0,1:T(8,128)(2,1)} %param.14) | copy-start | bytes 2162692
  22.4 19.6 %collective-permute-start.1 = (bf16[384,1024]{1,0:T(8,128)(2,1)S(1)}, bf16[384,1024]{1,0:T(8,128)(2,1)S(1)}, u32[]{:S(2)}, u32[]{:S(2)}) collective-permute-start(bf16[384,1024]{1,0:T(8,128)(2,1)S(1)} %pad_maximum_fusion.rest_0_), channel_id=1, source_target_pairs={{0,2},{2,4},{4,6},{6,0},{1,3},{3,5},{5,7},{7,1},{8,10},{10,12},{12... | collective-permute-start | bytes 2359304 | tf_op jit(solution)/shard_map/ppermute | solution.py:30
  22.7 19.4 %collective-permute-start = (bf16[384,1024]{1,0:T(8,128)(2,1)S(1)}, bf16[384,1024]{1,0:T(8,128)(2,1)}, u32[]{:S(2)}, u32[]{:S(2)}) collective-permute-start(bf16[384,1024]{1,0:T(8,128)(2,1)S(1)} %pad_maximum_fusion.rest_0_), channel_id=1, source_target_pairs={{0,6},{2,0},{4,2},{6,4},{1,7},{3,1},{5,3},{7,5},{8,14},{10,8},{12,... | collective-permute-start | bytes 2359304 | tf_op jit(solution)/shard_map/ppermute | solution.py:30
  25.1 32.3 %collective-permute-start.4 = (bf16[384,1024]{1,0:T(8,128)(2,1)S(1)}, bf16[384,1024]{1,0:T(8,128)(2,1)}, u32[]{:S(2)}, u32[]{:S(2)}) collective-permute-start(bf16[384,1024]{1,0:T(8,128)(2,1)S(1)} %pad_maximum_fusion.rest_0_), channel_id=1, source_target_pairs={{0,1},{1,0},{2,3},{3,2},{4,5},{5,4},{6,7},{7,6},{8,9},{9,8},{10,11... | collective-permute-start | bytes 2359304 | tf_op jit(solution)/shard_map/ppermute | solution.py:34
  42.0 10.5 %collective-permute-start.2 = (bf16[192,1024]{1,0:T(8,128)(2,1)S(1)}, bf16[192,1024]{1,0:T(8,128)(2,1)}, u32[]{:S(2)}, u32[]{:S(2)}) collective-permute-start(bf16[192,1024]{1,0:T(8,128)(2,1)S(1)} %slice.98), channel_id=1, source_target_pairs={{0,2},{2,4},{4,6},{6,0},{1,3},{3,5},{5,7},{7,1},{8,10},{10,12},{12... | collective-permute-start | bytes 1179656 | tf_op jit(solution)/shard_map/ppermute | solution.py:30
  43.1 11.8 %collective-permute-start.3 = (bf16[192,1024]{1,0:T(8,128)(2,1)S(1)}, bf16[192,1024]{1,0:T(8,128)(2,1)}, u32[]{:S(2)}, u32[]{:S(2)}) collective-permute-start(bf16[192,1024]{1,0:T(8,128)(2,1)S(1)} %slice.99), channel_id=1, source_target_pairs={{0,6},{2,0},{4,2},{6,4},{1,7},{3,1},{5,3},{7,5},{8,14},{10,8},{12,... | collective-permute-start | bytes 1179656 | tf_op jit(solution)/shard_map/ppermute | solution.py:30
  45.9 11.5 %collective-permute-start.5 = (bf16[384,1024]{1,0:T(8,128)(2,1)}, bf16[384,1024]{1,0:T(8,128)(2,1)}, u32[]{:S(2)}, u32[]{:S(2)}) collective-permute-start(bf16[384,1024]{1,0:T(8,128)(2,1)} %collective-permute-done.rest_1_), channel_id=1, source_target_pairs={{0,1},{1,0},{2,3},{3,2},{4,5},{5,4},{6,7},{7,6},{8,9},{9,8},{10,11... | collective-permute-start | bytes 2359304 | tf_op jit(solution)/shard_map/ppermute | solution.py:34
  48.0 9.4 %collective-permute-start.8 = (bf16[384,1024]{1,0:T(8,128)(2,1)S(1)}, bf16[384,1024]{1,0:T(8,128)(2,1)}, u32[]{:S(2)}, u32[]{:S(2)}) collective-permute-start(bf16[384,1024]{1,0:T(8,128)(2,1)S(1)} %collective-permute-done.1.rest_4_), channel_id=1, source_target_pairs={{0,1},{1,0},{2,3},{3,2},{4,5},{5,4},{6,7},{7,6},{8,9},{9,8},{10,11... | collective-permute-start | bytes 2359304 | tf_op jit(solution)/shard_map/ppermute | solution.py:34
  52.5 4.9 %collective-permute-start.6 = (bf16[192,1024]{1,0:T(8,128)(2,1)}, bf16[192,1024]{1,0:T(8,128)(2,1)}, u32[]{:S(2)}, u32[]{:S(2)}) collective-permute-start(bf16[192,1024]{1,0:T(8,128)(2,1)} %collective-permute-done.2.rest_2_), channel_id=1, source_target_pairs={{0,1},{1,0},{2,3},{3,2},{4,5},{5,4},{6,7},{7,6},{8,9},{9,8},{10,11... | collective-permute-start | bytes 1179656 | tf_op jit(solution)/shard_map/ppermute | solution.py:34
  54.9 2.5 collective-permute-start.7
  67.7 9.4 %copy-start.4 = (bf16[704,512]{1,0:T(8,128)(2,1)S(1)}, bf16[704,512]{1,0:T(8,128)(2,1)}, u32[]{:S(2)}) copy-start(bf16[704,512]{1,0:T(8,128)(2,1)} %copy-done.3) | copy-start | bytes 2162692
  89.0 1.1 copy-start.5
  90.1 1.0 copy-start.8
  90.1 1.0 copy-start.9
  91.3 8.5 %collective-permute-start.10 = (bf16[96,1408]{1,0:T(8,128)(2,1)S(1)}, bf16[96,1408]{1,0:T(8,128)(2,1)S(1)}, u32[]{:S(2)}, u32[]{:S(2)}) collective-permute-start(bf16[96,1408]{1,0:T(8,128)(2,1)S(1)} %get-tuple-element.63.refs_0_), channel_id=1, source_target_pairs={{0,8},{8,16},{16,24},{24,0},{1,9},{9,17},{17,25},{25,1},{2,10},{10... | collective-permute-start | bytes 811016 | tf_op jit(solution)/shard_map/ppermute | solution.py:30
  92.6 7.3 %collective-permute-start.9 = (bf16[96,1408]{1,0:T(8,128)(2,1)S(1)}, bf16[96,1408]{1,0:T(8,128)(2,1)S(1)}, u32[]{:S(2)}, u32[]{:S(2)}) collective-permute-start(bf16[96,1408]{1,0:T(8,128)(2,1)S(1)} %get-tuple-element.63.refs_0_), channel_id=1, source_target_pairs={{0,24},{8,0},{16,8},{24,16},{1,25},{9,1},{17,9},{25,17},{2,26},{10... | collective-permute-start | bytes 811016 | tf_op jit(solution)/shard_map/ppermute | solution.py:30
  94.1 8.6 %collective-permute-start.14 = (bf16[96,1408]{1,0:T(8,128)(2,1)S(1)}, bf16[96,1408]{1,0:T(8,128)(2,1)S(1)}, u32[]{:S(2)}, u32[]{:S(2)}) collective-permute-start(bf16[96,1408]{1,0:T(8,128)(2,1)S(1)} %get-tuple-element.62.refs_5_), channel_id=1, source_target_pairs={{0,32},{32,64},{64,96},{96,0},{1,33},{33,65},{65,97},{97,1},{2,34}... | collective-permute-start | bytes 811016 | tf_op jit(solution)/shard_map/ppermute | solution.py:30
  95.2 8.7 %collective-permute-start.13 = (bf16[96,1408]{1,0:T(8,128)(2,1)S(1)}, bf16[96,1408]{1,0:T(8,128)(2,1)S(1)}, u32[]{:S(2)}, u32[]{:S(2)}) collective-permute-start(bf16[96,1408]{1,0:T(8,128)(2,1)S(1)} %get-tuple-element.62.refs_5_), channel_id=1, source_target_pairs={{0,96},{32,0},{64,32},{96,64},{1,97},{33,1},{65,33},{97,65},{2,98}... | collective-permute-start | bytes 811016 | tf_op jit(solution)/shard_map/ppermute | solution.py:30
  99.8 9.0 %collective-permute-start.11 = (bf16[48,1408]{1,0:T(8,128)(2,1)S(1)}, bf16[48,1408]{1,0:T(8,128)(2,1)S(1)}, u32[]{:S(2)}, u32[]{:S(2)}) collective-permute-start(bf16[48,1408]{1,0:T(8,128)(2,1)S(1)} %slice.102), channel_id=1, source_target_pairs={{0,8},{8,16},{16,24},{24,0},{1,9},{9,17},{17,25},{25,1},{2,10},{10... | collective-permute-start | bytes 405512 | tf_op jit(solution)/shard_map/ppermute | solution.py:30
  99.9 8.9 %collective-permute-start.12 = (bf16[48,1408]{1,0:T(8,128)(2,1)S(1)}, bf16[48,1408]{1,0:T(8,128)(2,1)S(1)}, u32[]{:S(2)}, u32[]{:S(2)}) collective-permute-start(bf16[48,1408]{1,0:T(8,128)(2,1)S(1)} %slice.103), channel_id=1, source_target_pairs={{0,24},{8,0},{16,8},{24,16},{1,25},{9,1},{17,9},{25,17},{2,26},{10... | collective-permute-start | bytes 405512 | tf_op jit(solution)/shard_map/ppermute | solution.py:30
  102.7 8.4 %collective-permute-start.15 = (bf16[48,1408]{1,0:T(8,128)(2,1)S(1)}, bf16[48,1408]{1,0:T(8,128)(2,1)S(1)}, u32[]{:S(2)}, u32[]{:S(2)}) collective-permute-start(bf16[48,1408]{1,0:T(8,128)(2,1)S(1)} %slice.104), channel_id=1, source_target_pairs={{0,32},{32,64},{64,96},{96,0},{1,33},{33,65},{65,97},{97,1},{2,34}... | collective-permute-start | bytes 405512 | tf_op jit(solution)/shard_map/ppermute | solution.py:30
  103.9 7.9 %collective-permute-start.16 = (bf16[48,1408]{1,0:T(8,128)(2,1)S(1)}, bf16[48,1408]{1,0:T(8,128)(2,1)S(1)}, u32[]{:S(2)}, u32[]{:S(2)}) collective-permute-start(bf16[48,1408]{1,0:T(8,128)(2,1)S(1)} %slice.105), channel_id=1, source_target_pairs={{0,96},{32,0},{64,32},{96,64},{1,97},{33,1},{65,33},{97,65},{2,98}... | collective-permute-start | bytes 405512 | tf_op jit(solution)/shard_map/ppermute | solution.py:30
  112.9 48.2 %collective-permute-start.18 = (bf16[384,1408]{1,0:T(8,128)(2,1)S(1)}, bf16[384,1408]{1,0:T(8,128)(2,1)S(1)}, u32[]{:S(2)}, u32[]{:S(2)}) collective-permute-start(bf16[384,1408]{1,0:T(8,128)(2,1)S(1)} %get-tuple-element.19.rest_0_), channel_id=1, source_target_pairs={{0,32},{32,64},{64,96},{96,0},{1,33},{33,65},{65,97},{97,1},{2,34}... | collective-permute-start | bytes 3244040 | tf_op jit(solution)/shard_map/ppermute | solution.py:30
  113.9 47.4 %collective-permute-start.17 = (bf16[384,1408]{1,0:T(8,128)(2,1)S(1)}, bf16[384,1408]{1,0:T(8,128)(2,1)S(1)}, u32[]{:S(2)}, u32[]{:S(2)}) collective-permute-start(bf16[384,1408]{1,0:T(8,128)(2,1)S(1)} %get-tuple-element.19.rest_0_), channel_id=1, source_target_pairs={{0,96},{32,0},{64,32},{96,64},{1,97},{33,1},{65,33},{97,65},{2,98}... | collective-permute-start | bytes 3244040 | tf_op jit(solution)/shard_map/ppermute | solution.py:30
  116.5 48.2 %collective-permute-start.22 = (bf16[384,1408]{1,0:T(8,128)(2,1)}, bf16[384,1408]{1,0:T(8,128)(2,1)S(1)}, u32[]{:S(2)}, u32[]{:S(2)}) collective-permute-start(bf16[384,1408]{1,0:T(8,128)(2,1)} %get-tuple-element.20.rest_5_), channel_id=1, source_target_pairs={{0,8},{8,16},{16,24},{24,0},{1,9},{9,17},{17,25},{25,1},{2,10},{10... | collective-permute-start | bytes 3244040 | tf_op jit(solution)/shard_map/ppermute | solution.py:30
  116.5 48.4 %collective-permute-start.21 = (bf16[384,1408]{1,0:T(8,128)(2,1)}, bf16[384,1408]{1,0:T(8,128)(2,1)S(1)}, u32[]{:S(2)}, u32[]{:S(2)}) collective-permute-start(bf16[384,1408]{1,0:T(8,128)(2,1)} %get-tuple-element.20.rest_5_), channel_id=1, source_target_pairs={{0,24},{8,0},{16,8},{24,16},{1,25},{9,1},{17,9},{25,17},{2,26},{10... | collective-permute-start | bytes 3244040 | tf_op jit(solution)/shard_map/ppermute | solution.py:30
  161.1 3.6 %copy-start.10 = (bf16[384,1408]{1,0:T(8,128)(2,1)}, bf16[384,1408]{1,0:T(8,128)(2,1)S(1)}, u32[]{:S(2)}) copy-start(bf16[384,1408]{1,0:T(8,128)(2,1)S(1)} %collective-permute-done.18.rest_4_) | copy-start | bytes 3244036
  161.2 25.6 %collective-permute-start.19 = (bf16[192,1408]{1,0:T(8,128)(2,1)S(1)}, bf16[192,1408]{1,0:T(8,128)(2,1)S(1)}, u32[]{:S(2)}, u32[]{:S(2)}) collective-permute-start(bf16[192,1408]{1,0:T(8,128)(2,1)S(1)} %slice.106), channel_id=1, source_target_pairs={{0,32},{32,64},{64,96},{96,0},{1,33},{33,65},{65,97},{97,1},{2,34}... | collective-permute-start | bytes 1622024 | tf_op jit(solution)/shard_map/ppermute | solution.py:30
  161.3 3.6 %copy-start.11 = (bf16[384,1408]{1,0:T(8,128)(2,1)}, bf16[384,1408]{1,0:T(8,128)(2,1)S(1)}, u32[]{:S(2)}) copy-start(bf16[384,1408]{1,0:T(8,128)(2,1)S(1)} %collective-permute-done.17.rest_1_) | copy-start | bytes 3244036
  161.3 25.5 %collective-permute-start.20 = (bf16[192,1408]{1,0:T(8,128)(2,1)S(1)}, bf16[192,1408]{1,0:T(8,128)(2,1)S(1)}, u32[]{:S(2)}, u32[]{:S(2)}) collective-permute-start(bf16[192,1408]{1,0:T(8,128)(2,1)S(1)} %slice.107), channel_id=1, source_target_pairs={{0,96},{32,0},{64,32},{96,64},{1,97},{33,1},{65,33},{97,65},{2,98}... | collective-permute-start | bytes 1622024 | tf_op jit(solution)/shard_map/ppermute | solution.py:30
  164.7 23.3 %copy-start.12 = (bf16[384,1408]{1,0:T(8,128)(2,1)}, bf16[384,1408]{1,0:T(8,128)(2,1)S(1)}, u32[]{:S(2)}) copy-start(bf16[384,1408]{1,0:T(8,128)(2,1)S(1)} %collective-permute-done.22.rest_9_) | copy-start | bytes 3244036
  164.7 23.3 %collective-permute-start.23 = (bf16[192,1408]{1,0:T(8,128)(2,1)S(1)}, bf16[192,1408]{1,0:T(8,128)(2,1)S(1)}, u32[]{:S(2)}, u32[]{:S(2)}) collective-permute-start(bf16[192,1408]{1,0:T(8,128)(2,1)S(1)} %slice.108), channel_id=1, source_target_pairs={{0,8},{8,16},{16,24},{24,0},{1,9},{9,17},{17,25},{25,1},{2,10},{10... | collective-permute-start | bytes 1622024 | tf_op jit(solution)/shard_map/ppermute | solution.py:30
  164.8 23.2 %copy-start.13 = (bf16[384,1408]{1,0:T(8,128)(2,1)}, bf16[384,1408]{1,0:T(8,128)(2,1)S(1)}, u32[]{:S(2)}) copy-start(bf16[384,1408]{1,0:T(8,128)(2,1)S(1)} %collective-permute-done.21.rest_6_) | copy-start | bytes 3244036
  164.9 23.1 %collective-permute-start.24 = (bf16[192,1408]{1,0:T(8,128)(2,1)S(1)}, bf16[192,1408]{1,0:T(8,128)(2,1)S(1)}, u32[]{:S(2)}, u32[]{:S(2)}) collective-permute-start(bf16[192,1408]{1,0:T(8,128)(2,1)S(1)} %slice.109), channel_id=1, source_target_pairs={{0,24},{8,0},{16,8},{24,16},{1,25},{9,1},{17,9},{25,17},{2,26},{10... | collective-permute-start | bytes 1622024 | tf_op jit(solution)/shard_map/ppermute | solution.py:30
  200.5 11.0 %collective-permute-start.25 = (bf16[1536,512]{1,0:T(8,128)(2,1)}, bf16[1536,512]{1,0:T(8,128)(2,1)S(1)}, u32[]{:S(2)}, u32[]{:S(2)}) collective-permute-start(bf16[1536,512]{1,0:T(8,128)(2,1)} %get-tuple-element.22), channel_id=1, source_target_pairs={{0,1},{1,0},{2,3},{3,2},{4,5},{5,4},{6,7},{7,6},{8,9},{9,8},{10,11... | collective-permute-start | bytes 4718600 | tf_op jit(solution)/shard_map/ppermute | solution.py:34
  213.5 7.5 %collective-permute-start.26 = (bf16[192,512]{1,0:T(8,128)(2,1)S(1)}, bf16[192,512]{1,0:T(8,128)(2,1)S(1)}, u32[]{:S(2)}, u32[]{:S(2)}) collective-permute-start(bf16[192,512]{1,0:T(8,128)(2,1)S(1)} %get-tuple-element.56), channel_id=1, source_target_pairs={{0,2},{2,4},{4,6},{6,0},{1,3},{3,5},{5,7},{7,1},{8,10},{10,12},{12... | collective-permute-start | bytes 589832 | tf_op jit(solution)/shard_map/ppermute | solution.py:30
  214.7 6.2 %collective-permute-start.28 = (bf16[192,512]{1,0:T(8,128)(2,1)S(1)}, bf16[192,512]{1,0:T(8,128)(2,1)S(1)}, u32[]{:S(2)}, u32[]{:S(2)}) collective-permute-start(bf16[192,512]{1,0:T(8,128)(2,1)S(1)} %get-tuple-element.57), channel_id=1, source_target_pairs={{0,6},{2,0},{4,2},{6,4},{1,7},{3,1},{5,3},{7,5},{8,14},{10,8},{12,... | collective-permute-start | bytes 589832 | tf_op jit(solution)/shard_map/ppermute | solution.py:30
  221.1 16.4 %collective-permute-start.27 = (bf16[384,512]{1,0:T(8,128)(2,1)S(1)}, bf16[384,512]{1,0:T(8,128)(2,1)}, u32[]{:S(2)}, u32[]{:S(2)}) collective-permute-start(bf16[384,512]{1,0:T(8,128)(2,1)S(1)} %pad_maximum_fusion.1), channel_id=1, source_target_pairs={{0,2},{2,4},{4,6},{6,0},{1,3},{3,5},{5,7},{7,1},{8,10},{10,12},{12... | collective-permute-start | bytes 1179656 | tf_op jit(solution)/shard_map/ppermute | solution.py:30
  222.1 15.4 %collective-permute-start.29 = (bf16[384,512]{1,0:T(8,128)(2,1)S(1)}, bf16[384,512]{1,0:T(8,128)(2,1)}, u32[]{:S(2)}, u32[]{:S(2)}) collective-permute-start(bf16[384,512]{1,0:T(8,128)(2,1)S(1)} %pad_maximum_fusion.2), channel_id=1, source_target_pairs={{0,6},{2,0},{4,2},{6,4},{1,7},{3,1},{5,3},{7,5},{8,14},{10,8},{12,... | collective-permute-start | bytes 1179656 | tf_op jit(solution)/shard_map/ppermute | solution.py:30
  239.7 1.2 copy-start.2
  (1 other events, 0.9 us)
Sparse Core Ops, SparseCore 0:
  10.7 56.9 all-gather.1
  90.3 132.4 reduce-scatter.1
